TPU v7x, 32 devices: a whole 2x2x4 slice. The times are simulated.
32 devices in a mesh: sp: 8 (over z, y), tp: 4 (over x, core).
Axes of the slice: x: 2, y: 2, z: 4, core: 2. Of those that a mesh axis runs over, the one named last changes fastest.
Arguments:
- inputs: bfloat16 [4096, 4096], P('sp', 'tp'), may hold values from -24 to 24
- length: int32 [1], replicated, may hold values from 2049 to 4096
- win_query: bfloat16 [4096, 1536], P(None, 'tp'), may hold values from -8 to 8
- win_key: bfloat16 [4096, 512], P(None, 'tp'), may hold values from -8 to 8
- win_value: bfloat16 [4096, 512], P(None, 'tp'), may hold values from -1.5 to 1.5
- sink_logit: float32 [24], P('tp'), may hold values from 4 to 8
- diff_query: bfloat16 [4096, 1024], P(None, 'tp'), may hold values from -8 to 8
- diff_key: bfloat16 [4096, 1024], P(None, 'tp'), may hold values from -8 to 8
- diff_value: bfloat16 [4096, 1024], P(None, 'tp'), may hold values from -0.09375 to 0.09375
- mix_lambda: float32 [16], P('tp'), may hold values from 0.3 to 0.8
- head_gain: float32 [64], replicated, may hold values from 0.1 to 1.9
- win_out: bfloat16 [1536, 4096], P('tp'), may hold values from -0.125 to 0.125
- diff_out: bfloat16 [1024, 4096], P('tp'), may hold values from -0.125 to 0.125
Outputs:
- merged_out: bfloat16 [4096, 4096], P(('sp', 'tp'))
All inputs are finite; a program needn't handle non-finite values.
Results may differ from a plain program's by a relative error of at most 0.015.
Values may be sent and summed in bfloat16 or wider, within the bound.
No kernel may reach another device: no remote copies, remote signals or barrier semaphores. Data moves between devices by JAX's collectives and lax.ppermute only.
A program may use at most 128 MiB of HBM per device.

v0:
```python
import functools
import math

import jax
import jax.numpy as jnp
from jax import lax
from jax.experimental import pallas as pl
from jax.experimental.pallas import tpu as pltpu
from jax.sharding import PartitionSpec as P

HEAD = 64
DQK = 32
GROUP = 3
WINDOW = 128

epsilon = 1e-06
masked_score = -1e30
LOG2E = math.log2(math.e)
SAFE_BOUND = 90.0


def whole(shape):
    return pl.BlockSpec(shape, lambda *_: (0,) * len(shape))


def smem():
    return pl.BlockSpec(memory_space=pltpu.SMEM)


def cost(flops, bytes_accessed=0, transcendentals=0):
    return pl.CostEstimate(
        flops=flops, bytes_accessed=bytes_accessed, transcendentals=transcendentals
    )


def flip(axis, bits):
    return [(i, i ^ bits) for i in range(lax.axis_size(axis))]


def add_slice(x, weight_refs, acc_ref):
    weight = jnp.concatenate([ref[...] for ref in weight_refs], axis=1)
    acc_ref[...] += jnp.dot(x, weight, preferred_element_type=jnp.float32)


def first_kernel(steps, scal_ref, own_ref, sib_ref, *refs):
    acc_ref = refs[-1]
    j = pl.program_id(0)

    @pl.when(j == 0)
    def _():
        acc_ref[...] = jnp.zeros_like(acc_ref)

    x = jnp.where(j < steps, own_ref[...], sib_ref[...])
    add_slice(x, refs[:-1], acc_ref)


def project_near(own, sib, weights, scal, steps):
    rows, depth = own.shape
    block = depth // steps
    width = sum(w.shape[1] for w in weights)

    def at_weight(j, scal):
        return ((scal[2] ^ (j // steps)) * steps + j % steps, 0)

    grid_spec = pltpu.PrefetchScalarGridSpec(
        num_scalar_prefetch=1,
        grid=(2 * steps,),
        in_specs=[
            pl.BlockSpec((rows, block), lambda j, idx: (0, jnp.minimum(j, steps - 1))),
            pl.BlockSpec((rows, block), lambda j, idx: (0, jnp.maximum(j - steps, 0))),
        ]
        + [pl.BlockSpec((block, w.shape[1]), at_weight) for w in weights],
        out_specs=pl.BlockSpec((rows, width), lambda j, idx: (0, 0)),
    )
    return pl.pallas_call(
        functools.partial(first_kernel, steps),
        grid_spec=grid_spec,
        out_shape=jax.ShapeDtypeStruct((rows, width), jnp.float32),
        compiler_params=pltpu.CompilerParams(
            dimension_semantics=("arbitrary",), vmem_limit_bytes=24 << 20
        ),
        cost_estimate=cost(4 * rows * depth * width, 4 * depth * width),
        name="project_near",
    )(scal, own, sib, *weights)


def fetch_kernel(pieces, scal_ref, *refs):
    count = len(pieces)
    sources, targets, semaphores = refs[:count], refs[count : 2 * count], refs[2 * count]
    copies = []
    for source, target, slices in zip(sources, targets, pieces):
        depth = target.shape[0] // len(slices)
        for i, k in enumerate(slices):
            at = 0 if k is None else pl.multiple_of((scal_ref[2] ^ k) * depth, depth)
            copies.append(
                pltpu.make_async_copy(
                    source.at[pl.ds(at, depth), :],
                    target.at[pl.ds(i * depth, depth), :],
                    semaphores.at[len(copies)],
                )
            )
    for copy in copies:
        copy.start()
    for copy in copies:
        copy.wait()


def fetch(scal, arrays, slices, tp):
    shapes = [
        (a.shape[0] if slices == [None] else a.shape[0] // tp * len(slices), a.shape[1])
        for a in arrays
    ]
    return pl.pallas_call(
        functools.partial(fetch_kernel, [slices] * len(arrays)),
        in_specs=[smem()] + [pl.BlockSpec(memory_space=pl.ANY)] * len(arrays),
        out_specs=[pl.BlockSpec(memory_space=pltpu.VMEM)] * len(arrays),
        out_shape=[pltpu.VMEM(shape, jnp.bfloat16) for shape in shapes],
        scratch_shapes=[pltpu.SemaphoreType.DMA((len(arrays) * len(slices),))],
        compiler_params=pltpu.CompilerParams(vmem_limit_bytes=1 << 20),
        cost_estimate=cost(3 << 30),
        name="fetch",
    )(scal, *arrays)


def far_kernel(count, heads, parts, scal_ref, acc_ref, *refs):
    xs = refs[:count]
    weight_refs = refs[count : count + 6]
    qt_ref, kv_ref = refs[count + 6 : count + 8]
    slot_refs = refs[count + 8 : count + 8 + heads]
    buf_ref = refs[count + 8 + heads]
    rows, _ = xs[0].shape
    here = scal_ref[0] // parts

    def project(which):
        whole_x = jnp.concatenate([x[...] for x in xs], axis=1)
        weight = jnp.concatenate([weight_refs[i][...] for i in which], axis=1)
        low = sum(weight_refs[i].shape[1] for i in range(which[0]))
        span = weight.shape[1]
        total = acc_ref[:, low : low + span] + jnp.dot(
            whole_x, weight, preferred_element_type=jnp.float32
        )
        ends = [sum(weight_refs[i].shape[1] for i in which[:n]) for n in range(len(which) + 1)]
        return [total[:, a:b] for a, b in zip(ends[:-1], ends[1:])]

    win_q, win_k, win_v, diff_q, diff_k, diff_v = project(range(6))
    diff_q = diff_q * (LOG2E * DQK ** (-0.5))
    for h in range(heads):
        lanes = slice(h * HEAD, (h + 1) * HEAD)
        q, k, v = diff_q[:, lanes], diff_k[:, lanes], diff_v[:, lanes]
        buf_ref[h, 0:rows, :] = jnp.concatenate([k, v], axis=1).astype(jnp.bfloat16)
        pair = jnp.concatenate([q[: rows // 2], q[rows // 2 :]], axis=1)
        buf_ref[h, rows : rows + rows // 2, :] = pair.astype(jnp.bfloat16)
    for slot in range(heads):
        slot_refs[slot][...] = buf_ref[slot ^ here]
    qt_ref[...] = jnp.transpose(win_q * (LOG2E * HEAD ** (-0.5))).astype(jnp.bfloat16)
    kv_ref[...] = jnp.concatenate([win_k, win_v], axis=1).astype(jnp.bfloat16)


def project_far(acc, chunk, rows, xs, weights, scal, heads, parts):
    depth = xs[0].shape[1]
    count = len(xs)
    width = acc.shape[1]
    kv_width = weights[1].shape[1] + weights[2].shape[1]
    q_width = weights[0].shape[1]
    shapes = [(q_width, rows), (rows, kv_width)] + [(rows + rows // 2, 2 * HEAD)] * heads
    return pl.pallas_call(
        functools.partial(far_kernel, count, heads, parts),
        in_specs=[smem(), pl.BlockSpec((rows, width), lambda j: (chunk, 0))]
        + [whole((rows, depth))] * count
        + [pl.BlockSpec(memory_space=pltpu.VMEM)] * 6,
        out_specs=[whole(shape) for shape in shapes],
        out_shape=[jax.ShapeDtypeStruct(shape, jnp.bfloat16) for shape in shapes],
        scratch_shapes=[pltpu.VMEM((heads, rows + rows // 2, 2 * HEAD), jnp.bfloat16)],
        grid=(1,),
        compiler_params=pltpu.CompilerParams(vmem_limit_bytes=24 << 20),
        cost_estimate=cost(2 * count * rows * depth * width),
        name="project_far",
    )(scal, acc, *xs, *weights)


def window_kernel(chunks, rows, kv_local, scal_ref, sink_ref, *refs):
    q_refs = refs[:chunks]
    kv_refs = refs[chunks : 2 * chunks]
    low_ref, high_ref, rows_ref, keys, values_t, out_ref = refs[2 * chunks :]
    here, live = scal_ref[0], scal_ref[1]
    span = rows + 2 * WINDOW
    size = rows // chunks
    keys[0:WINDOW, :] = low_ref[...]
    for c in range(chunks):
        keys[WINDOW + c * size : WINDOW + (c + 1) * size, :] = kv_refs[c][...]
    keys[WINDOW + rows : span, :] = high_ref[...]
    k_width = kv_local * HEAD
    turned = jnp.transpose(keys[:, k_width:].astype(jnp.float32)).astype(jnp.bfloat16)
    tail = (lax.broadcasted_iota(jnp.int32, (16, span), 0) == 0).astype(jnp.bfloat16)
    for h in range(kv_local):
        values_t[h, 0:HEAD, :] = turned[h * HEAD : (h + 1) * HEAD]
        values_t[h, HEAD : HEAD + 16, :] = tail
    step = 128
    for b in range(rows // step):
        first = here * rows + b * step

        @pl.when(first >= live)
        def _():
            out_ref[:, b * step : (b + 1) * step] = jnp.zeros(
                (out_ref.shape[0], step), jnp.float32
            )

        @pl.when(first < live)
        def _():
            wide = step + 2 * WINDOW
            c, at = (b * step) // size, (b * step) % size
            key_at = lax.broadcasted_iota(jnp.int32, (wide, step), 0)
            query_at = lax.broadcasted_iota(jnp.int32, (wide, step), 1)
            key_pos = first - WINDOW + key_at
            gap = key_at - WINDOW - query_at
            allowed = (
                (gap <= WINDOW) & (gap >= -WINDOW) & (key_pos >= 0) & (key_pos < live)
            )
            live_row = (
                first + lax.broadcasted_iota(jnp.int32, (1, step), 1)
            ) < live
            for h in range(kv_local):
                key_block = keys[b * step : b * step + wide, h * HEAD : (h + 1) * HEAD]
                value_block = values_t[h, :, b * step : b * step + wide]
                for g in range(GROUP):
                    head = h * GROUP + g
                    q = q_refs[c][head * HEAD : (head + 1) * HEAD, at : at + step]
                    s = jnp.dot(key_block, q, preferred_element_type=jnp.float32)
                    s = jnp.where(allowed, s, masked_score)
                    sink = sink_ref[head] * LOG2E
                    top = jnp.maximum(jnp.max(s, axis=0, keepdims=True), sink)
                    e = jnp.exp2(s - top).astype(jnp.bfloat16)
                    mixed = jnp.dot(value_block, e, preferred_element_type=jnp.float32)
                    total = mixed[HEAD : HEAD + 1] + jnp.exp2(sink - top)
                    result = jnp.where(live_row, mixed[0:HEAD] / total, 0.0)
                    out_ref[head * HEAD : (head + 1) * HEAD, b * step : (b + 1) * step] = (
                        result
                    )

        block = out_ref[:, b * step : (b + 1) * step]
        rows_ref[b * step : (b + 1) * step, :] = jnp.transpose(block).astype(jnp.bfloat16)


def window_part(scal, sink_logit, q_parts, kv_parts, low, high):
    chunks = len(q_parts)
    q_width, size = q_parts[0].shape
    kv_width = kv_parts[0].shape[1]
    rows = size * chunks
    kv_local = kv_width // (2 * HEAD)
    operands = (*q_parts, *kv_parts, low, high)
    return pl.pallas_call(
        functools.partial(window_kernel, chunks, rows, kv_local),
        in_specs=[smem(), smem()] + [whole(a.shape) for a in operands],
        out_specs=whole((rows, q_width)),
        out_shape=jax.ShapeDtypeStruct((rows, q_width), jnp.bfloat16),
        scratch_shapes=[
            pltpu.VMEM((rows + 2 * WINDOW, kv_width), jnp.bfloat16),
            pltpu.VMEM((kv_local, HEAD + 16, rows + 2 * WINDOW), jnp.bfloat16),
            pltpu.VMEM((q_width, rows), jnp.float32),
        ],
        grid=(1,),
        compiler_params=pltpu.CompilerParams(vmem_limit_bytes=16 << 20),
        cost_estimate=cost(40 * q_width * rows * 384),
        name="window",
    )(scal, sink_logit, *operands)


def diff_kernel(chunks, rows, parts, count, scal_ref, lam_ref, gain_ref, *refs):
    heads = count // parts
    kv_refs = refs[: chunks * parts]
    q_refs = refs[chunks * parts : chunks * (parts + heads)]
    out_refs = refs[chunks * (parts + heads) : chunks * (parts + heads) + heads]
    out_ref, keys, values_t, queries, weighted, running = refs[-6:]
    here, live = scal_ref[0], scal_ref[1]
    size = rows // chunks
    total = rows * count
    step = 512
    pair = 2 * size

    top_key = jnp.zeros((1, 2 * HEAD), jnp.float32)
    queries[...] = jnp.zeros_like(queries)
    for c in range(chunks):
        for d in range(count):
            at = pl.multiple_of((here ^ d) * rows + c * size, size)
            block = kv_refs[c * parts + d % parts][d // parts]
            keys[pl.ds(at, size), :] = block
            wide = block.astype(jnp.float32)
            top_key = jnp.maximum(top_key, jnp.max(jnp.abs(wide), axis=0, keepdims=True))
            alive = (at + lax.broadcasted_iota(jnp.int32, (1, size), 1)) < live
            turned = jnp.where(alive, jnp.transpose(wide)[HEAD:], 0.0)
            values_t[0:HEAD, pl.ds(at, size)] = turned.astype(jnp.bfloat16)
            if d % parts == 0:
                half = size // 2
                pairs = q_refs[c * heads + d // parts][size : size + half, :]
                turned = jnp.transpose(pairs.astype(jnp.float32))
                turned = jnp.concatenate([turned[0:HEAD], turned[HEAD:]], axis=1)
                turned = turned.astype(jnp.bfloat16)
                tile = c * heads + d // parts
                queries[tile, 0:DQK, 0:size] = turned[0:DQK]
                queries[tile, DQK : 2 * DQK, size:pair] = turned[DQK:]
    counted = lax.broadcasted_iota(jnp.int32, (16, total), 0) == 0
    counted &= lax.broadcasted_iota(jnp.int32, (16, total), 1) < live
    values_t[HEAD : HEAD + 16, :] = counted.astype(jnp.bfloat16)
    limit = jnp.transpose(jnp.broadcast_to(top_key, (8, 2 * HEAD)))[:, 0:1]
    gain = jnp.transpose(jnp.broadcast_to(gain_ref[...], (8, HEAD)))[:, 0:1]

    full = live // step
    left = live - full * step

    def tile_body(tile, carry):
        c, zd = tile // heads, tile % heads
        first = (here ^ (zd * parts)) * rows + c * size

        @pl.when(first >= live)
        def _():
            out_ref[tile] = jnp.zeros(out_ref.shape[1:], out_ref.dtype)

        @pl.when(first < live)
        def _():
            q = queries[tile]
            bound = jnp.max(jnp.sum(jnp.abs(q.astype(jnp.float32)) * limit, axis=0, keepdims=True))
            safe = bound < SAFE_BOUND

            def scores(j):
                at = pl.multiple_of(j * step, step)
                return jnp.dot(keys[pl.ds(at, step), :], q, preferred_element_type=jnp.float32)

            def values(j):
                return values_t[:, pl.ds(pl.multiple_of(j * step, step), step)]

            def inside(shape):
                return lax.broadcasted_iota(jnp.int32, shape, 0) < left

            weighted[...] = jnp.zeros_like(weighted)

            @pl.when(safe)
            def _():
                def several(j, number):
                    raised = [jnp.exp2(scores(j + i)).astype(jnp.bfloat16) for i in range(number)]
                    added = [
                        jnp.dot(values(j + i), e, preferred_element_type=jnp.float32)
                        for i, e in enumerate(raised)
                    ]
                    weighted[...] += functools.reduce(lambda a, b: a + b, added)

                def one(j, carry):
                    several(4 * j, 4)
                    return carry

                pairs = (live + 2 * step - 1) // (2 * step)
                lax.fori_loop(0, pairs // 2, one, 0)

                @pl.when(pairs % 2 == 1)
                def _():
                    several(2 * (pairs - 1), 2)

            @pl.when(jnp.logical_not(safe))
            def _():
                running[...] = jnp.full_like(running, masked_score)

                def add(j, s):
                    old = running[...]
                    new = jnp.maximum(old, jnp.max(s, axis=0, keepdims=True))
                    e = jnp.exp2(s - new).astype(jnp.bfloat16)
                    weighted[...] = weighted[...] * jnp.exp2(old - new) + jnp.dot(
                        values(j), e, preferred_element_type=jnp.float32
                    )
                    running[...] = new

                def one(j, carry):
                    add(j, scores(j))
                    return carry

                lax.fori_loop(0, full, one, 0)

                @pl.when(left > 0)
                def _():
                    s = scores(full)
                    add(full, jnp.where(inside(s.shape), s, masked_score))

            maps = weighted[0:HEAD, :] / weighted[HEAD : HEAD + 1, :]
            mix = maps[:, 0:size] - lam_ref[here // parts] * maps[:, size:pair]
            normed = mix * lax.rsqrt(jnp.mean(mix * mix, axis=0, keepdims=True) + epsilon)
            normed = normed * gain
            position = first + lax.broadcasted_iota(jnp.int32, (1, size), 1)
            out_ref[tile] = jnp.where(position < live, normed, 0.0).astype(jnp.bfloat16)

        return carry

    lax.fori_loop(0, chunks * heads, tile_body, 0)
    for c in range(chunks):
        for d in range(heads):
            out_refs[d][c] = out_ref[c * heads + d]


def diff_part(scal, mix_lambda, gain, kvs, qs, chunks, rows, parts):
    heads = len(qs) // chunks
    count = heads * parts
    size = rows // chunks
    blocks = (*kvs, *qs)
    return pl.pallas_call(
        functools.partial(diff_kernel, chunks, rows, parts, count),
        in_specs=[smem(), smem(), whole(gain.shape)] + [whole(a.shape) for a in blocks],
        out_specs=[whole((chunks, HEAD, size))] * heads,
        out_shape=[jax.ShapeDtypeStruct((chunks, HEAD, size), jnp.bfloat16)] * heads,
        scratch_shapes=[
            pltpu.VMEM((chunks * heads, HEAD, size), jnp.bfloat16),
            pltpu.VMEM((rows * count, 2 * HEAD), jnp.bfloat16),
            pltpu.VMEM((HEAD + 16, rows * count), jnp.bfloat16),
            pltpu.VMEM((chunks * heads, 2 * HEAD, 2 * size), jnp.bfloat16),
            pltpu.VMEM((HEAD + 16, 2 * size), jnp.float32),
            pltpu.VMEM((1, 2 * size), jnp.float32),
        ],
        grid=(1,),
        compiler_params=pltpu.CompilerParams(vmem_limit_bytes=32 << 20),
        cost_estimate=cost(1000 * heads * rows * rows * count),
        name="differential",
    )(scal, mix_lambda, gain, *blocks)


def out_kernel(heads, parts, begin, scal_ref, win_keep_ref, win_send_ref, *refs):
    diff_refs = refs[:heads]
    win_w_ref, diff_w_ref, keep_ref, send_ref, stacked = refs[heads:]
    here, core = scal_ref[0] // parts, scal_ref[2] % 2
    half = stacked.shape[1]
    win_width = win_keep_ref.shape[1]

    @pl.when(pl.program_id(0) == 0)
    def _():
        stacked[0, :, 0:win_width] = win_keep_ref[...]
        stacked[1, :, 0:win_width] = win_send_ref[...]
        pieces = []
        for h in range(heads):
            piece = diff_refs[0][0]
            for d in range(1, heads):
                piece = jnp.where((here ^ d) == h, diff_refs[d][0], piece)
            pieces.append(piece)
        turned = jnp.transpose(jnp.concatenate(pieces, axis=0).astype(jnp.float32))
        turned = turned.astype(jnp.bfloat16)
        stacked[core, :, win_width:] = turned[0:half]
        stacked[1 - core, :, win_width:] = turned[half:]

    block = keep_ref.shape[1]
    at = pl.multiple_of(begin + pl.program_id(0) * block, block)
    lanes = pl.ds(at, block)
    weight = jnp.concatenate([win_w_ref[:, lanes], diff_w_ref[:, lanes]], axis=0)
    for i, ref in enumerate((keep_ref, send_ref)):
        ref[...] = jnp.dot(stacked[i], weight, preferred_element_type=jnp.float32).astype(
            jnp.bfloat16
        )


def out_part(scal, offset, win_rows, diffs, win_out, diff_out, begin, width, block, parts):
    heads = len(diffs)
    depth = win_out.shape[0] + diff_out.shape[0]
    size = diffs[0].shape[2]
    half = size // 2
    q_width = win_rows.shape[1]

    def rows_at(bit):
        return lambda j, scal: (scal[2] ^ (2 * offset + bit), 0)

    grid_spec = pltpu.PrefetchScalarGridSpec(
        num_scalar_prefetch=1,
        grid=(width // block,),
        in_specs=[pl.BlockSpec((half, q_width), rows_at(bit)) for bit in range(2)]
        + [
            pl.BlockSpec((1, HEAD, size), lambda j, scal: ((scal[2] // 2) ^ offset, 0, 0))
            for _ in diffs
        ]
        + [pl.BlockSpec(memory_space=pltpu.VMEM)] * 2,
        out_specs=[pl.BlockSpec((half, block), lambda j, scal: (0, j))] * 2,
        scratch_shapes=[pltpu.VMEM((2, half, depth), jnp.bfloat16)],
    )
    return pl.pallas_call(
        functools.partial(out_kernel, heads, parts, begin),
        grid_spec=grid_spec,
        out_shape=[jax.ShapeDtypeStruct((half, width), jnp.bfloat16)] * 2,
        compiler_params=pltpu.CompilerParams(
            dimension_semantics=("arbitrary",), vmem_limit_bytes=16 << 20
        ),
        cost_estimate=cost(2 * size * depth * width),
        name="project_out",
    )(scal, win_rows, win_rows, *diffs, win_out, diff_out)


def body(
    inputs,
    length,
    win_query,
    win_key,
    win_value,
    sink_logit,
    diff_query,
    diff_key,
    diff_value,
    mix_lambda,
    head_gain,
    win_out,
    diff_out,
):
    rows = inputs.shape[0]
    sp, tp = lax.axis_size("sp"), lax.axis_size("tp")
    chips = tp // 2
    size = rows // chips
    heads = mix_lambda.shape[0]
    parts = sp // heads
    here, me = lax.axis_index("sp"), lax.axis_index("tp")
    weights = (win_query, win_key, win_value, diff_query, diff_key, diff_value)
    steps = 2
    scal = jnp.stack([here, length[0], me]).astype(jnp.int32)
    far_weights = fetch(scal, weights, list(range(2, tp)), tp)
    out_weights = fetch(scal, (win_out, diff_out), [None], tp)

    pieces = [inputs[c * size : (c + 1) * size] for c in range(chips)]
    far = [
        [lax.ppermute(pieces[c], "tp", flip("tp", 2 * o)) for o in range(1, chips)]
        for c in range(chips)
    ]
    sib = lax.ppermute(inputs, "tp", flip("tp", 1))
    acc = project_near(inputs, sib, weights, scal, steps)
    q_parts, kv_parts, kvs, qs = [], [], [], []
    for c in range(chips):
        xs = []
        for piece in far[c]:
            xs += [piece, lax.ppermute(piece, "tp", flip("tp", 1))]
        q_t, kv, *slots = project_far(acc, c, size, xs, far_weights, scal, heads, parts)
        q_parts.append(q_t)
        kv_parts.append(kv)
        moved = [slots[0]]
        for d in range(1, heads):
            moved.append(lax.ppermute(slots[d], "sp", flip("sp", d * parts)))
        mine = jnp.stack([m[:size] for m in moved])
        kvs += [mine] + [lax.ppermute(mine, "sp", flip("sp", e)) for e in range(1, parts)]
        qs += moved

    up = [(i, i + 1) for i in range(sp - 1)]
    down = [(i + 1, i) for i in range(sp - 1)]
    low = lax.ppermute(kv_parts[-1][size - WINDOW :], "sp", up)
    high = lax.ppermute(kv_parts[0][:WINDOW], "sp", down)
    win_rows = window_part(scal, sink_logit, q_parts, kv_parts, low, high)

    gain = head_gain.reshape(1, HEAD)
    mixed = diff_part(scal, mix_lambda, gain, kvs, qs, chips, rows, parts)
    diffs = [mixed[0]]
    for d in range(1, heads):
        diffs.append(lax.ppermute(mixed[d], "sp", flip("sp", d * parts)))

    width = win_out.shape[1]
    block = width // 4

    def project(o, begin, end):
        return out_part(
            scal, o, win_rows, diffs, *out_weights, begin, end - begin, block, parts
        )

    def add(*values):
        return functools.reduce(lambda a, b: a + b, [v.astype(jnp.float32) for v in values])

    cuts = (0, width // 4, width)
    arrived = []
    for begin, end in zip(cuts[:-1], cuts[1:]):
        count = 1 if begin == 0 else 2
        span = (end - begin) // count
        crossed = [[] for _ in range(count)]
        for o in range(1, chips):
            keep, away = project(o, begin, end)
            other = lax.ppermute(away, "tp", flip("tp", 1))
            pair = add(keep, other).astype(jnp.bfloat16)
            for i in range(count):
                piece = pair[:, i * span : (i + 1) * span]
                crossed[i].append(lax.ppermute(piece, "tp", flip("tp", 2 * o)))
        arrived += crossed
    keep, away = project(0, 0, width)
    other = lax.ppermute(away, "tp", flip("tp", 1))
    outs, begin = [], 0
    for crossed in arrived:
        end = begin + crossed[0].shape[1]
        outs.append(add(keep[:, begin:end], other[:, begin:end], *crossed).astype(jnp.bfloat16))
        begin = end
    return jnp.concatenate(outs, axis=1)


def solution(mesh):
    placed = (
        P("sp", "tp"),
        P(),
        P(None, "tp"),
        P(None, "tp"),
        P(None, "tp"),
        P("tp"),
        P(None, "tp"),
        P(None, "tp"),
        P(None, "tp"),
        P("tp"),
        P(),
        P("tp", None),
        P("tp", None),
    )

    return jax.shard_map(
        body, mesh=mesh, in_specs=placed, out_specs=P(("sp", "tp"), None), check_vma=False
    )
```

profile of v0, /device:TPU:0, one launch (start us, length us, event | category | flops | bytes accessed | tf_op | source)
XLA Modules:
  0.0 157.0 jit_solution(3354145653796812420)
XLA Ops:
  0.0 0.5 collective-permute-start
  0.5 2.4 %fusion = (bf16[256,1024]{1,0:T(8,128)(2,1)}, bf16[256,1024]{1,0:T(8,128)(2,1)}) fusion(bf16[512,1024]{1,0:T(8,128)(2,1)} %own_ref.1), kind=kLoop, calls=%fused_computation.17 | loop fusion | bytes 2097152 | tf_op jit(solution)/shard_map/slice | solution.py:515
  2.9 2.5 %collective-permute-start.1 = (bf16[256,1024]{1,0:T(8,128)(2,1)}, bf16[256,1024]{1,0:T(8,128)(2,1)}, u32[]{:S(2)}, u32[]{:S(2)}) collective-permute-start(bf16[256,1024]{1,0:T(8,128)(2,1)} %get-tuple-element.68), channel_id=1, source_target_pairs={{0,2},{1,3},{2,0},{3,1},{4,6},{5,7},{6,4},{7,5},{8,10},{9,11},{10,... | collective-permute-start | bytes 1572872 | tf_op jit(solution)/shard_map/ppermute | solution.py:517
  6.0 0.1 pad_add_fusion.scal_ref
  6.1 12.3 %collective-permute-done.1.refs_0_ = bf16[256,1024]{1,0:T(8,128)(2,1)} collective-permute-done((bf16[256,1024]{1,0:T(8,128)(2,1)}, bf16[256,1024]{1,0:T(8,128)(2,1)}, u32[]{:S(2)}, u32[]{:S(2)}) %collective-permute-start.1) | collective-permute-done | bytes 524320 | tf_op jit(solution)/shard_map/ppermute | solution.py:517
  18.5 1.9 %copy-done.1 = bf16[4096,384]{1,0:T(8,128)(2,1)S(1)} copy-done((bf16[4096,384]{1,0:T(8,128)(2,1)S(1)}, bf16[4096,384]{1,0:T(8,128)(2,1)}, u32[]{:S(2)}) %copy-start.1) | copy-done | bytes 3145752
  20.3 1.6 %copy-done.4 = bf16[4096,256]{1,0:T(8,128)(2,1)S(1)} copy-done((bf16[4096,256]{1,0:T(8,128)(2,1)S(1)}, bf16[4096,256]{1,0:T(8,128)(2,1)}, u32[]{:S(2)}) %copy-start.4) | copy-done | bytes 2097176
  21.9 1.6 %copy-done.6 = bf16[4096,256]{1,0:T(8,128)(2,1)S(1)} copy-done((bf16[4096,256]{1,0:T(8,128)(2,1)S(1)}, bf16[4096,256]{1,0:T(8,128)(2,1)}, u32[]{:S(2)}) %copy-start.6) | copy-done | bytes 2097176
  23.5 1.2 copy-done.8
  24.8 1.2 copy-done.10
  26.0 1.1 fetch.2
  27.1 2.3 %collective-permute-done.3.refs_0_ = bf16[256,1024]{1,0:T(8,128)(2,1)} collective-permute-done((bf16[256,1024]{1,0:T(8,128)(2,1)}, bf16[256,1024]{1,0:T(8,128)(2,1)}, u32[]{:S(2)}, u32[]{:S(2)}) %collective-permute-start.3) | collective-permute-done | bytes 524320 | tf_op jit(solution)/shard_map/ppermute | solution.py:517
  29.4 0.3 copy-done.11
  29.7 5.1 %project_near.1.acc_ref = f32[512,1408]{1,0:T(8,128)S(1)} custom-call(s32[3]{0:T(128)S(1)} %pad_add_fusion.scal_ref, bf16[512,1024]{1,0:T(8,128)(2,1)S(1)} %copy-done, bf16[512,1024]{1,0:T(8,128)(2,1)S(1)} %collective-permute-done.sib_ref, bf16[4096,384]{1,0:T(8,128)(2,1)S(1)} %copy-done.2, bf16[4096,128]{1,0:T(8,128)(2,1)S(1)} %copy-done.9, ...), custom_call_target="tpu_custom_call" | custom-call | flops 2952790016 | bytes 5767168 | tf_op jit(solution)/shard_map/project_near/pallas_call | solution.py:75
  34.8 3.0 %project_far.2 = (bf16[384,256]{1,0:T(8,128)(2,1)S(1)}, bf16[256,256]{1,0:T(8,128)(2,1)S(1)}, bf16[384,128]{1,0:T(8,128)(2,1)S(1)}, bf16[384,128]{1,0:T(8,128)(2...) custom-call(s32[3]{0:T(128)S(1)} %pad_add_fusion.scal_ref, f32[512,1408]{1,0:T(8,128)S(1)} %project_near.1.acc_ref, ...), custom_call_target="tpu_custom_call" | custom-call | flops 1476395008 | tf_op jit(solution)/shard_map/project_far/pallas_call | solution.py:166
  37.8 4.2 %collective-permute-start.9 = (bf16[384,128]{1,0:T(8,128)(2,1)S(1)}, bf16[384,128]{1,0:T(8,128)(2,1)S(1)}, u32[]{:S(2)}, u32[]{:S(2)}) collective-permute-start(bf16[384,128]{1,0:T(8,128)(2,1)S(1)} %get-tuple-element.48), channel_id=1, source_target_pairs={{0,24},{4,28},{8,16},{12,20},{16,8},{20,12},{24,0},{28,4},{1,25},{... | collective-permute-start | bytes 294920 | tf_op jit(solution)/shard_map/ppermute | solution.py:532
  42.0 0.6 collective-permute-start.7
  42.6 3.2 %project_far.3 = (bf16[384,256]{1,0:T(8,128)(2,1)S(1)}, bf16[256,256]{1,0:T(8,128)(2,1)S(1)}, bf16[384,128]{1,0:T(8,128)(2,1)S(1)}, bf16[384,128]{1,0:T(8,128)(2...) custom-call(s32[3]{0:T(128)S(1)} %pad_add_fusion.scal_ref, f32[512,1408]{1,0:T(8,128)S(1)} %project_near.1.acc_ref, ...), custom_call_target="tpu_custom_call" | custom-call | flops 1476395008 | tf_op jit(solution)/shard_map/project_far/pallas_call | solution.py:166
  45.8 3.8 %collective-permute-start.13 = (bf16[384,128]{1,0:T(8,128)(2,1)S(1)}, bf16[384,128]{1,0:T(8,128)(2,1)S(1)}, u32[]{:S(2)}, u32[]{:S(2)}) collective-permute-start(bf16[384,128]{1,0:T(8,128)(2,1)S(1)} %get-tuple-element.52), channel_id=1, source_target_pairs={{0,24},{4,28},{8,16},{12,20},{16,8},{20,12},{24,0},{28,4},{1,25},{... | collective-permute-start | bytes 294920 | tf_op jit(solution)/shard_map/ppermute | solution.py:532
  49.6 0.7 collective-permute-start.11
  50.3 5.2 %collective-permute-done.8.refs_6_ = bf16[384,128]{1,0:T(8,128)(2,1)S(1)} collective-permute-done((bf16[384,128]{1,0:T(8,128)(2,1)S(1)}, bf16[384,128]{1,0:T(8,128)(2,1)S(1)}, u32[]{:S(2)}, u32[]{:S(2)}) %collective-permute-start.8) | collective-permute-done | bytes 98336 | tf_op jit(solution)/shard_map/ppermute | solution.py:532
  55.6 1.6 %collective-permute-start.10 = (bf16[4,256,128]{2,1,0:T(8,128)(2,1)S(1)}, bf16[4,256,128]{2,1,0:T(8,128)(2,1)S(1)}, u32[]{:S(2)}, u32[]{:S(2)}) collective-permute-start(bf16[4,256,128]{2,1,0:T(8,128)(2,1)S(1)} %pad_maximum_fusion.1.refs_0_), channel_id=1, source_target_pairs={{0,4},{4,0},{8,12},{12,8},{16,20},{20,16},{24,28},{28,24},{1,5},{5... | collective-permute-start | bytes 786440 | tf_op jit(solution)/shard_map/ppermute | solution.py:534
  57.2 2.1 %collective-permute-done.12.refs_10_ = bf16[384,128]{1,0:T(8,128)(2,1)S(1)} collective-permute-done((bf16[384,128]{1,0:T(8,128)(2,1)S(1)}, bf16[384,128]{1,0:T(8,128)(2,1)S(1)}, u32[]{:S(2)}, u32[]{:S(2)}) %collective-permute-start.12) | collective-permute-done | bytes 98336 | tf_op jit(solution)/shard_map/ppermute | solution.py:532
  59.4 1.6 %collective-permute-start.14 = (bf16[4,256,128]{2,1,0:T(8,128)(2,1)S(1)}, bf16[4,256,128]{2,1,0:T(8,128)(2,1)S(1)}, u32[]{:S(2)}, u32[]{:S(2)}) collective-permute-start(bf16[4,256,128]{2,1,0:T(8,128)(2,1)S(1)} %pad_maximum_fusion.2.refs_2_), channel_id=1, source_target_pairs={{0,4},{4,0},{8,12},{12,8},{16,20},{20,16},{24,28},{28,24},{1,5},{5... | collective-permute-start | bytes 786440 | tf_op jit(solution)/shard_map/ppermute | solution.py:534
  61.0 0.9 fetch.3
  61.9 2.4 %collective-permute-start.5 = (bf16[128,256]{1,0:T(8,128)(2,1)S(1)}, bf16[128,256]{1,0:T(8,128)(2,1)S(1)}, u32[]{:S(2)}, u32[]{:S(2)}) collective-permute-start(bf16[128,256]{1,0:T(8,128)(2,1)S(1)} %slice.62), channel_id=1, source_target_pairs={{0,4},{4,8},{8,12},{12,16},{16,20},{20,24},{24,28},{1,5},{5,9},{9,... | collective-permute-start | bytes 196616 | tf_op jit(solution)/shard_map/ppermute | solution.py:539
  64.4 1.3 collective-permute-start.6
  65.7 2.9 %collective-permute-done.14.refs_3_ = bf16[4,256,128]{2,1,0:T(8,128)(2,1)S(1)} collective-permute-done((bf16[4,256,128]{2,1,0:T(8,128)(2,1)S(1)}, bf16[4,256,128]{2,1,0:T(8,128)(2,1)S(1)}, u32[]{:S(2)}, u32[]{:S(2)}) %collective-permute-start.14) | collective-permute-done | bytes 262176 | tf_op jit(solution)/shard_map/ppermute | solution.py:534
  68.6 41.9 %differential.1 = (bf16[2,64,256]{2,1,0:T(8,128)(2,1)S(1)}, bf16[2,64,256]{2,1,0:T(8,128)(2,1)S(1)}, bf16[2,64,256]{2,1,0:T(8,128)(2,1)S(1)}, bf16[2,64,256]{2,1,0:T(8,128)(2,1)S(1)}) custom-call(s32[3]{0:T(128)S(1)} %pad_add_fusion.scal_ref, f32[4]{0:T(128)S(1)} %copy-done.14, f32[1,64]{1,0:T(1,128)S(1)} %bitcast.19, ...), custom_call_target="tpu_custom_call" | custom-call | flops 8388608000 | tf_op jit(solution)/shard_map/differential/pallas_call | solution.py:401
  110.5 0.1 collective-permute-start.15
  110.6 3.2 %collective-permute-start.16 = (bf16[2,64,256]{2,1,0:T(8,128)(2,1)S(1)}, bf16[2,64,256]{2,1,0:T(8,128)(2,1)S(1)}, u32[]{:S(2)}, u32[]{:S(2)}) collective-permute-start(bf16[2,64,256]{2,1,0:T(8,128)(2,1)S(1)} %get-tuple-element.55), channel_id=1, source_target_pairs={{0,16},{4,20},{8,24},{12,28},{16,0},{20,4},{24,8},{28,12},{1,17},{... | collective-permute-start | bytes 196616 | tf_op jit(solution)/shard_map/ppermute | solution.py:547
  113.8 1.2 collective-permute-start.17
  115.0 7.1 %window.1.win_keep_ref.win_send_ref = bf16[512,384]{1,0:T(8,128)(2,1)S(1)} custom-call(s32[3]{0:T(128)S(1)} %pad_add_fusion.scal_ref, f32[6]{0:T(128)S(1)} %copy-done.16, bf16[384,256]{1,0:T(8,128)(2,1)S(1)} %get-tuple-element.41.refs_0_, bf16[384,256]{1,0:T(8,128)(2,1)S(1)} %get-tuple-element.42.refs_1_, bf16[256,256]{1,0:T(8,128)(2,1)S(1)} %get-tuple-element.43.refs_2_, ...), custom_call_target="tpu_custom_call" | custom-call | flops 3019898880 | tf_op jit(solution)/shard_map/window/pallas_call | solution.py:251
  122.1 2.6 %project_out.5 = (bf16[128,3072]{1,0:T(8,128)(2,1)S(1)}, bf16[128,3072]{1,0:T(8,128)(2,1)S(1)}) custom-call(s32[3]{0:T(128)S(1)} %pad_add_fusion.scal_ref, bf16[512,384]{1,0:T(8,128)(2,1)S(1)} %window.1.win_keep_ref.win_send_ref, bf16[512,384]{1,0:T(8,128)(2,1)S(1)} %window.1.win_keep_ref.win_send_ref, bf16[2,64,256]{2,1,0:T(8,128)(2,1)S(1)} %get-tuple-element.53.refs_0_, ...), custom_call_target="tpu_custom_call" | custom-call | flops 1006632960 | tf_op jit(solution)/shard_map/project_out/pallas_call | solution.py:475
  124.9 1.2 project_out.4
  126.1 0.5 collective-permute-start.19
  126.6 3.3 %project_out.3 = (bf16[128,4096]{1,0:T(8,128)(2,1)S(1)}, bf16[128,4096]{1,0:T(8,128)(2,1)S(1)}) custom-call(s32[3]{0:T(128)S(1)} %pad_add_fusion.scal_ref, bf16[512,384]{1,0:T(8,128)(2,1)S(1)} %window.1.win_keep_ref.win_send_ref, bf16[512,384]{1,0:T(8,128)(2,1)S(1)} %window.1.win_keep_ref.win_send_ref, bf16[2,64,256]{2,1,0:T(8,128)(2,1)S(1)} %get-tuple-element.53.refs_0_, ...), custom_call_target="tpu_custom_call" | custom-call | flops 1342177280 | tf_op jit(solution)/shard_map/project_out/pallas_call | solution.py:475
  129.9 0.1 collective-permute-start.18
  130.0 1.6 collective-permute-start.20
  131.6 0.2 add_convert_fusion
  131.9 0.6 collective-permute-start.22
  132.5 1.5 collective-permute-start.23
  134.0 5.3 %collective-permute-done.20 = bf16[128,1024]{1,0:T(8,128)(2,1)S(1)} collective-permute-done((bf16[128,1024]{1,0:T(8,128)(2,1)S(1)}, bf16[128,1024]{1,0:T(8,128)(2,1)S(1)}, u32[]{:S(2)}, u32[]{:S(2)}) %collective-permute-start.20) | collective-permute-done | bytes 262176 | tf_op jit(solution)/shard_map/ppermute | solution.py:572
  139.3 0.1 add_convert_fusion.3
  139.4 8.3 %collective-permute-done.22 = bf16[128,1536]{1,0:T(8,128)(2,1)S(1)} collective-permute-done((bf16[128,1536]{1,0:T(8,128)(2,1)S(1)}, bf16[128,1536]{1,0:T(8,128)(2,1)S(1)}, u32[]{:S(2)}, u32[]{:S(2)}) %collective-permute-start.22) | collective-permute-done | bytes 393248 | tf_op jit(solution)/shard_map/ppermute | solution.py:572
  147.7 7.9 %collective-permute-done.23 = bf16[128,1536]{1,0:T(8,128)(2,1)S(1)} collective-permute-done((bf16[128,1536]{1,0:T(8,128)(2,1)S(1)}, bf16[128,1536]{1,0:T(8,128)(2,1)S(1)}, u32[]{:S(2)}, u32[]{:S(2)}) %collective-permute-start.23) | collective-permute-done | bytes 393248 | tf_op jit(solution)/shard_map/ppermute | solution.py:572
  155.7 0.3 add_convert_fusion.2
  156.0 1.1 pad_maximum_fusion
  (64 shorter events, 0.5 us)
Async XLA Ops:
  0.0 18.5 %copy-start.3 = (bf16[4096,256]{1,0:T(8,128)(2,1)S(1)}, bf16[4096,256]{1,0:T(8,128)(2,1)}, u32[]{:S(2)}) copy-start(bf16[4096,256]{1,0:T(8,128)(2,1)} %refs_3_.3) | copy-start | bytes 6291460
  0.0 29.4 %collective-permute-start = (bf16[512,1024]{1,0:T(8,128)(2,1)}, bf16[512,1024]{1,0:T(8,128)(2,1)S(1)}, u32[]{:S(2)}, u32[]{:S(2)}) collective-permute-start(bf16[512,1024]{1,0:T(8,128)(2,1)} %own_ref.1), channel_id=1, source_target_pairs={{0,1},{1,0},{2,3},{3,2},{4,5},{5,4},{6,7},{7,6},{8,9},{9,8},{10,11... | collective-permute-start | bytes 3145736 | tf_op jit(solution)/shard_map/ppermute | solution.py:520
  2.9 15.6 %collective-permute-start.1 = (bf16[256,1024]{1,0:T(8,128)(2,1)}, bf16[256,1024]{1,0:T(8,128)(2,1)}, u32[]{:S(2)}, u32[]{:S(2)}) collective-permute-start(bf16[256,1024]{1,0:T(8,128)(2,1)} %get-tuple-element.68), channel_id=1, source_target_pairs={{0,2},{1,3},{2,0},{3,1},{4,6},{5,7},{6,4},{7,5},{8,10},{9,11},{10,... | collective-permute-start | bytes 1572872 | tf_op jit(solution)/shard_map/ppermute | solution.py:517
  5.4 24.0 %collective-permute-start.3 = (bf16[256,1024]{1,0:T(8,128)(2,1)}, bf16[256,1024]{1,0:T(8,128)(2,1)}, u32[]{:S(2)}, u32[]{:S(2)}) collective-permute-start(bf16[256,1024]{1,0:T(8,128)(2,1)} %get-tuple-element.67), channel_id=1, source_target_pairs={{0,2},{1,3},{2,0},{3,1},{4,6},{5,7},{6,4},{7,5},{8,10},{9,11},{10,... | collective-permute-start | bytes 1572872 | tf_op jit(solution)/shard_map/ppermute | solution.py:517
  6.1 23.3 %copy-start = (bf16[512,1024]{1,0:T(8,128)(2,1)S(1)}, bf16[512,1024]{1,0:T(8,128)(2,1)}, u32[]{:S(2)}) copy-start(bf16[512,1024]{1,0:T(8,128)(2,1)} %own_ref.1) | copy-start | bytes 3145732
  18.4 16.3 %collective-permute-start.2 = (bf16[256,1024]{1,0:T(8,128)(2,1)}, bf16[256,1024]{1,0:T(8,128)(2,1)S(1)}, u32[]{:S(2)}, u32[]{:S(2)}) collective-permute-start(bf16[256,1024]{1,0:T(8,128)(2,1)} %collective-permute-done.1.refs_0_), channel_id=1, source_target_pairs={{0,1},{1,0},{2,3},{3,2},{4,5},{5,4},{6,7},{7,6},{8,9},{9,8},{10,11... | collective-permute-start | bytes 1572872 | tf_op jit(solution)/shard_map/ppermute | solution.py:526
  18.5 1.9 %copy-start.1 = (bf16[4096,384]{1,0:T(8,128)(2,1)S(1)}, bf16[4096,384]{1,0:T(8,128)(2,1)}, u32[]{:S(2)}) copy-start(bf16[4096,384]{1,0:T(8,128)(2,1)} %refs_0_.4) | copy-start | bytes 9437188
  20.3 1.6 %copy-start.4 = (bf16[4096,256]{1,0:T(8,128)(2,1)S(1)}, bf16[4096,256]{1,0:T(8,128)(2,1)}, u32[]{:S(2)}) copy-start(bf16[4096,256]{1,0:T(8,128)(2,1)} %refs_4_.3) | copy-start | bytes 6291460
  21.9 1.6 %copy-start.6 = (bf16[4096,256]{1,0:T(8,128)(2,1)S(1)}, bf16[4096,256]{1,0:T(8,128)(2,1)}, u32[]{:S(2)}) copy-start(bf16[4096,256]{1,0:T(8,128)(2,1)} %refs_5_.3) | copy-start | bytes 6291460
  23.5 1.2 copy-start.8
  24.8 1.2 copy-start.10
  26.0 3.4 %copy-start.2 = (bf16[4096,384]{1,0:T(8,128)(2,1)S(1)}, bf16[4096,384]{1,0:T(8,128)(2,1)}, u32[]{:S(2)}) copy-start(bf16[4096,384]{1,0:T(8,128)(2,1)} %refs_0_.4) | copy-start | bytes 9437188
  26.0 3.4 %copy-start.5 = (bf16[4096,256]{1,0:T(8,128)(2,1)S(1)}, bf16[4096,256]{1,0:T(8,128)(2,1)}, u32[]{:S(2)}) copy-start(bf16[4096,256]{1,0:T(8,128)(2,1)} %refs_4_.3) | copy-start | bytes 6291460
  26.0 3.4 %copy-start.7 = (bf16[4096,256]{1,0:T(8,128)(2,1)S(1)}, bf16[4096,256]{1,0:T(8,128)(2,1)}, u32[]{:S(2)}) copy-start(bf16[4096,256]{1,0:T(8,128)(2,1)} %refs_5_.3) | copy-start | bytes 6291460
  26.0 3.4 %copy-start.9 = (bf16[4096,128]{1,0:T(8,128)(2,1)S(1)}, bf16[4096,128]{1,0:T(8,128)(2,1)}, u32[]{:S(2)}) copy-start(bf16[4096,128]{1,0:T(8,128)(2,1)} %refs_1_.4) | copy-start | bytes 3145732
  26.0 3.7 %copy-start.11 = (bf16[4096,128]{1,0:T(8,128)(2,1)S(1)}, bf16[4096,128]{1,0:T(8,128)(2,1)}, u32[]{:S(2)}) copy-start(bf16[4096,128]{1,0:T(8,128)(2,1)} %refs_2_.3) | copy-start | bytes 3145732
  29.4 13.3 %collective-permute-start.4 = (bf16[256,1024]{1,0:T(8,128)(2,1)}, bf16[256,1024]{1,0:T(8,128)(2,1)S(1)}, u32[]{:S(2)}, u32[]{:S(2)}) collective-permute-start(bf16[256,1024]{1,0:T(8,128)(2,1)} %collective-permute-done.3.refs_0_), channel_id=1, source_target_pairs={{0,1},{1,0},{2,3},{3,2},{4,5},{5,4},{6,7},{7,6},{8,9},{9,8},{10,11... | collective-permute-start | bytes 1572872 | tf_op jit(solution)/shard_map/ppermute | solution.py:526
  37.8 11.8 %collective-permute-start.9 = (bf16[384,128]{1,0:T(8,128)(2,1)S(1)}, bf16[384,128]{1,0:T(8,128)(2,1)S(1)}, u32[]{:S(2)}, u32[]{:S(2)}) collective-permute-start(bf16[384,128]{1,0:T(8,128)(2,1)S(1)} %get-tuple-element.48), channel_id=1, source_target_pairs={{0,24},{4,28},{8,16},{12,20},{16,8},{20,12},{24,0},{28,4},{1,25},{... | collective-permute-start | bytes 294920 | tf_op jit(solution)/shard_map/ppermute | solution.py:532
  42.0 13.6 %collective-permute-start.8 = (bf16[384,128]{1,0:T(8,128)(2,1)S(1)}, bf16[384,128]{1,0:T(8,128)(2,1)S(1)}, u32[]{:S(2)}, u32[]{:S(2)}) collective-permute-start(bf16[384,128]{1,0:T(8,128)(2,1)S(1)} %get-tuple-element.47), channel_id=1, source_target_pairs={{0,16},{4,20},{8,24},{12,28},{16,0},{20,4},{24,8},{28,12},{1,17},{... | collective-permute-start | bytes 294920 | tf_op jit(solution)/shard_map/ppermute | solution.py:532
  42.0 13.6 %collective-permute-start.7 = (bf16[384,128]{1,0:T(8,128)(2,1)S(1)}, bf16[384,128]{1,0:T(8,128)(2,1)S(1)}, u32[]{:S(2)}, u32[]{:S(2)}) collective-permute-start(bf16[384,128]{1,0:T(8,128)(2,1)S(1)} %get-tuple-element.46), channel_id=1, source_target_pairs={{0,8},{4,12},{8,0},{12,4},{16,24},{20,28},{24,16},{28,20},{1,9},{5... | collective-permute-start | bytes 294920 | tf_op jit(solution)/shard_map/ppermute | solution.py:532
  42.6 18.4 %copy-start.12 = (bf16[384,4096]{1,0:T(8,128)(2,1)S(1)}, bf16[384,4096]{1,0:T(8,128)(2,1)}, u32[]{:S(2)}) copy-start(bf16[384,4096]{1,0:T(8,128)(2,1)} %refs_0_.5) | copy-start | bytes 9437188
  42.6 18.4 %copy-start.13 = (bf16[256,4096]{1,0:T(8,128)(2,1)S(1)}, bf16[256,4096]{1,0:T(8,128)(2,1)}, u32[]{:S(2)}) copy-start(bf16[256,4096]{1,0:T(8,128)(2,1)} %refs_1_.5) | copy-start | bytes 6291460
  45.8 11.4 %collective-permute-start.13 = (bf16[384,128]{1,0:T(8,128)(2,1)S(1)}, bf16[384,128]{1,0:T(8,128)(2,1)S(1)}, u32[]{:S(2)}, u32[]{:S(2)}) collective-permute-start(bf16[384,128]{1,0:T(8,128)(2,1)S(1)} %get-tuple-element.52), channel_id=1, source_target_pairs={{0,24},{4,28},{8,16},{12,20},{16,8},{20,12},{24,0},{28,4},{1,25},{... | collective-permute-start | bytes 294920 | tf_op jit(solution)/shard_map/ppermute | solution.py:532
  49.6 9.7 %collective-permute-start.12 = (bf16[384,128]{1,0:T(8,128)(2,1)S(1)}, bf16[384,128]{1,0:T(8,128)(2,1)S(1)}, u32[]{:S(2)}, u32[]{:S(2)}) collective-permute-start(bf16[384,128]{1,0:T(8,128)(2,1)S(1)} %get-tuple-element.51), channel_id=1, source_target_pairs={{0,16},{4,20},{8,24},{12,28},{16,0},{20,4},{24,8},{28,12},{1,17},{... | collective-permute-start | bytes 294920 | tf_op jit(solution)/shard_map/ppermute | solution.py:532
  49.6 9.7 %collective-permute-start.11 = (bf16[384,128]{1,0:T(8,128)(2,1)S(1)}, bf16[384,128]{1,0:T(8,128)(2,1)S(1)}, u32[]{:S(2)}, u32[]{:S(2)}) collective-permute-start(bf16[384,128]{1,0:T(8,128)(2,1)S(1)} %get-tuple-element.50), channel_id=1, source_target_pairs={{0,8},{4,12},{8,0},{12,4},{16,24},{20,28},{24,16},{28,20},{1,9},{5... | collective-permute-start | bytes 294920 | tf_op jit(solution)/shard_map/ppermute | solution.py:532
  55.6 10.0 %collective-permute-start.10 = (bf16[4,256,128]{2,1,0:T(8,128)(2,1)S(1)}, bf16[4,256,128]{2,1,0:T(8,128)(2,1)S(1)}, u32[]{:S(2)}, u32[]{:S(2)}) collective-permute-start(bf16[4,256,128]{2,1,0:T(8,128)(2,1)S(1)} %pad_maximum_fusion.1.refs_0_), channel_id=1, source_target_pairs={{0,4},{4,0},{8,12},{12,8},{16,20},{20,16},{24,28},{28,24},{1,5},{5... | collective-permute-start | bytes 786440 | tf_op jit(solution)/shard_map/ppermute | solution.py:534
  59.4 9.2 %copy-start.14 = (f32[4]{0:T(128)S(1)}, f32[4]{0:T(128)}, u32[]{:S(2)}) copy-start(f32[4]{0:T(128)} %lam_ref.1) | copy-start | bytes 52
  59.4 9.2 %copy-start.15 = (f32[64]{0:T(128)S(1)}, f32[64]{0:T(128)}, u32[]{:S(2)}) copy-start(f32[64]{0:T(128)} %param.23) | copy-start | bytes 772
  59.4 9.2 %collective-permute-start.14 = (bf16[4,256,128]{2,1,0:T(8,128)(2,1)S(1)}, bf16[4,256,128]{2,1,0:T(8,128)(2,1)S(1)}, u32[]{:S(2)}, u32[]{:S(2)}) collective-permute-start(bf16[4,256,128]{2,1,0:T(8,128)(2,1)S(1)} %pad_maximum_fusion.2.refs_2_), channel_id=1, source_target_pairs={{0,4},{4,0},{8,12},{12,8},{16,20},{20,16},{24,28},{28,24},{1,5},{5... | collective-permute-start | bytes 786440 | tf_op jit(solution)/shard_map/ppermute | solution.py:534
  61.9 53.0 %collective-permute-start.5 = (bf16[128,256]{1,0:T(8,128)(2,1)S(1)}, bf16[128,256]{1,0:T(8,128)(2,1)S(1)}, u32[]{:S(2)}, u32[]{:S(2)}) collective-permute-start(bf16[128,256]{1,0:T(8,128)(2,1)S(1)} %slice.62), channel_id=1, source_target_pairs={{0,4},{4,8},{8,12},{12,16},{16,20},{20,24},{24,28},{1,5},{5,9},{9,... | collective-permute-start | bytes 196616 | tf_op jit(solution)/shard_map/ppermute | solution.py:539
  64.4 50.6 %collective-permute-start.6 = (bf16[128,256]{1,0:T(8,128)(2,1)S(1)}, bf16[128,256]{1,0:T(8,128)(2,1)S(1)}, u32[]{:S(2)}, u32[]{:S(2)}) collective-permute-start(bf16[128,256]{1,0:T(8,128)(2,1)S(1)} %slice.63), channel_id=1, source_target_pairs={{4,0},{8,4},{12,8},{16,12},{20,16},{24,20},{28,24},{5,1},{9,5},{13... | collective-permute-start | bytes 196616 | tf_op jit(solution)/shard_map/ppermute | solution.py:540
  68.6 46.4 %copy-start.16 = (f32[6]{0:T(128)S(1)}, f32[6]{0:T(128)}, u32[]{:S(2)}) copy-start(f32[6]{0:T(128)} %sink_ref.1) | copy-start | bytes 76
  110.5 11.6 %collective-permute-start.15 = (bf16[2,64,256]{2,1,0:T(8,128)(2,1)S(1)}, bf16[2,64,256]{2,1,0:T(8,128)(2,1)S(1)}, u32[]{:S(2)}, u32[]{:S(2)}) collective-permute-start(bf16[2,64,256]{2,1,0:T(8,128)(2,1)S(1)} %get-tuple-element.54), channel_id=1, source_target_pairs={{0,8},{4,12},{8,0},{12,4},{16,24},{20,28},{24,16},{28,20},{1,9},{5... | collective-permute-start | bytes 196616 | tf_op jit(solution)/shard_map/ppermute | solution.py:547
  110.6 11.5 %collective-permute-start.16 = (bf16[2,64,256]{2,1,0:T(8,128)(2,1)S(1)}, bf16[2,64,256]{2,1,0:T(8,128)(2,1)S(1)}, u32[]{:S(2)}, u32[]{:S(2)}) collective-permute-start(bf16[2,64,256]{2,1,0:T(8,128)(2,1)S(1)} %get-tuple-element.55), channel_id=1, source_target_pairs={{0,16},{4,20},{8,24},{12,28},{16,0},{20,4},{24,8},{28,12},{1,17},{... | collective-permute-start | bytes 196616 | tf_op jit(solution)/shard_map/ppermute | solution.py:547
  113.8 8.3 %collective-permute-start.17 = (bf16[2,64,256]{2,1,0:T(8,128)(2,1)S(1)}, bf16[2,64,256]{2,1,0:T(8,128)(2,1)S(1)}, u32[]{:S(2)}, u32[]{:S(2)}) collective-permute-start(bf16[2,64,256]{2,1,0:T(8,128)(2,1)S(1)} %get-tuple-element.56), channel_id=1, source_target_pairs={{0,24},{4,28},{8,16},{12,20},{16,8},{20,12},{24,0},{28,4},{1,25},{... | collective-permute-start | bytes 196616 | tf_op jit(solution)/shard_map/ppermute | solution.py:547
  124.8 6.8 %collective-permute-start.21 = (bf16[128,3072]{1,0:T(8,128)(2,1)S(1)}, bf16[128,3072]{1,0:T(8,128)(2,1)S(1)}, u32[]{:S(2)}, u32[]{:S(2)}) collective-permute-start(bf16[128,3072]{1,0:T(8,128)(2,1)S(1)} %get-tuple-element.64), channel_id=1, source_target_pairs={{0,1},{1,0},{2,3},{3,2},{4,5},{5,4},{6,7},{7,6},{8,9},{9,8},{10,11... | collective-permute-start | bytes 2359304 | tf_op jit(solution)/shard_map/ppermute | solution.py:568
  126.1 3.9 %collective-permute-start.19 = (bf16[128,1024]{1,0:T(8,128)(2,1)S(1)}, bf16[128,1024]{1,0:T(8,128)(2,1)S(1)}, u32[]{:S(2)}, u32[]{:S(2)}) collective-permute-start(bf16[128,1024]{1,0:T(8,128)(2,1)S(1)} %get-tuple-element.62), channel_id=1, source_target_pairs={{0,1},{1,0},{2,3},{3,2},{4,5},{5,4},{6,7},{7,6},{8,9},{9,8},{10,11... | collective-permute-start | bytes 786440 | tf_op jit(solution)/shard_map/ppermute | solution.py:568
  129.9 9.4 %collective-permute-start.18 = (bf16[128,4096]{1,0:T(8,128)(2,1)S(1)}, bf16[128,4096]{1,0:T(8,128)(2,1)S(1)}, u32[]{:S(2)}, u32[]{:S(2)}) collective-permute-start(bf16[128,4096]{1,0:T(8,128)(2,1)S(1)} %get-tuple-element.60), channel_id=1, source_target_pairs={{0,1},{1,0},{2,3},{3,2},{4,5},{5,4},{6,7},{7,6},{8,9},{9,8},{10,11... | collective-permute-start | bytes 3145736 | tf_op jit(solution)/shard_map/ppermute | solution.py:575
  130.0 9.2 %collective-permute-start.20 = (bf16[128,1024]{1,0:T(8,128)(2,1)S(1)}, bf16[128,1024]{1,0:T(8,128)(2,1)S(1)}, u32[]{:S(2)}, u32[]{:S(2)}) collective-permute-start(bf16[128,1024]{1,0:T(8,128)(2,1)S(1)} %add_convert_fusion.4), channel_id=1, source_target_pairs={{0,2},{1,3},{2,0},{3,1},{4,6},{5,7},{6,4},{7,5},{8,10},{9,11},{10,... | collective-permute-start | bytes 786440 | tf_op jit(solution)/shard_map/ppermute | solution.py:572
  131.9 15.9 %collective-permute-start.22 = (bf16[128,1536]{1,0:T(8,128)(2,1)S(1)}, bf16[128,1536]{1,0:T(8,128)(2,1)S(1)}, u32[]{:S(2)}, u32[]{:S(2)}) collective-permute-start(bf16[128,1536]{1,0:T(8,128)(2,1)S(1)} %get-tuple-element.69), channel_id=1, source_target_pairs={{0,2},{1,3},{2,0},{3,1},{4,6},{5,7},{6,4},{7,5},{8,10},{9,11},{10,... | collective-permute-start | bytes 1179656 | tf_op jit(solution)/shard_map/ppermute | solution.py:572
  132.5 23.2 %collective-permute-start.23 = (bf16[128,1536]{1,0:T(8,128)(2,1)S(1)}, bf16[128,1536]{1,0:T(8,128)(2,1)S(1)}, u32[]{:S(2)}, u32[]{:S(2)}) collective-permute-start(bf16[128,1536]{1,0:T(8,128)(2,1)S(1)} %get-tuple-element.70), channel_id=1, source_target_pairs={{0,2},{1,3},{2,0},{3,1},{4,6},{5,7},{6,4},{7,5},{8,10},{9,11},{10,... | collective-permute-start | bytes 1179656 | tf_op jit(solution)/shard_map/ppermute | solution.py:572
where the time goes:
time: 157 us
  Pallas kernels  69.4 us (44%)
  waiting for transfers between devices  46.5 us (30%)
  starting transfers between devices  28 us (18%)
  local copies, waits for them, and re-layouts  10.3 us (7%)
  other arithmetic  1.89 us (1%)
    pallas_call x1, Pallas kernels, diff_part(): pl.pallas_call(functools.partial(diff_kernel, chunks, rows, parts, count)...  41.9 us
    ppermute x3, waiting for transfers between devices, body(): crossed[i].append(lax.ppermute(piece, 'tp', flip('tp', 2 * o)))  21.6 us
    ppermute x2, waiting for transfers between devices, body(): lax.ppermute(pieces[c], 'tp', flip('tp', 2 * o))  14.6 us
    ppermute x6, starting transfers between devices, body(): moved.append(lax.ppermute(slots[d], 'sp', flip('sp', d * parts)))  9.34 us
    unnamed x34, local copies, waits for them, and re-layouts  7.82 us
    ppermute x6, waiting for transfers between devices, body(): moved.append(lax.ppermute(slots[d], 'sp', flip('sp', d * parts)))  7.34 us
    pallas_call x1, Pallas kernels, window_part(): pl.pallas_call(functools.partial(window_kernel, chunks, rows, kv_local),...  7.12 us
    pallas_call x3, Pallas kernels, out_part(): pl.pallas_call(functools.partial(out_kernel, heads, parts, begin), grid_s...  7.1 us
  transfers between devices with their start and end apart: 24, of which 8 were waited for; matrix products, arithmetic and copies ran while one was open for 2% of the time, Pallas kernels for 42%

commit v1 on v0

--- a/solution.py
+++ b/solution.py
@@ -19,8 +19,8 @@
 SAFE_BOUND = 90.0
 
 
-def whole(shape):
-    return pl.BlockSpec(shape, lambda *_: (0,) * len(shape))
+def vmem():
+    return pl.BlockSpec(memory_space=pltpu.VMEM)
 
 
 def smem():
@@ -37,112 +37,88 @@
     return [(i, i ^ bits) for i in range(lax.axis_size(axis))]
 
 
-def add_slice(x, weight_refs, acc_ref):
-    weight = jnp.concatenate([ref[...] for ref in weight_refs], axis=1)
-    acc_ref[...] += jnp.dot(x, weight, preferred_element_type=jnp.float32)
-
-
-def first_kernel(steps, scal_ref, own_ref, sib_ref, *refs):
-    acc_ref = refs[-1]
-    j = pl.program_id(0)
-
-    @pl.when(j == 0)
-    def _():
-        acc_ref[...] = jnp.zeros_like(acc_ref)
-
-    x = jnp.where(j < steps, own_ref[...], sib_ref[...])
-    add_slice(x, refs[:-1], acc_ref)
-
-
-def project_near(own, sib, weights, scal, steps):
+def near_kernel(scal_ref, own_ref, sib_ref, *refs):
+    weight_refs, acc_ref = refs[:-1], refs[-1]
+    depth = own_ref.shape[1]
+    me = scal_ref[2]
+    low = 0
+    for group in ((0, 1), (2, 3), (4,), (5,)):
+        total = None
+        for x_ref, k in ((own_ref, 0), (sib_ref, 1)):
+            at = pl.multiple_of((me ^ k) * depth, depth)
+            weight = jnp.concatenate([weight_refs[i][pl.ds(at, depth), :] for i in group], axis=1)
+            added = jnp.dot(x_ref[...], weight, preferred_element_type=jnp.float32)
+            total = added if total is None else total + added
+        acc_ref[:, low : low + total.shape[1]] = total
+        low += total.shape[1]
+
+
+def project_near(own, sib, weights, scal):
     rows, depth = own.shape
-    block = depth // steps
     width = sum(w.shape[1] for w in weights)
-
-    def at_weight(j, scal):
-        return ((scal[2] ^ (j // steps)) * steps + j % steps, 0)
-
-    grid_spec = pltpu.PrefetchScalarGridSpec(
-        num_scalar_prefetch=1,
-        grid=(2 * steps,),
-        in_specs=[
-            pl.BlockSpec((rows, block), lambda j, idx: (0, jnp.minimum(j, steps - 1))),
-            pl.BlockSpec((rows, block), lambda j, idx: (0, jnp.maximum(j - steps, 0))),
-        ]
-        + [pl.BlockSpec((block, w.shape[1]), at_weight) for w in weights],
-        out_specs=pl.BlockSpec((rows, width), lambda j, idx: (0, 0)),
-    )
     return pl.pallas_call(
-        functools.partial(first_kernel, steps),
-        grid_spec=grid_spec,
+        near_kernel,
+        in_specs=[smem()] + [vmem()] * 8,
+        out_specs=vmem(),
         out_shape=jax.ShapeDtypeStruct((rows, width), jnp.float32),
-        compiler_params=pltpu.CompilerParams(
-            dimension_semantics=("arbitrary",), vmem_limit_bytes=24 << 20
-        ),
-        cost_estimate=cost(4 * rows * depth * width, 4 * depth * width),
+        compiler_params=pltpu.CompilerParams(vmem_limit_bytes=24 << 20),
+        cost_estimate=cost(4 * rows * depth * width),
         name="project_near",
     )(scal, own, sib, *weights)
 
 
-def fetch_kernel(pieces, scal_ref, *refs):
-    count = len(pieces)
+def copy_kernel(begin, *refs):
+    count = len(refs) // 2
     sources, targets, semaphores = refs[:count], refs[count : 2 * count], refs[2 * count]
-    copies = []
-    for source, target, slices in zip(sources, targets, pieces):
-        depth = target.shape[0] // len(slices)
-        for i, k in enumerate(slices):
-            at = 0 if k is None else pl.multiple_of((scal_ref[2] ^ k) * depth, depth)
-            copies.append(
-                pltpu.make_async_copy(
-                    source.at[pl.ds(at, depth), :],
-                    target.at[pl.ds(i * depth, depth), :],
-                    semaphores.at[len(copies)],
-                )
-            )
+    copies = [
+        pltpu.make_async_copy(
+            source.at[pl.ds(begin, target.shape[0]), :], target, semaphores.at[i]
+        )
+        for i, (source, target) in enumerate(zip(sources, targets))
+    ]
     for copy in copies:
         copy.start()
     for copy in copies:
         copy.wait()
 
 
-def fetch(scal, arrays, slices, tp):
-    shapes = [
-        (a.shape[0] if slices == [None] else a.shape[0] // tp * len(slices), a.shape[1])
-        for a in arrays
-    ]
+def fetch(arrays, begin=0, rows=None, room=1 << 20):
+    shapes = [(a.shape[0] if rows is None else rows, a.shape[1]) for a in arrays]
     return pl.pallas_call(
-        functools.partial(fetch_kernel, [slices] * len(arrays)),
-        in_specs=[smem()] + [pl.BlockSpec(memory_space=pl.ANY)] * len(arrays),
+        functools.partial(copy_kernel, begin),
+        in_specs=[pl.BlockSpec(memory_space=pltpu.HBM)] * len(arrays),
         out_specs=[pl.BlockSpec(memory_space=pltpu.VMEM)] * len(arrays),
         out_shape=[pltpu.VMEM(shape, jnp.bfloat16) for shape in shapes],
-        scratch_shapes=[pltpu.SemaphoreType.DMA((len(arrays) * len(slices),))],
-        compiler_params=pltpu.CompilerParams(vmem_limit_bytes=1 << 20),
-        cost_estimate=cost(3 << 30),
+        scratch_shapes=[pltpu.SemaphoreType.DMA((len(arrays),))],
+        compiler_params=pltpu.CompilerParams(vmem_limit_bytes=room),
+        cost_estimate=cost(1 << 30),
         name="fetch",
-    )(scal, *arrays)
-
-
-def far_kernel(count, heads, parts, scal_ref, acc_ref, *refs):
+    )(*arrays)
+
+
+def far_kernel(begin, count, heads, parts, scal_ref, acc_ref, *refs):
     xs = refs[:count]
     weight_refs = refs[count : count + 6]
     qt_ref, kv_ref = refs[count + 6 : count + 8]
     slot_refs = refs[count + 8 : count + 8 + heads]
     buf_ref = refs[count + 8 + heads]
-    rows, _ = xs[0].shape
+    rows, depth = xs[0].shape
     here = scal_ref[0] // parts
 
     def project(which):
-        whole_x = jnp.concatenate([x[...] for x in xs], axis=1)
-        weight = jnp.concatenate([weight_refs[i][...] for i in which], axis=1)
         low = sum(weight_refs[i].shape[1] for i in range(which[0]))
-        span = weight.shape[1]
-        total = acc_ref[:, low : low + span] + jnp.dot(
-            whole_x, weight, preferred_element_type=jnp.float32
-        )
+        span = sum(weight_refs[i].shape[1] for i in which)
+        total = acc_ref[begin : begin + rows, low : low + span]
+        for n, x in enumerate(xs):
+            at = pl.multiple_of((scal_ref[2] ^ (2 + n)) * depth, depth)
+            weight = jnp.concatenate([weight_refs[i][pl.ds(at, depth), :] for i in which], axis=1)
+            total += jnp.dot(x[...], weight, preferred_element_type=jnp.float32)
         ends = [sum(weight_refs[i].shape[1] for i in which[:n]) for n in range(len(which) + 1)]
         return [total[:, a:b] for a, b in zip(ends[:-1], ends[1:])]
 
-    win_q, win_k, win_v, diff_q, diff_k, diff_v = project(range(6))
+    diff_k, diff_v = project((4, 5))
+    win_v, diff_q = project((2, 3))
+    win_q, win_k = project((0, 1))
     diff_q = diff_q * (LOG2E * DQK ** (-0.5))
     for h in range(heads):
         lanes = slice(h * HEAD, (h + 1) * HEAD)
@@ -164,31 +140,26 @@
     q_width = weights[0].shape[1]
     shapes = [(q_width, rows), (rows, kv_width)] + [(rows + rows // 2, 2 * HEAD)] * heads
     return pl.pallas_call(
-        functools.partial(far_kernel, count, heads, parts),
-        in_specs=[smem(), pl.BlockSpec((rows, width), lambda j: (chunk, 0))]
-        + [whole((rows, depth))] * count
-        + [pl.BlockSpec(memory_space=pltpu.VMEM)] * 6,
-        out_specs=[whole(shape) for shape in shapes],
+        functools.partial(far_kernel, chunk * rows, count, heads, parts),
+        in_specs=[smem()] + [vmem()] * (1 + count + 6),
+        out_specs=[vmem() for shape in shapes],
         out_shape=[jax.ShapeDtypeStruct(shape, jnp.bfloat16) for shape in shapes],
         scratch_shapes=[pltpu.VMEM((heads, rows + rows // 2, 2 * HEAD), jnp.bfloat16)],
-        grid=(1,),
         compiler_params=pltpu.CompilerParams(vmem_limit_bytes=24 << 20),
         cost_estimate=cost(2 * count * rows * depth * width),
         name="project_far",
     )(scal, acc, *xs, *weights)
 
 
-def window_kernel(chunks, rows, kv_local, scal_ref, sink_ref, *refs):
-    q_refs = refs[:chunks]
-    kv_refs = refs[chunks : 2 * chunks]
-    low_ref, high_ref, rows_ref, keys, values_t, out_ref = refs[2 * chunks :]
+def window_kernel(begin, whole_rows, kv_local, scal_ref, sink_ref, *refs):
+    q_ref, low_ref, kv_ref, high_ref, rows_ref, keys, values_t, out_ref = refs
+    last = low_ref.shape[0] - WINDOW
     here, live = scal_ref[0], scal_ref[1]
+    rows = kv_ref.shape[0]
     span = rows + 2 * WINDOW
-    size = rows // chunks
-    keys[0:WINDOW, :] = low_ref[...]
-    for c in range(chunks):
-        keys[WINDOW + c * size : WINDOW + (c + 1) * size, :] = kv_refs[c][...]
-    keys[WINDOW + rows : span, :] = high_ref[...]
+    keys[0:WINDOW, :] = low_ref[last:, :]
+    keys[WINDOW : WINDOW + rows, :] = kv_ref[...]
+    keys[WINDOW + rows : span, :] = high_ref[0:WINDOW, :]
     k_width = kv_local * HEAD
     turned = jnp.transpose(keys[:, k_width:].astype(jnp.float32)).astype(jnp.bfloat16)
     tail = (lax.broadcasted_iota(jnp.int32, (16, span), 0) == 0).astype(jnp.bfloat16)
@@ -197,7 +168,7 @@
         values_t[h, HEAD : HEAD + 16, :] = tail
     step = 128
     for b in range(rows // step):
-        first = here * rows + b * step
+        first = here * whole_rows + begin + b * step
 
         @pl.when(first >= live)
         def _():
@@ -208,7 +179,7 @@
         @pl.when(first < live)
         def _():
             wide = step + 2 * WINDOW
-            c, at = (b * step) // size, (b * step) % size
+            at = b * step
             key_at = lax.broadcasted_iota(jnp.int32, (wide, step), 0)
             query_at = lax.broadcasted_iota(jnp.int32, (wide, step), 1)
             key_pos = first - WINDOW + key_at
@@ -224,7 +195,7 @@
                 value_block = values_t[h, :, b * step : b * step + wide]
                 for g in range(GROUP):
                     head = h * GROUP + g
-                    q = q_refs[c][head * HEAD : (head + 1) * HEAD, at : at + step]
+                    q = q_ref[head * HEAD : (head + 1) * HEAD, at : at + step]
                     s = jnp.dot(key_block, q, preferred_element_type=jnp.float32)
                     s = jnp.where(allowed, s, masked_score)
                     sink = sink_ref[head] * LOG2E
@@ -241,28 +212,24 @@
         rows_ref[b * step : (b + 1) * step, :] = jnp.transpose(block).astype(jnp.bfloat16)
 
 
-def window_part(scal, sink_logit, q_parts, kv_parts, low, high):
-    chunks = len(q_parts)
-    q_width, size = q_parts[0].shape
-    kv_width = kv_parts[0].shape[1]
-    rows = size * chunks
+def window_part(scal, sink_logit, q_t, low, kv, high, begin, whole_rows):
+    q_width, rows = q_t.shape
+    kv_width = kv.shape[1]
     kv_local = kv_width // (2 * HEAD)
-    operands = (*q_parts, *kv_parts, low, high)
     return pl.pallas_call(
-        functools.partial(window_kernel, chunks, rows, kv_local),
-        in_specs=[smem(), smem()] + [whole(a.shape) for a in operands],
-        out_specs=whole((rows, q_width)),
+        functools.partial(window_kernel, begin, whole_rows, kv_local),
+        in_specs=[smem()] * 2 + [vmem()] * 4,
+        out_specs=vmem(),
         out_shape=jax.ShapeDtypeStruct((rows, q_width), jnp.bfloat16),
         scratch_shapes=[
             pltpu.VMEM((rows + 2 * WINDOW, kv_width), jnp.bfloat16),
             pltpu.VMEM((kv_local, HEAD + 16, rows + 2 * WINDOW), jnp.bfloat16),
             pltpu.VMEM((q_width, rows), jnp.float32),
         ],
-        grid=(1,),
         compiler_params=pltpu.CompilerParams(vmem_limit_bytes=16 << 20),
         cost_estimate=cost(40 * q_width * rows * 384),
         name="window",
-    )(scal, sink_logit, *operands)
+    )(scal, sink_logit, q_t, low, kv, high)
 
 
 def diff_kernel(chunks, rows, parts, count, scal_ref, lam_ref, gain_ref, *refs):
@@ -400,8 +367,8 @@
     blocks = (*kvs, *qs)
     return pl.pallas_call(
         functools.partial(diff_kernel, chunks, rows, parts, count),
-        in_specs=[smem(), smem(), whole(gain.shape)] + [whole(a.shape) for a in blocks],
-        out_specs=[whole((chunks, HEAD, size))] * heads,
+        in_specs=[smem()] * 2 + [vmem()] * (1 + len(blocks)),
+        out_specs=[vmem()] * heads,
         out_shape=[jax.ShapeDtypeStruct((chunks, HEAD, size), jnp.bfloat16)] * heads,
         scratch_shapes=[
             pltpu.VMEM((chunks * heads, HEAD, size), jnp.bfloat16),
@@ -411,29 +378,30 @@
             pltpu.VMEM((HEAD + 16, 2 * size), jnp.float32),
             pltpu.VMEM((1, 2 * size), jnp.float32),
         ],
-        grid=(1,),
         compiler_params=pltpu.CompilerParams(vmem_limit_bytes=32 << 20),
         cost_estimate=cost(1000 * heads * rows * rows * count),
         name="differential",
     )(scal, mix_lambda, gain, *blocks)
 
 
-def out_kernel(heads, parts, begin, scal_ref, win_keep_ref, win_send_ref, *refs):
+def out_kernel(heads, parts, offset, begin, scal_ref, win_ref, *refs):
     diff_refs = refs[:heads]
     win_w_ref, diff_w_ref, keep_ref, send_ref, stacked = refs[heads:]
-    here, core = scal_ref[0] // parts, scal_ref[2] % 2
+    here, me = scal_ref[0] // parts, scal_ref[2]
+    chip, core = (me // 2) ^ offset, me % 2
     half = stacked.shape[1]
-    win_width = win_keep_ref.shape[1]
+    win_width = win_ref.shape[1]
 
     @pl.when(pl.program_id(0) == 0)
     def _():
-        stacked[0, :, 0:win_width] = win_keep_ref[...]
-        stacked[1, :, 0:win_width] = win_send_ref[...]
+        for bit in range(2):
+            at = pl.multiple_of((me ^ (2 * offset + bit)) * half, half)
+            stacked[bit, :, 0:win_width] = win_ref[pl.ds(at, half), :]
         pieces = []
         for h in range(heads):
-            piece = diff_refs[0][0]
+            piece = diff_refs[0][chip]
             for d in range(1, heads):
-                piece = jnp.where((here ^ d) == h, diff_refs[d][0], piece)
+                piece = jnp.where((here ^ d) == h, diff_refs[d][chip], piece)
             pieces.append(piece)
         turned = jnp.transpose(jnp.concatenate(pieces, axis=0).astype(jnp.float32))
         turned = turned.astype(jnp.bfloat16)
@@ -455,33 +423,20 @@
     depth = win_out.shape[0] + diff_out.shape[0]
     size = diffs[0].shape[2]
     half = size // 2
-    q_width = win_rows.shape[1]
-
-    def rows_at(bit):
-        return lambda j, scal: (scal[2] ^ (2 * offset + bit), 0)
-
-    grid_spec = pltpu.PrefetchScalarGridSpec(
-        num_scalar_prefetch=1,
+
+    return pl.pallas_call(
+        functools.partial(out_kernel, heads, parts, offset, begin),
+        in_specs=[smem()] + [vmem()] * (3 + heads),
+        out_specs=[pl.BlockSpec((half, block), lambda j: (0, j))] * 2,
+        scratch_shapes=[pltpu.VMEM((2, half, depth), jnp.bfloat16)],
         grid=(width // block,),
-        in_specs=[pl.BlockSpec((half, q_width), rows_at(bit)) for bit in range(2)]
-        + [
-            pl.BlockSpec((1, HEAD, size), lambda j, scal: ((scal[2] // 2) ^ offset, 0, 0))
-            for _ in diffs
-        ]
-        + [pl.BlockSpec(memory_space=pltpu.VMEM)] * 2,
-        out_specs=[pl.BlockSpec((half, block), lambda j, scal: (0, j))] * 2,
-        scratch_shapes=[pltpu.VMEM((2, half, depth), jnp.bfloat16)],
-    )
-    return pl.pallas_call(
-        functools.partial(out_kernel, heads, parts, begin),
-        grid_spec=grid_spec,
         out_shape=[jax.ShapeDtypeStruct((half, width), jnp.bfloat16)] * 2,
         compiler_params=pltpu.CompilerParams(
             dimension_semantics=("arbitrary",), vmem_limit_bytes=16 << 20
         ),
         cost_estimate=cost(2 * size * depth * width),
         name="project_out",
-    )(scal, win_rows, win_rows, *diffs, win_out, diff_out)
+    )(scal, win_rows, *diffs, win_out, diff_out)
 
 
 def body(
@@ -507,24 +462,25 @@
     parts = sp // heads
     here, me = lax.axis_index("sp"), lax.axis_index("tp")
     weights = (win_query, win_key, win_value, diff_query, diff_key, diff_value)
-    steps = 2
     scal = jnp.stack([here, length[0], me]).astype(jnp.int32)
-    far_weights = fetch(scal, weights, list(range(2, tp)), tp)
-    out_weights = fetch(scal, (win_out, diff_out), [None], tp)
-
-    pieces = [inputs[c * size : (c + 1) * size] for c in range(chips)]
+    weights = fetch(weights, room=46 << 20)
+    out_weights = fetch((win_out, diff_out), room=38 << 20)
+
+    pieces = []
+    for c in range(chips):
+        pieces += fetch((inputs,), c * size, size)
     far = [
         [lax.ppermute(pieces[c], "tp", flip("tp", 2 * o)) for o in range(1, chips)]
         for c in range(chips)
     ]
     sib = lax.ppermute(inputs, "tp", flip("tp", 1))
-    acc = project_near(inputs, sib, weights, scal, steps)
+    acc = project_near(inputs, sib, weights, scal)
     q_parts, kv_parts, kvs, qs = [], [], [], []
     for c in range(chips):
         xs = []
         for piece in far[c]:
             xs += [piece, lax.ppermute(piece, "tp", flip("tp", 1))]
-        q_t, kv, *slots = project_far(acc, c, size, xs, far_weights, scal, heads, parts)
+        q_t, kv, *slots = project_far(acc, c, size, xs, weights, scal, heads, parts)
         q_parts.append(q_t)
         kv_parts.append(kv)
         moved = [slots[0]]
@@ -538,7 +494,13 @@
     down = [(i + 1, i) for i in range(sp - 1)]
     low = lax.ppermute(kv_parts[-1][size - WINDOW :], "sp", up)
     high = lax.ppermute(kv_parts[0][:WINDOW], "sp", down)
-    win_rows = window_part(scal, sink_logit, q_parts, kv_parts, low, high)
+    edges = [low, *kv_parts, high]
+    win_rows = []
+    for c in range(chips):
+        win_rows.append(
+            window_part(scal, sink_logit, q_parts[c], *edges[c : c + 3], c * size, rows)
+        )
+    win_rows = jnp.concatenate(win_rows)
 
     gain = head_gain.reshape(1, HEAD)
     mixed = diff_part(scal, mix_lambda, gain, kvs, qs, chips, rows, parts)
@@ -557,10 +519,10 @@
     def add(*values):
         return functools.reduce(lambda a, b: a + b, [v.astype(jnp.float32) for v in values])
 
-    cuts = (0, width // 4, width)
+    cuts = (0, width // 4, width // 2, width)
     arrived = []
     for begin, end in zip(cuts[:-1], cuts[1:]):
-        count = 1 if begin == 0 else 2
+        count = (end - begin) // block
         span = (end - begin) // count
         crossed = [[] for _ in range(count)]
         for o in range(1, chips):

time: 157 us -> 164 us (1.045)
  local copies, waits for them, and re-layouts: 10.3 us -> 2.7 us
  starting transfers between devices: 28 us -> 34.3 us
  Pallas kernels: 69.4 us -> 73.6 us
  waiting for transfers between devices: 46.5 us -> 49.7 us
    unnamed x34 -> x20, local copies, waits for them, and re-layouts: 7.82 us -> 2.61 us
    ppermute x3, waiting for transfers between devices: 0.01 us -> 4.34 us  [body(): diffs.append(lax.ppermute(mixed[d], 'sp', flip('sp', d * parts)))]
    pallas_call x9 -> x13, Pallas kernels: 27.5 us -> 31.7 us  [the longest x2 7.72 us: window_part(): pl.pallas_call(functools.partial(window_kernel, begin, whole_rows, kv_loc...]
    ppermute x2, waiting for transfers between devices: 2.91 us -> 0.01 us  [body(): lax.ppermute(mine, 'sp', flip('sp', e))]
    slice x1 -> x0, local copies, waits for them, and re-layouts: 2.37 us -> none  [body(): pieces = [inputs[c * size:(c + 1) * size] for c in range(chips)]]
    ppermute x6, waiting for transfers between devices: 7.34 us -> 9.67 us  [body(): moved.append(lax.ppermute(slots[d], 'sp', flip('sp', d * parts)))]
    ppermute x1, starting transfers between devices: 2.42 us -> 4.56 us  [body(): low = lax.ppermute(kv_parts[-1][size - WINDOW:], 'sp', up)]
    ppermute x2, starting transfers between devices: 3.16 us -> 4.95 us  [body(): lax.ppermute(mine, 'sp', flip('sp', e))]
  transfers between devices with their start and end apart: 24 -> 26, of which waited for: 8 -> 12; matrix products, arithmetic and copies ran while one was open for 2% -> 0% of each run, Pallas kernels for 42% -> 19%
where the time goes in v1:
time: 164 us
  Pallas kernels  73.6 us (45%)
  waiting for transfers between devices  49.7 us (30%)
  starting transfers between devices  34.3 us (21%)
  local copies, waits for them, and re-layouts  2.7 us (2%)
  other arithmetic  2.14 us (1%)
    pallas_call x1, Pallas kernels, diff_part(): pl.pallas_call(functools.partial(diff_kernel, chunks, rows, parts, count)...  41.9 us
    ppermute x4, waiting for transfers between devices, body(): crossed[i].append(lax.ppermute(piece, 'tp', flip('tp', 2 * o)))  20.7 us
    ppermute x2, waiting for transfers between devices, body(): lax.ppermute(pieces[c], 'tp', flip('tp', 2 * o))  15 us
    ppermute x6, waiting for transfers between devices, body(): moved.append(lax.ppermute(slots[d], 'sp', flip('sp', d * parts)))  9.67 us
    ppermute x6, starting transfers between devices, body(): moved.append(lax.ppermute(slots[d], 'sp', flip('sp', d * parts)))  9.4 us
    pallas_call x2, Pallas kernels, window_part(): pl.pallas_call(functools.partial(window_kernel, begin, whole_rows, kv_loc...  7.72 us
    pallas_call x4, Pallas kernels, out_part(): pl.pallas_call(functools.partial(out_kernel, heads, parts, offset, begin)...  7.55 us
    pallas_call x2, Pallas kernels, project_far(): pl.pallas_call(functools.partial(far_kernel, chunk * rows, count, heads,...  6.05 us
  transfers between devices with their start and end apart: 26, of which 12 were waited for; matrix products, arithmetic and copies ran while one was open for 0% of the time, Pallas kernels for 19%

profile of v1, /device:TPU:0, one launch (start us, length us, event | category | flops | bytes accessed | tf_op | source)
XLA Modules:
  0.0 163.5 jit_solution(7239410508958849540)
XLA Ops:
  0.0 0.5 collective-permute-start
  0.5 1.2 copy-done.4
  1.8 2.5 %collective-permute-start.1 = (bf16[256,1024]{1,0:T(8,128)(2,1)S(1)}, bf16[256,1024]{1,0:T(8,128)(2,1)}, u32[]{:S(2)}, u32[]{:S(2)}) collective-permute-start(bf16[256,1024]{1,0:T(8,128)(2,1)S(1)} %fetch.5), channel_id=1, source_target_pairs={{0,2},{1,3},{2,0},{3,1},{4,6},{5,7},{6,4},{7,5},{8,10},{9,11},{10,... | collective-permute-start | bytes 1572872 | tf_op jit(solution)/shard_map/ppermute | solution.py:473
  4.3 0.8 fetch.6
  5.2 1.2 collective-permute-start.3
  6.3 10.9 %collective-permute-done.1.refs_0_ = bf16[256,1024]{1,0:T(8,128)(2,1)} collective-permute-done((bf16[256,1024]{1,0:T(8,128)(2,1)S(1)}, bf16[256,1024]{1,0:T(8,128)(2,1)}, u32[]{:S(2)}, u32[]{:S(2)}) %collective-permute-start.1) | collective-permute-done | bytes 524320 | tf_op jit(solution)/shard_map/ppermute | solution.py:473
  17.2 0.4 fetch.7
  17.6 1.3 copy-done
  19.6 4.5 %fetch.4 = (bf16[4096,384]{1,0:T(8,128)(2,1)S(1)}, bf16[4096,128]{1,0:T(8,128)(2,1)S(1)}, bf16[4096,128]{1,0:T(8,128)(2,1)S(1)}, bf16[4096,256]{1,0:T(8,128)(2,1...) custom-call(bf16[4096,384]{1,0:T(8,128)(2,1)} %refs_0_.4, bf16[4096,128]{1,0:T(8,128)(2,1)} %refs_1_.2, ...), custom_call_target="tpu_custom_call" | custom-call | flops 1073741824 | tf_op jit(solution)/shard_map/fetch/pallas_call | solution.py:87
  24.1 4.1 %collective-permute-done.3.refs_0_ = bf16[256,1024]{1,0:T(8,128)(2,1)} collective-permute-done((bf16[256,1024]{1,0:T(8,128)(2,1)}, bf16[256,1024]{1,0:T(8,128)(2,1)}, u32[]{:S(2)}, u32[]{:S(2)}) %collective-permute-start.3) | collective-permute-done | bytes 524320 | tf_op jit(solution)/shard_map/ppermute | solution.py:473
  28.4 4.6 %project_near.1.acc_ref = f32[512,1408]{1,0:T(8,128)S(1)} custom-call(s32[3]{0:T(128)S(1)} %pad_add_fusion.scal_ref, bf16[512,1024]{1,0:T(8,128)(2,1)S(1)} %copy-done.6, bf16[512,1024]{1,0:T(8,128)(2,1)} %collective-permute-done.sib_ref, bf16[4096,384]{1,0:T(8,128)(2,1)S(1)} %get-tuple-element.37.refs_0_.refs_2_, ...), custom_call_target="tpu_custom_call" | custom-call | flops 2952790016 | tf_op jit(solution)/shard_map/project_near/pallas_call | solution.py:59
  33.0 3.1 %project_far.2 = (bf16[384,256]{1,0:T(8,128)(2,1)S(1)}, bf16[256,256]{1,0:T(8,128)(2,1)S(1)}, bf16[384,128]{1,0:T(8,128)(2,1)S(1)}, bf16[384,128]{1,0:T(8,128)(2...) custom-call(s32[3]{0:T(128)S(1)} %pad_add_fusion.scal_ref, f32[512,1408]{1,0:T(8,128)S(1)} %project_near.1.acc_ref, ...), custom_call_target="tpu_custom_call" | custom-call | flops 1476395008 | tf_op jit(solution)/shard_map/project_far/pallas_call | solution.py:142
  36.1 1.3 collective-permute-start.6
  37.5 2.9 %project_far.3 = (bf16[384,256]{1,0:T(8,128)(2,1)S(1)}, bf16[256,256]{1,0:T(8,128)(2,1)S(1)}, bf16[384,128]{1,0:T(8,128)(2,1)S(1)}, bf16[384,128]{1,0:T(8,128)(2...) custom-call(s32[3]{0:T(128)S(1)} %pad_add_fusion.scal_ref, f32[512,1408]{1,0:T(8,128)S(1)} %project_near.1.acc_ref, ...), custom_call_target="tpu_custom_call" | custom-call | flops 1476395008 | tf_op jit(solution)/shard_map/project_far/pallas_call | solution.py:142
  40.4 4.6 %collective-permute-start.5 = (bf16[128,256]{1,0:T(8,128)(2,1)S(1)}, bf16[128,256]{1,0:T(8,128)(2,1)S(1)}, u32[]{:S(2)}, u32[]{:S(2)}) collective-permute-start(bf16[128,256]{1,0:T(8,128)(2,1)S(1)} %slice.60), channel_id=1, source_target_pairs={{0,4},{4,8},{8,12},{12,16},{16,20},{20,24},{24,28},{1,5},{5,9},{9,... | collective-permute-start | bytes 196616 | tf_op jit(solution)/shard_map/ppermute | solution.py:495
  45.0 3.9 %collective-permute-start.9 = (bf16[384,128]{1,0:T(8,128)(2,1)S(1)}, bf16[384,128]{1,0:T(8,128)(2,1)S(1)}, u32[]{:S(2)}, u32[]{:S(2)}) collective-permute-start(bf16[384,128]{1,0:T(8,128)(2,1)S(1)} %get-tuple-element.50), channel_id=1, source_target_pairs={{0,24},{4,28},{8,16},{12,20},{16,8},{20,12},{24,0},{28,4},{1,25},{... | collective-permute-start | bytes 294920 | tf_op jit(solution)/shard_map/ppermute | solution.py:488
  48.9 0.6 collective-permute-start.7
  49.6 3.1 %collective-permute-done.9.refs_7_ = bf16[384,128]{1,0:T(8,128)(2,1)S(1)} collective-permute-done((bf16[384,128]{1,0:T(8,128)(2,1)S(1)}, bf16[384,128]{1,0:T(8,128)(2,1)S(1)}, u32[]{:S(2)}, u32[]{:S(2)}) %collective-permute-start.9) | collective-permute-done | bytes 98336 | tf_op jit(solution)/shard_map/ppermute | solution.py:488
  52.7 3.8 %collective-permute-start.13 = (bf16[384,128]{1,0:T(8,128)(2,1)S(1)}, bf16[384,128]{1,0:T(8,128)(2,1)S(1)}, u32[]{:S(2)}, u32[]{:S(2)}) collective-permute-start(bf16[384,128]{1,0:T(8,128)(2,1)S(1)} %get-tuple-element.54), channel_id=1, source_target_pairs={{0,24},{4,28},{8,16},{12,20},{16,8},{20,12},{24,0},{28,4},{1,25},{... | collective-permute-start | bytes 294920 | tf_op jit(solution)/shard_map/ppermute | solution.py:488
  56.4 5.0 %collective-permute-done.8.refs_6_ = bf16[384,128]{1,0:T(8,128)(2,1)S(1)} collective-permute-done((bf16[384,128]{1,0:T(8,128)(2,1)S(1)}, bf16[384,128]{1,0:T(8,128)(2,1)S(1)}, u32[]{:S(2)}, u32[]{:S(2)}) %collective-permute-start.8) | collective-permute-done | bytes 98336 | tf_op jit(solution)/shard_map/ppermute | solution.py:488
  61.4 1.1 collective-permute-start.11
  62.5 3.0 %collective-permute-start.10 = (bf16[4,256,128]{2,1,0:T(8,128)(2,1)S(1)}, bf16[4,256,128]{2,1,0:T(8,128)(2,1)S(1)}, u32[]{:S(2)}, u32[]{:S(2)}) collective-permute-start(bf16[4,256,128]{2,1,0:T(8,128)(2,1)S(1)} %pad_maximum_fusion.2.refs_0_), channel_id=1, source_target_pairs={{0,4},{4,0},{8,12},{12,8},{16,20},{20,16},{24,28},{28,24},{1,5},{5... | collective-permute-start | bytes 786440 | tf_op jit(solution)/shard_map/ppermute | solution.py:490
  65.5 1.5 collective-permute-done.12.refs_10_
  67.2 2.0 %collective-permute-start.14 = (bf16[4,256,128]{2,1,0:T(8,128)(2,1)S(1)}, bf16[4,256,128]{2,1,0:T(8,128)(2,1)S(1)}, u32[]{:S(2)}, u32[]{:S(2)}) collective-permute-start(bf16[4,256,128]{2,1,0:T(8,128)(2,1)S(1)} %pad_maximum_fusion.3.refs_2_), channel_id=1, source_target_pairs={{0,4},{4,0},{8,12},{12,8},{16,20},{20,16},{24,28},{28,24},{1,5},{5... | collective-permute-start | bytes 786440 | tf_op jit(solution)/shard_map/ppermute | solution.py:490
  69.2 3.8 %window.3 = bf16[256,384]{1,0:T(8,128)(2,1)S(1)} custom-call(s32[3]{0:T(128)S(1)} %pad_add_fusion.scal_ref, f32[6]{0:T(128)S(1)} %copy-done.7, bf16[384,256]{1,0:T(8,128)(2,1)S(1)} %get-tuple-element.46.refs_0_, bf16[256,256]{1,0:T(8,128)(2,1)S(1)} %get-tuple-element.45.refs_2_.refs_1_, bf16[256,256]{1,0:T(8,128)(2,1)S(1)} %get-tuple-element.44.refs_3_.refs_2_, ...), custom_call_target="tpu_custom_call" | custom-call | flops 1509949440 | tf_op jit(solution)/shard_map/window/pallas_call | solution.py:219
  73.0 3.9 %window.2 = bf16[256,384]{1,0:T(8,128)(2,1)S(1)} custom-call(s32[3]{0:T(128)S(1)} %pad_add_fusion.scal_ref, f32[6]{0:T(128)S(1)} %copy-done.7, bf16[384,256]{1,0:T(8,128)(2,1)S(1)} %get-tuple-element.43.refs_0_, bf16[128,256]{1,0:T(8,128)(2,1)S(1)} %collective-permute-done.5.refs_1_, bf16[256,256]{1,0:T(8,128)(2,1)S(1)} %get-tuple-element.45.refs_2_.refs_1_, ...), custom_call_target="tpu_custom_call" | custom-call | flops 1509949440 | tf_op jit(solution)/shard_map/window/pallas_call | solution.py:219
  77.0 41.9 %differential.1 = (bf16[2,64,256]{2,1,0:T(8,128)(2,1)S(1)}, bf16[2,64,256]{2,1,0:T(8,128)(2,1)S(1)}, bf16[2,64,256]{2,1,0:T(8,128)(2,1)S(1)}, bf16[2,64,256]{2,1,0:T(8,128)(2,1)S(1)}) custom-call(s32[3]{0:T(128)S(1)} %pad_add_fusion.scal_ref, f32[4]{0:T(128)S(1)} %copy-done.8, f32[1,64]{1,0:T(1,128)S(1)} %bitcast.19, ...), custom_call_target="tpu_custom_call" | custom-call | flops 8388608000 | tf_op jit(solution)/shard_map/differential/pallas_call | solution.py:368
  118.9 1.0 collective-permute-start.15
  119.9 1.7 %collective-permute-start.16 = (bf16[2,64,256]{2,1,0:T(8,128)(2,1)S(1)}, bf16[2,64,256]{2,1,0:T(8,128)(2,1)S(1)}, u32[]{:S(2)}, u32[]{:S(2)}) collective-permute-start(bf16[2,64,256]{2,1,0:T(8,128)(2,1)S(1)} %get-tuple-element.57), channel_id=1, source_target_pairs={{0,16},{4,20},{8,24},{12,28},{16,0},{20,4},{24,8},{28,12},{1,17},{... | collective-permute-start | bytes 196616 | tf_op jit(solution)/shard_map/ppermute | solution.py:509
  121.7 1.7 %collective-permute-start.17 = (bf16[2,64,256]{2,1,0:T(8,128)(2,1)S(1)}, bf16[2,64,256]{2,1,0:T(8,128)(2,1)S(1)}, u32[]{:S(2)}, u32[]{:S(2)}) collective-permute-start(bf16[2,64,256]{2,1,0:T(8,128)(2,1)S(1)} %get-tuple-element.58), channel_id=1, source_target_pairs={{0,24},{4,28},{8,16},{12,20},{16,8},{20,12},{24,0},{28,4},{1,25},{... | collective-permute-start | bytes 196616 | tf_op jit(solution)/shard_map/ppermute | solution.py:509
  123.5 2.7 %collective-permute-done.16.refs_2_ = bf16[2,64,256]{2,1,0:T(8,128)(2,1)S(1)} collective-permute-done((bf16[2,64,256]{2,1,0:T(8,128)(2,1)S(1)}, bf16[2,64,256]{2,1,0:T(8,128)(2,1)S(1)}, u32[]{:S(2)}, u32[]{:S(2)}) %collective-permute-start.16) | collective-permute-done | bytes 65568 | tf_op jit(solution)/shard_map/ppermute | solution.py:509
  126.1 1.6 collective-permute-done.17.refs_3_
  127.7 1.2 project_out.5
  129.0 2.0 %project_out.7 = (bf16[128,2048]{1,0:T(8,128)(2,1)S(1)}, bf16[128,2048]{1,0:T(8,128)(2,1)S(1)}) custom-call(s32[3]{0:T(128)S(1)} %pad_add_fusion.scal_ref, bf16[512,384]{1,0:T(8,128)(2,1)S(1)} %pad_maximum_fusion.1.win_ref, bf16[2,64,256]{2,1,0:T(8,128)(2,1)S(1)} %get-tuple-element.55.refs_0_, bf16[2,64,256]{2,1,0:T(8,128)(2,1)S(1)} %collective-permute-done.15.refs_1_, ...), custom_call_target="tpu_custom_call" | custom-call | flops 671088640 | tf_op jit(solution)/shard_map/project_out/pallas_call | solution.py:427
  131.0 0.5 collective-permute-start.23
  131.5 1.2 project_out.6
  132.8 3.2 %project_out.4 = (bf16[128,4096]{1,0:T(8,128)(2,1)S(1)}, bf16[128,4096]{1,0:T(8,128)(2,1)S(1)}) custom-call(s32[3]{0:T(128)S(1)} %pad_add_fusion.scal_ref, bf16[512,384]{1,0:T(8,128)(2,1)S(1)} %pad_maximum_fusion.1.win_ref, bf16[2,64,256]{2,1,0:T(8,128)(2,1)S(1)} %get-tuple-element.55.refs_0_, bf16[2,64,256]{2,1,0:T(8,128)(2,1)S(1)} %collective-permute-done.15.refs_1_, ...), custom_call_target="tpu_custom_call" | custom-call | flops 1342177280 | tf_op jit(solution)/shard_map/project_out/pallas_call | solution.py:427
  136.0 0.5 collective-permute-start.18
  136.7 1.5 collective-permute-start.20
  138.3 0.6 collective-permute-start.22
  139.1 1.5 collective-permute-start.25
  140.6 0.6 collective-permute-start.24
  141.2 4.7 %collective-permute-done.20 = bf16[128,1024]{1,0:T(8,128)(2,1)S(1)} collective-permute-done((bf16[128,1024]{1,0:T(8,128)(2,1)S(1)}, bf16[128,1024]{1,0:T(8,128)(2,1)S(1)}, u32[]{:S(2)}, u32[]{:S(2)}) %collective-permute-start.20) | collective-permute-done | bytes 262176 | tf_op jit(solution)/shard_map/ppermute | solution.py:534
  145.9 5.6 %collective-permute-done.22 = bf16[128,1024]{1,0:T(8,128)(2,1)S(1)} collective-permute-done((bf16[128,1024]{1,0:T(8,128)(2,1)S(1)}, bf16[128,1024]{1,0:T(8,128)(2,1)S(1)}, u32[]{:S(2)}, u32[]{:S(2)}) %collective-permute-start.22) | collective-permute-done | bytes 262176 | tf_op jit(solution)/shard_map/ppermute | solution.py:534
  151.5 5.6 %collective-permute-done.25 = bf16[128,1024]{1,0:T(8,128)(2,1)S(1)} collective-permute-done((bf16[128,1024]{1,0:T(8,128)(2,1)S(1)}, bf16[128,1024]{1,0:T(8,128)(2,1)S(1)}, u32[]{:S(2)}, u32[]{:S(2)}) %collective-permute-start.25) | collective-permute-done | bytes 262176 | tf_op jit(solution)/shard_map/ppermute | solution.py:534
  157.1 4.7 %collective-permute-done.24 = bf16[128,1024]{1,0:T(8,128)(2,1)S(1)} collective-permute-done((bf16[128,1024]{1,0:T(8,128)(2,1)S(1)}, bf16[128,1024]{1,0:T(8,128)(2,1)S(1)}, u32[]{:S(2)}, u32[]{:S(2)}) %collective-permute-start.24) | collective-permute-done | bytes 262176 | tf_op jit(solution)/shard_map/ppermute | solution.py:534
  161.8 0.7 add_convert_fusion.5
  162.5 1.0 pad_maximum_fusion
  (58 shorter events, 1.0 us)
Async XLA Ops:
  0.0 28.4 %collective-permute-start = (bf16[512,1024]{1,0:T(8,128)(2,1)}, bf16[512,1024]{1,0:T(8,128)(2,1)}, u32[]{:S(2)}, u32[]{:S(2)}) collective-permute-start(bf16[512,1024]{1,0:T(8,128)(2,1)} %refs_0_.6), channel_id=1, source_target_pairs={{0,1},{1,0},{2,3},{3,2},{4,5},{5,4},{6,7},{7,6},{8,9},{9,8},{10,11... | collective-permute-start | bytes 3145736 | tf_op jit(solution)/shard_map/ppermute | solution.py:476
  0.5 1.2 copy-start.4
  1.7 2.6 %copy-start.5 = (bf16[512,1024]{1,0:T(8,128)(2,1)S(1)}, bf16[512,1024]{1,0:T(8,128)(2,1)}, u32[]{:S(2)}) copy-start(bf16[512,1024]{1,0:T(8,128)(2,1)} %refs_0_.6) | copy-start | bytes 3145732
  1.7 15.5 %copy-start.3 = (bf16[256,4096]{1,0:T(8,128)(2,1)S(1)}, bf16[256,4096]{1,0:T(8,128)(2,1)}, u32[]{:S(2)}) copy-start(bf16[256,4096]{1,0:T(8,128)(2,1)} %refs_1_.3) | copy-start | bytes 6291460
  1.8 15.4 %copy-start.2 = (bf16[384,4096]{1,0:T(8,128)(2,1)S(1)}, bf16[384,4096]{1,0:T(8,128)(2,1)}, u32[]{:S(2)}) copy-start(bf16[384,4096]{1,0:T(8,128)(2,1)} %refs_0_.7) | copy-start | bytes 9437188
  1.8 15.4 %collective-permute-start.1 = (bf16[256,1024]{1,0:T(8,128)(2,1)S(1)}, bf16[256,1024]{1,0:T(8,128)(2,1)}, u32[]{:S(2)}, u32[]{:S(2)}) collective-permute-start(bf16[256,1024]{1,0:T(8,128)(2,1)S(1)} %fetch.5), channel_id=1, source_target_pairs={{0,2},{1,3},{2,0},{3,1},{4,6},{5,7},{6,4},{7,5},{8,10},{9,11},{10,... | collective-permute-start | bytes 1572872 | tf_op jit(solution)/shard_map/ppermute | solution.py:473
  5.2 23.1 %collective-permute-start.3 = (bf16[256,1024]{1,0:T(8,128)(2,1)}, bf16[256,1024]{1,0:T(8,128)(2,1)}, u32[]{:S(2)}, u32[]{:S(2)}) collective-permute-start(bf16[256,1024]{1,0:T(8,128)(2,1)} %fetch.6), channel_id=1, source_target_pairs={{0,2},{1,3},{2,0},{3,1},{4,6},{5,7},{6,4},{7,5},{8,10},{9,11},{10,... | collective-permute-start | bytes 1572872 | tf_op jit(solution)/shard_map/ppermute | solution.py:473
  17.2 15.8 %collective-permute-start.2 = (bf16[256,1024]{1,0:T(8,128)(2,1)}, bf16[256,1024]{1,0:T(8,128)(2,1)}, u32[]{:S(2)}, u32[]{:S(2)}) collective-permute-start(bf16[256,1024]{1,0:T(8,128)(2,1)} %collective-permute-done.1.refs_0_), channel_id=1, source_target_pairs={{0,1},{1,0},{2,3},{3,2},{4,5},{5,4},{6,7},{7,6},{8,9},{9,8},{10,11... | collective-permute-start | bytes 1572872 | tf_op jit(solution)/shard_map/ppermute | solution.py:482
  17.6 1.3 copy-start
  19.6 8.7 %copy-start.6 = (bf16[512,1024]{1,0:T(8,128)(2,1)S(1)}, bf16[512,1024]{1,0:T(8,128)(2,1)}, u32[]{:S(2)}) copy-start(bf16[512,1024]{1,0:T(8,128)(2,1)} %refs_0_.6) | copy-start | bytes 3145732
  28.3 9.2 %collective-permute-start.4 = (bf16[256,1024]{1,0:T(8,128)(2,1)}, bf16[256,1024]{1,0:T(8,128)(2,1)S(1)}, u32[]{:S(2)}, u32[]{:S(2)}) collective-permute-start(bf16[256,1024]{1,0:T(8,128)(2,1)} %collective-permute-done.3.refs_0_), channel_id=1, source_target_pairs={{0,1},{1,0},{2,3},{3,2},{4,5},{5,4},{6,7},{7,6},{8,9},{9,8},{10,11... | collective-permute-start | bytes 1572872 | tf_op jit(solution)/shard_map/ppermute | solution.py:482
  36.1 33.0 %collective-permute-start.6 = (bf16[128,256]{1,0:T(8,128)(2,1)S(1)}, bf16[128,256]{1,0:T(8,128)(2,1)S(1)}, u32[]{:S(2)}, u32[]{:S(2)}) collective-permute-start(bf16[128,256]{1,0:T(8,128)(2,1)S(1)} %slice.61), channel_id=1, source_target_pairs={{4,0},{8,4},{12,8},{16,12},{20,16},{24,20},{28,24},{5,1},{9,5},{13... | collective-permute-start | bytes 196616 | tf_op jit(solution)/shard_map/ppermute | solution.py:496
  40.4 28.8 %copy-start.7 = (f32[6]{0:T(128)S(1)}, f32[6]{0:T(128)}, u32[]{:S(2)}) copy-start(f32[6]{0:T(128)} %sink_ref.3) | copy-start | bytes 76
  40.4 32.5 %collective-permute-start.5 = (bf16[128,256]{1,0:T(8,128)(2,1)S(1)}, bf16[128,256]{1,0:T(8,128)(2,1)S(1)}, u32[]{:S(2)}, u32[]{:S(2)}) collective-permute-start(bf16[128,256]{1,0:T(8,128)(2,1)S(1)} %slice.60), channel_id=1, source_target_pairs={{0,4},{4,8},{8,12},{12,16},{16,20},{20,24},{24,28},{1,5},{5,9},{9,... | collective-permute-start | bytes 196616 | tf_op jit(solution)/shard_map/ppermute | solution.py:495
  45.0 7.7 %collective-permute-start.9 = (bf16[384,128]{1,0:T(8,128)(2,1)S(1)}, bf16[384,128]{1,0:T(8,128)(2,1)S(1)}, u32[]{:S(2)}, u32[]{:S(2)}) collective-permute-start(bf16[384,128]{1,0:T(8,128)(2,1)S(1)} %get-tuple-element.50), channel_id=1, source_target_pairs={{0,24},{4,28},{8,16},{12,20},{16,8},{20,12},{24,0},{28,4},{1,25},{... | collective-permute-start | bytes 294920 | tf_op jit(solution)/shard_map/ppermute | solution.py:488
  48.9 12.5 %collective-permute-start.8 = (bf16[384,128]{1,0:T(8,128)(2,1)S(1)}, bf16[384,128]{1,0:T(8,128)(2,1)S(1)}, u32[]{:S(2)}, u32[]{:S(2)}) collective-permute-start(bf16[384,128]{1,0:T(8,128)(2,1)S(1)} %get-tuple-element.49), channel_id=1, source_target_pairs={{0,16},{4,20},{8,24},{12,28},{16,0},{20,4},{24,8},{28,12},{1,17},{... | collective-permute-start | bytes 294920 | tf_op jit(solution)/shard_map/ppermute | solution.py:488
  48.9 12.5 %collective-permute-start.7 = (bf16[384,128]{1,0:T(8,128)(2,1)S(1)}, bf16[384,128]{1,0:T(8,128)(2,1)S(1)}, u32[]{:S(2)}, u32[]{:S(2)}) collective-permute-start(bf16[384,128]{1,0:T(8,128)(2,1)S(1)} %get-tuple-element.48), channel_id=1, source_target_pairs={{0,8},{4,12},{8,0},{12,4},{16,24},{20,28},{24,16},{28,20},{1,9},{5... | collective-permute-start | bytes 294920 | tf_op jit(solution)/shard_map/ppermute | solution.py:488
  52.7 9.9 %collective-permute-start.13 = (bf16[384,128]{1,0:T(8,128)(2,1)S(1)}, bf16[384,128]{1,0:T(8,128)(2,1)S(1)}, u32[]{:S(2)}, u32[]{:S(2)}) collective-permute-start(bf16[384,128]{1,0:T(8,128)(2,1)S(1)} %get-tuple-element.54), channel_id=1, source_target_pairs={{0,24},{4,28},{8,16},{12,20},{16,8},{20,12},{24,0},{28,4},{1,25},{... | collective-permute-start | bytes 294920 | tf_op jit(solution)/shard_map/ppermute | solution.py:488
  61.4 5.6 %collective-permute-start.12 = (bf16[384,128]{1,0:T(8,128)(2,1)S(1)}, bf16[384,128]{1,0:T(8,128)(2,1)S(1)}, u32[]{:S(2)}, u32[]{:S(2)}) collective-permute-start(bf16[384,128]{1,0:T(8,128)(2,1)S(1)} %get-tuple-element.53), channel_id=1, source_target_pairs={{0,16},{4,20},{8,24},{12,28},{16,0},{20,4},{24,8},{28,12},{1,17},{... | collective-permute-start | bytes 294920 | tf_op jit(solution)/shard_map/ppermute | solution.py:488
  61.4 5.7 %collective-permute-start.11 = (bf16[384,128]{1,0:T(8,128)(2,1)S(1)}, bf16[384,128]{1,0:T(8,128)(2,1)S(1)}, u32[]{:S(2)}, u32[]{:S(2)}) collective-permute-start(bf16[384,128]{1,0:T(8,128)(2,1)S(1)} %get-tuple-element.52), channel_id=1, source_target_pairs={{0,8},{4,12},{8,0},{12,4},{16,24},{20,28},{24,16},{28,20},{1,9},{5... | collective-permute-start | bytes 294920 | tf_op jit(solution)/shard_map/ppermute | solution.py:488
  62.5 14.4 %collective-permute-start.10 = (bf16[4,256,128]{2,1,0:T(8,128)(2,1)S(1)}, bf16[4,256,128]{2,1,0:T(8,128)(2,1)S(1)}, u32[]{:S(2)}, u32[]{:S(2)}) collective-permute-start(bf16[4,256,128]{2,1,0:T(8,128)(2,1)S(1)} %pad_maximum_fusion.2.refs_0_), channel_id=1, source_target_pairs={{0,4},{4,0},{8,12},{12,8},{16,20},{20,16},{24,28},{28,24},{1,5},{5... | collective-permute-start | bytes 786440 | tf_op jit(solution)/shard_map/ppermute | solution.py:490
  67.2 9.8 %collective-permute-start.14 = (bf16[4,256,128]{2,1,0:T(8,128)(2,1)S(1)}, bf16[4,256,128]{2,1,0:T(8,128)(2,1)S(1)}, u32[]{:S(2)}, u32[]{:S(2)}) collective-permute-start(bf16[4,256,128]{2,1,0:T(8,128)(2,1)S(1)} %pad_maximum_fusion.3.refs_2_), channel_id=1, source_target_pairs={{0,4},{4,0},{8,12},{12,8},{16,20},{20,16},{24,28},{28,24},{1,5},{5... | collective-permute-start | bytes 786440 | tf_op jit(solution)/shard_map/ppermute | solution.py:490
  73.0 4.0 %copy-start.8 = (f32[4]{0:T(128)S(1)}, f32[4]{0:T(128)}, u32[]{:S(2)}) copy-start(f32[4]{0:T(128)} %lam_ref.1) | copy-start | bytes 52
  73.0 4.0 %copy-start.9 = (f32[64]{0:T(128)S(1)}, f32[64]{0:T(128)}, u32[]{:S(2)}) copy-start(f32[64]{0:T(128)} %param.23) | copy-start | bytes 772
  77.0 50.8 %copy-start.1 = (bf16[256,4096]{1,0:T(8,128)(2,1)S(1)}, bf16[256,4096]{1,0:T(8,128)(2,1)}, u32[]{:S(2)}) copy-start(bf16[256,4096]{1,0:T(8,128)(2,1)} %copy-done) | copy-start | bytes 6291460
  118.9 4.5 %collective-permute-start.15 = (bf16[2,64,256]{2,1,0:T(8,128)(2,1)S(1)}, bf16[2,64,256]{2,1,0:T(8,128)(2,1)S(1)}, u32[]{:S(2)}, u32[]{:S(2)}) collective-permute-start(bf16[2,64,256]{2,1,0:T(8,128)(2,1)S(1)} %get-tuple-element.56), channel_id=1, source_target_pairs={{0,8},{4,12},{8,0},{12,4},{16,24},{20,28},{24,16},{28,20},{1,9},{5... | collective-permute-start | bytes 196616 | tf_op jit(solution)/shard_map/ppermute | solution.py:509
  119.9 6.2 %collective-permute-start.16 = (bf16[2,64,256]{2,1,0:T(8,128)(2,1)S(1)}, bf16[2,64,256]{2,1,0:T(8,128)(2,1)S(1)}, u32[]{:S(2)}, u32[]{:S(2)}) collective-permute-start(bf16[2,64,256]{2,1,0:T(8,128)(2,1)S(1)} %get-tuple-element.57), channel_id=1, source_target_pairs={{0,16},{4,20},{8,24},{12,28},{16,0},{20,4},{24,8},{28,12},{1,17},{... | collective-permute-start | bytes 196616 | tf_op jit(solution)/shard_map/ppermute | solution.py:509
  121.7 6.1 %collective-permute-start.17 = (bf16[2,64,256]{2,1,0:T(8,128)(2,1)S(1)}, bf16[2,64,256]{2,1,0:T(8,128)(2,1)S(1)}, u32[]{:S(2)}, u32[]{:S(2)}) collective-permute-start(bf16[2,64,256]{2,1,0:T(8,128)(2,1)S(1)} %get-tuple-element.58), channel_id=1, source_target_pairs={{0,24},{4,28},{8,16},{12,20},{16,8},{20,12},{24,0},{28,4},{1,25},{... | collective-permute-start | bytes 196616 | tf_op jit(solution)/shard_map/ppermute | solution.py:509
  128.9 7.6 %collective-permute-start.19 = (bf16[128,1024]{1,0:T(8,128)(2,1)S(1)}, bf16[128,1024]{1,0:T(8,128)(2,1)S(1)}, u32[]{:S(2)}, u32[]{:S(2)}) collective-permute-start(bf16[128,1024]{1,0:T(8,128)(2,1)S(1)} %get-tuple-element.64), channel_id=1, source_target_pairs={{0,1},{1,0},{2,3},{3,2},{4,5},{5,4},{6,7},{7,6},{8,9},{9,8},{10,11... | collective-permute-start | bytes 786440 | tf_op jit(solution)/shard_map/ppermute | solution.py:530
  131.0 7.9 %collective-permute-start.23 = (bf16[128,2048]{1,0:T(8,128)(2,1)S(1)}, bf16[128,2048]{1,0:T(8,128)(2,1)S(1)}, u32[]{:S(2)}, u32[]{:S(2)}) collective-permute-start(bf16[128,2048]{1,0:T(8,128)(2,1)S(1)} %get-tuple-element.68), channel_id=1, source_target_pairs={{0,1},{1,0},{2,3},{3,2},{4,5},{5,4},{6,7},{7,6},{8,9},{9,8},{10,11... | collective-permute-start | bytes 1572872 | tf_op jit(solution)/shard_map/ppermute | solution.py:530
  132.7 5.5 %collective-permute-start.21 = (bf16[128,1024]{1,0:T(8,128)(2,1)S(1)}, bf16[128,1024]{1,0:T(8,128)(2,1)S(1)}, u32[]{:S(2)}, u32[]{:S(2)}) collective-permute-start(bf16[128,1024]{1,0:T(8,128)(2,1)S(1)} %get-tuple-element.66), channel_id=1, source_target_pairs={{0,1},{1,0},{2,3},{3,2},{4,5},{5,4},{6,7},{7,6},{8,9},{9,8},{10,11... | collective-permute-start | bytes 786440 | tf_op jit(solution)/shard_map/ppermute | solution.py:530
  136.0 25.8 %collective-permute-start.18 = (bf16[128,4096]{1,0:T(8,128)(2,1)S(1)}, bf16[128,4096]{1,0:T(8,128)(2,1)S(1)}, u32[]{:S(2)}, u32[]{:S(2)}) collective-permute-start(bf16[128,4096]{1,0:T(8,128)(2,1)S(1)} %get-tuple-element.62), channel_id=1, source_target_pairs={{0,1},{1,0},{2,3},{3,2},{4,5},{5,4},{6,7},{7,6},{8,9},{9,8},{10,11... | collective-permute-start | bytes 3145736 | tf_op jit(solution)/shard_map/ppermute | solution.py:537
  136.7 9.2 %collective-permute-start.20 = (bf16[128,1024]{1,0:T(8,128)(2,1)S(1)}, bf16[128,1024]{1,0:T(8,128)(2,1)S(1)}, u32[]{:S(2)}, u32[]{:S(2)}) collective-permute-start(bf16[128,1024]{1,0:T(8,128)(2,1)S(1)} %add_convert_fusion.6), channel_id=1, source_target_pairs={{0,2},{1,3},{2,0},{3,1},{4,6},{5,7},{6,4},{7,5},{8,10},{9,11},{10,... | collective-permute-start | bytes 786440 | tf_op jit(solution)/shard_map/ppermute | solution.py:534
  138.3 13.3 %collective-permute-start.22 = (bf16[128,1024]{1,0:T(8,128)(2,1)S(1)}, bf16[128,1024]{1,0:T(8,128)(2,1)S(1)}, u32[]{:S(2)}, u32[]{:S(2)}) collective-permute-start(bf16[128,1024]{1,0:T(8,128)(2,1)S(1)} %add_convert_fusion.4), channel_id=1, source_target_pairs={{0,2},{1,3},{2,0},{3,1},{4,6},{5,7},{6,4},{7,5},{8,10},{9,11},{10,... | collective-permute-start | bytes 786440 | tf_op jit(solution)/shard_map/ppermute | solution.py:534
  139.1 18.1 %collective-permute-start.25 = (bf16[128,1024]{1,0:T(8,128)(2,1)S(1)}, bf16[128,1024]{1,0:T(8,128)(2,1)S(1)}, u32[]{:S(2)}, u32[]{:S(2)}) collective-permute-start(bf16[128,1024]{1,0:T(8,128)(2,1)S(1)} %get-tuple-element.74), channel_id=1, source_target_pairs={{0,2},{1,3},{2,0},{3,1},{4,6},{5,7},{6,4},{7,5},{8,10},{9,11},{10,... | collective-permute-start | bytes 786440 | tf_op jit(solution)/shard_map/ppermute | solution.py:534
  140.6 21.2 %collective-permute-start.24 = (bf16[128,1024]{1,0:T(8,128)(2,1)S(1)}, bf16[128,1024]{1,0:T(8,128)(2,1)S(1)}, u32[]{:S(2)}, u32[]{:S(2)}) collective-permute-start(bf16[128,1024]{1,0:T(8,128)(2,1)S(1)} %get-tuple-element.73), channel_id=1, source_target_pairs={{0,2},{1,3},{2,0},{3,1},{4,6},{5,7},{6,4},{7,5},{8,10},{9,11},{10,... | collective-permute-start | bytes 786440 | tf_op jit(solution)/shard_map/ppermute | solution.py:534

commit v2 on v1

--- a/solution.py
+++ b/solution.py
@@ -63,7 +63,6 @@
         out_shape=jax.ShapeDtypeStruct((rows, width), jnp.float32),
         compiler_params=pltpu.CompilerParams(vmem_limit_bytes=24 << 20),
         cost_estimate=cost(4 * rows * depth * width),
-        name="project_near",
     )(scal, own, sib, *weights)
 
 
@@ -92,7 +91,6 @@
         scratch_shapes=[pltpu.SemaphoreType.DMA((len(arrays),))],
         compiler_params=pltpu.CompilerParams(vmem_limit_bytes=room),
         cost_estimate=cost(1 << 30),
-        name="fetch",
     )(*arrays)
 
 
@@ -147,7 +145,6 @@
         scratch_shapes=[pltpu.VMEM((heads, rows + rows // 2, 2 * HEAD), jnp.bfloat16)],
         compiler_params=pltpu.CompilerParams(vmem_limit_bytes=24 << 20),
         cost_estimate=cost(2 * count * rows * depth * width),
-        name="project_far",
     )(scal, acc, *xs, *weights)
 
 
@@ -228,65 +225,98 @@
         ],
         compiler_params=pltpu.CompilerParams(vmem_limit_bytes=16 << 20),
         cost_estimate=cost(40 * q_width * rows * 384),
-        name="window",
     )(scal, sink_logit, q_t, low, kv, high)
 
 
-def diff_kernel(chunks, rows, parts, count, scal_ref, lam_ref, gain_ref, *refs):
-    heads = count // parts
-    kv_refs = refs[: chunks * parts]
-    q_refs = refs[chunks * parts : chunks * (parts + heads)]
-    out_refs = refs[chunks * (parts + heads) : chunks * (parts + heads) + heads]
-    out_ref, keys, values_t, queries, weighted, running = refs[-6:]
+def diff_kernel(chunks, rows, heads, parts, others, offset, scal_ref, *refs):
+    first_call = offset is None
+    kv_refs = refs[: chunks * len(others)]
+    refs = refs[chunks * len(others) :]
+    size = rows // chunks
     here, live = scal_ref[0], scal_ref[1]
-    size = rows // chunks
-    total = rows * count
+    mine, part = here // parts, here % parts
+    if first_call:
+        q_refs, refs = refs[: chunks * heads], refs[chunks * heads :]
+        queries, weighted, running, flags, keys, values_t = refs
+    else:
+        queries, weighted_in, running_in, flags, lam_ref, gain_ref = refs[:6]
+        out_refs = refs[6 : 6 + heads]
+        weighted, running, out_ref, keys, values_t = refs[6 + heads :]
+        base = ((scal_ref[2] // 2) ^ offset) * heads
     step = 512
     pair = 2 * size
+    total = keys.shape[0]
+
+    live_keys = jnp.int32(0)
+    for e in others:
+        for h in range(heads):
+            live_keys += jnp.clip(live - (h * parts + (part ^ e)) * rows, 0, rows)
 
     top_key = jnp.zeros((1, 2 * HEAD), jnp.float32)
-    queries[...] = jnp.zeros_like(queries)
-    for c in range(chunks):
-        for d in range(count):
-            at = pl.multiple_of((here ^ d) * rows + c * size, size)
-            block = kv_refs[c * parts + d % parts][d // parts]
-            keys[pl.ds(at, size), :] = block
-            wide = block.astype(jnp.float32)
-            top_key = jnp.maximum(top_key, jnp.max(jnp.abs(wide), axis=0, keepdims=True))
-            alive = (at + lax.broadcasted_iota(jnp.int32, (1, size), 1)) < live
-            turned = jnp.where(alive, jnp.transpose(wide)[HEAD:], 0.0)
-            values_t[0:HEAD, pl.ds(at, size)] = turned.astype(jnp.bfloat16)
-            if d % parts == 0:
-                half = size // 2
-                pairs = q_refs[c * heads + d // parts][size : size + half, :]
+    for n, e in enumerate(others):
+        for c in range(chunks):
+            for d in range(heads):
+                owner, source = mine ^ d, part ^ e
+                place = owner * len(others)
+                if not first_call:
+                    place += source - (source > part).astype(jnp.int32)
+                at = pl.multiple_of(place * rows + c * size, size)
+                block = kv_refs[c * len(others) + n][d]
+                keys[pl.ds(at, size), :] = block
+                wide = block.astype(jnp.float32)
+                top_key = jnp.maximum(top_key, jnp.max(jnp.abs(wide), axis=0, keepdims=True))
+                alive = (at + lax.broadcasted_iota(jnp.int32, (1, size), 1)) < live_keys
+                turned = jnp.where(alive, jnp.transpose(wide)[HEAD:], 0.0)
+                values_t[0:HEAD, pl.ds(at, size)] = turned.astype(jnp.bfloat16)
+    counted = lax.broadcasted_iota(jnp.int32, (16, total), 0) == 0
+    counted &= lax.broadcasted_iota(jnp.int32, (16, total), 1) < live_keys
+    values_t[HEAD : HEAD + 16, :] = counted.astype(jnp.bfloat16)
+    limit = jnp.transpose(jnp.broadcast_to(top_key, (8, 2 * HEAD)))[:, 0:1]
+    if first_call:
+        queries[...] = jnp.zeros_like(queries)
+        for c in range(chunks):
+            for d in range(heads):
+                pairs = q_refs[c * heads + d][size : size + size // 2, :]
                 turned = jnp.transpose(pairs.astype(jnp.float32))
                 turned = jnp.concatenate([turned[0:HEAD], turned[HEAD:]], axis=1)
                 turned = turned.astype(jnp.bfloat16)
-                tile = c * heads + d // parts
+                tile = c * heads + d
                 queries[tile, 0:DQK, 0:size] = turned[0:DQK]
                 queries[tile, DQK : 2 * DQK, size:pair] = turned[DQK:]
-    counted = lax.broadcasted_iota(jnp.int32, (16, total), 0) == 0
-    counted &= lax.broadcasted_iota(jnp.int32, (16, total), 1) < live
-    values_t[HEAD : HEAD + 16, :] = counted.astype(jnp.bfloat16)
-    limit = jnp.transpose(jnp.broadcast_to(top_key, (8, 2 * HEAD)))[:, 0:1]
-    gain = jnp.transpose(jnp.broadcast_to(gain_ref[...], (8, HEAD)))[:, 0:1]
-
-    full = live // step
-    left = live - full * step
-
-    def tile_body(tile, carry):
-        c, zd = tile // heads, tile % heads
-        first = (here ^ (zd * parts)) * rows + c * size
-
-        @pl.when(first >= live)
-        def _():
-            out_ref[tile] = jnp.zeros(out_ref.shape[1:], out_ref.dtype)
+    else:
+        gain = jnp.transpose(jnp.broadcast_to(gain_ref[...], (8, HEAD)))[:, 0:1]
+
+    units = (live_keys + step - 1) // step
+
+    def tile_body(index, carry):
+        tile = index if first_call else base + index
+        c, d = tile // heads, tile % heads
+        first = (here ^ (d * parts)) * rows + c * size
+        slot = tile if first_call else 0
+
+        if first_call:
+            flags[tile] = jnp.int32(0)
+        else:
+
+            @pl.when(first >= live)
+            def _():
+                out_ref[index] = jnp.zeros(out_ref.shape[1:], out_ref.dtype)
 
         @pl.when(first < live)
         def _():
             q = queries[tile]
             bound = jnp.max(jnp.sum(jnp.abs(q.astype(jnp.float32)) * limit, axis=0, keepdims=True))
             safe = bound < SAFE_BOUND
+            if first_call:
+                flags[tile] = safe.astype(jnp.int32)
+                weighted[slot] = jnp.zeros(weighted.shape[1:], jnp.float32)
+                running[slot] = jnp.where(
+                    safe, jnp.zeros((1, pair), jnp.float32), masked_score
+                )
+            else:
+                safe &= flags[tile] == 1
+                weighted[slot] = weighted_in[tile]
+                running[slot] = running_in[tile]
 
             def scores(j):
                 at = pl.multiple_of(j * step, step)
@@ -294,11 +324,6 @@
 
             def values(j):
                 return values_t[:, pl.ds(pl.multiple_of(j * step, step), step)]
-
-            def inside(shape):
-                return lax.broadcasted_iota(jnp.int32, shape, 0) < left
-
-            weighted[...] = jnp.zeros_like(weighted)
 
             @pl.when(safe)
             def _():
@@ -308,87 +333,105 @@
                         jnp.dot(values(j + i), e, preferred_element_type=jnp.float32)
                         for i, e in enumerate(raised)
                     ]
-                    weighted[...] += functools.reduce(lambda a, b: a + b, added)
+                    weighted[slot] += functools.reduce(lambda a, b: a + b, added)
 
                 def one(j, carry):
                     several(4 * j, 4)
                     return carry
 
-                pairs = (live + 2 * step - 1) // (2 * step)
-                lax.fori_loop(0, pairs // 2, one, 0)
-
-                @pl.when(pairs % 2 == 1)
-                def _():
-                    several(2 * (pairs - 1), 2)
+                lax.fori_loop(0, units // 4, one, 0)
+                for number in (1, 2, 3):
+
+                    @pl.when(units % 4 == number)
+                    def _():
+                        several(units - number, number)
 
             @pl.when(jnp.logical_not(safe))
             def _():
-                running[...] = jnp.full_like(running, masked_score)
-
-                def add(j, s):
-                    old = running[...]
+                def one(j, carry):
+                    s = scores(j)
+                    inside = lax.broadcasted_iota(jnp.int32, s.shape, 0) < live_keys - j * step
+                    s = jnp.where(inside, s, masked_score)
+                    old = running[slot]
                     new = jnp.maximum(old, jnp.max(s, axis=0, keepdims=True))
                     e = jnp.exp2(s - new).astype(jnp.bfloat16)
-                    weighted[...] = weighted[...] * jnp.exp2(old - new) + jnp.dot(
+                    weighted[slot] = weighted[slot] * jnp.exp2(old - new) + jnp.dot(
                         values(j), e, preferred_element_type=jnp.float32
                     )
-                    running[...] = new
-
-                def one(j, carry):
-                    add(j, scores(j))
+                    running[slot] = new
                     return carry
 
-                lax.fori_loop(0, full, one, 0)
-
-                @pl.when(left > 0)
-                def _():
-                    s = scores(full)
-                    add(full, jnp.where(inside(s.shape), s, masked_score))
-
-            maps = weighted[0:HEAD, :] / weighted[HEAD : HEAD + 1, :]
-            mix = maps[:, 0:size] - lam_ref[here // parts] * maps[:, size:pair]
-            normed = mix * lax.rsqrt(jnp.mean(mix * mix, axis=0, keepdims=True) + epsilon)
-            normed = normed * gain
-            position = first + lax.broadcasted_iota(jnp.int32, (1, size), 1)
-            out_ref[tile] = jnp.where(position < live, normed, 0.0).astype(jnp.bfloat16)
+                lax.fori_loop(0, units, one, 0)
+
+            if not first_call:
+                maps = weighted[slot, 0:HEAD, :] / weighted[slot, HEAD : HEAD + 1, :]
+                mix = maps[:, 0:size] - lam_ref[mine] * maps[:, size:pair]
+                normed = mix * lax.rsqrt(jnp.mean(mix * mix, axis=0, keepdims=True) + epsilon)
+                normed = normed * gain
+                position = first + lax.broadcasted_iota(jnp.int32, (1, size), 1)
+                out_ref[index] = jnp.where(position < live, normed, 0.0).astype(jnp.bfloat16)
 
         return carry
 
-    lax.fori_loop(0, chunks * heads, tile_body, 0)
-    for c in range(chunks):
+    lax.fori_loop(0, chunks * heads if first_call else heads, tile_body, 0)
+    if not first_call:
         for d in range(heads):
-            out_refs[d][c] = out_ref[c * heads + d]
-
-
-def diff_part(scal, mix_lambda, gain, kvs, qs, chunks, rows, parts):
+            out_refs[d][...] = out_ref[d]
+
+
+def diff_first(scal, kvs, qs, rows, parts):
+    chunks = len(kvs)
     heads = len(qs) // chunks
-    count = heads * parts
     size = rows // chunks
-    blocks = (*kvs, *qs)
+    tiles = chunks * heads
+    keys = rows * heads
     return pl.pallas_call(
-        functools.partial(diff_kernel, chunks, rows, parts, count),
-        in_specs=[smem()] * 2 + [vmem()] * (1 + len(blocks)),
+        functools.partial(diff_kernel, chunks, rows, heads, parts, [0], None),
+        in_specs=[smem()] + [vmem()] * (len(kvs) + len(qs)),
+        out_specs=[vmem()] * 3 + [smem()],
+        out_shape=[
+            pltpu.VMEM((tiles, 2 * HEAD, 2 * size), jnp.bfloat16),
+            pltpu.VMEM((tiles, HEAD + 16, 2 * size), jnp.float32),
+            pltpu.VMEM((tiles, 1, 2 * size), jnp.float32),
+            jax.ShapeDtypeStruct((tiles,), jnp.int32),
+        ],
+        scratch_shapes=[
+            pltpu.VMEM((keys, 2 * HEAD), jnp.bfloat16),
+            pltpu.VMEM((HEAD + 16, keys), jnp.bfloat16),
+        ],
+        compiler_params=pltpu.CompilerParams(vmem_limit_bytes=24 << 20),
+        cost_estimate=cost(500 * heads * rows * keys),
+    )(scal, *kvs, *qs)
+
+
+def diff_last(scal, kvs, state, mix_lambda, gain, rows, parts, chunks, offset):
+    tiles = state[0].shape[0]
+    heads = tiles // chunks
+    size = rows // chunks
+    others = list(range(1, parts))
+    keys = rows * heads * len(others)
+    return pl.pallas_call(
+        functools.partial(diff_kernel, chunks, rows, heads, parts, others, offset),
+        in_specs=[smem()] + [vmem()] * (len(kvs) + 3) + [smem()] * 2 + [vmem()],
         out_specs=[vmem()] * heads,
-        out_shape=[jax.ShapeDtypeStruct((chunks, HEAD, size), jnp.bfloat16)] * heads,
+        out_shape=[jax.ShapeDtypeStruct((HEAD, size), jnp.bfloat16)] * heads,
         scratch_shapes=[
-            pltpu.VMEM((chunks * heads, HEAD, size), jnp.bfloat16),
-            pltpu.VMEM((rows * count, 2 * HEAD), jnp.bfloat16),
-            pltpu.VMEM((HEAD + 16, rows * count), jnp.bfloat16),
-            pltpu.VMEM((chunks * heads, 2 * HEAD, 2 * size), jnp.bfloat16),
-            pltpu.VMEM((HEAD + 16, 2 * size), jnp.float32),
-            pltpu.VMEM((1, 2 * size), jnp.float32),
+            pltpu.VMEM((1, HEAD + 16, 2 * size), jnp.float32),
+            pltpu.VMEM((1, 1, 2 * size), jnp.float32),
+            pltpu.VMEM((heads, HEAD, size), jnp.bfloat16),
+            pltpu.VMEM((keys, 2 * HEAD), jnp.bfloat16),
+            pltpu.VMEM((HEAD + 16, keys), jnp.bfloat16),
         ],
-        compiler_params=pltpu.CompilerParams(vmem_limit_bytes=32 << 20),
-        cost_estimate=cost(1000 * heads * rows * rows * count),
-        name="differential",
-    )(scal, mix_lambda, gain, *blocks)
+        compiler_params=pltpu.CompilerParams(vmem_limit_bytes=24 << 20),
+        cost_estimate=cost(500 * heads * rows * keys),
+    )(scal, *kvs, *state, mix_lambda, gain)
 
 
 def out_kernel(heads, parts, offset, begin, scal_ref, win_ref, *refs):
     diff_refs = refs[:heads]
     win_w_ref, diff_w_ref, keep_ref, send_ref, stacked = refs[heads:]
     here, me = scal_ref[0] // parts, scal_ref[2]
-    chip, core = (me // 2) ^ offset, me % 2
+    core = me % 2
     half = stacked.shape[1]
     win_width = win_ref.shape[1]
 
@@ -399,9 +442,9 @@
             stacked[bit, :, 0:win_width] = win_ref[pl.ds(at, half), :]
         pieces = []
         for h in range(heads):
-            piece = diff_refs[0][chip]
+            piece = diff_refs[0][...]
             for d in range(1, heads):
-                piece = jnp.where((here ^ d) == h, diff_refs[d][chip], piece)
+                piece = jnp.where((here ^ d) == h, diff_refs[d][...], piece)
             pieces.append(piece)
         turned = jnp.transpose(jnp.concatenate(pieces, axis=0).astype(jnp.float32))
         turned = turned.astype(jnp.bfloat16)
@@ -421,7 +464,7 @@
 def out_part(scal, offset, win_rows, diffs, win_out, diff_out, begin, width, block, parts):
     heads = len(diffs)
     depth = win_out.shape[0] + diff_out.shape[0]
-    size = diffs[0].shape[2]
+    size = diffs[0].shape[1]
     half = size // 2
 
     return pl.pallas_call(
@@ -435,7 +478,6 @@
             dimension_semantics=("arbitrary",), vmem_limit_bytes=16 << 20
         ),
         cost_estimate=cost(2 * size * depth * width),
-        name="project_out",
     )(scal, win_rows, *diffs, win_out, diff_out)
 
 
@@ -468,14 +510,14 @@
 
     pieces = []
     for c in range(chips):
-        pieces += fetch((inputs,), c * size, size)
+        pieces += fetch((inputs,), c * size, size, room=60 << 20)
     far = [
         [lax.ppermute(pieces[c], "tp", flip("tp", 2 * o)) for o in range(1, chips)]
         for c in range(chips)
     ]
     sib = lax.ppermute(inputs, "tp", flip("tp", 1))
     acc = project_near(inputs, sib, weights, scal)
-    q_parts, kv_parts, kvs, qs = [], [], [], []
+    q_parts, kv_parts, own_kvs, other_kvs, qs = [], [], [], [], []
     for c in range(chips):
         xs = []
         for piece in far[c]:
@@ -487,7 +529,8 @@
         for d in range(1, heads):
             moved.append(lax.ppermute(slots[d], "sp", flip("sp", d * parts)))
         mine = jnp.stack([m[:size] for m in moved])
-        kvs += [mine] + [lax.ppermute(mine, "sp", flip("sp", e)) for e in range(1, parts)]
+        own_kvs.append(mine)
+        other_kvs += [lax.ppermute(mine, "sp", flip("sp", e)) for e in range(1, parts)]
         qs += moved
 
     up = [(i, i + 1) for i in range(sp - 1)]
@@ -503,17 +546,27 @@
     win_rows = jnp.concatenate(win_rows)
 
     gain = head_gain.reshape(1, HEAD)
-    mixed = diff_part(scal, mix_lambda, gain, kvs, qs, chips, rows, parts)
-    diffs = [mixed[0]]
-    for d in range(1, heads):
-        diffs.append(lax.ppermute(mixed[d], "sp", flip("sp", d * parts)))
+    state = diff_first(scal, own_kvs, qs, rows, parts)
+
+    def attend(o):
+        return diff_last(
+            scal, other_kvs, state, mix_lambda, gain, rows, parts, chips, o
+        )
+
+    def give_back(mixed):
+        return [mixed[0]] + [
+            lax.ppermute(mixed[d], "sp", flip("sp", d * parts)) for d in range(1, heads)
+        ]
+
+    mixed = [attend(o) for o in range(chips)]
+    diffs = [give_back(mixed[o]) for o in range(chips)]
 
     width = win_out.shape[1]
     block = width // 4
 
     def project(o, begin, end):
         return out_part(
-            scal, o, win_rows, diffs, *out_weights, begin, end - begin, block, parts
+            scal, o, win_rows, diffs[o], *out_weights, begin, end - begin, block, parts
         )
 
     def add(*values):
@@ -533,14 +586,19 @@
                 piece = pair[:, i * span : (i + 1) * span]
                 crossed[i].append(lax.ppermute(piece, "tp", flip("tp", 2 * o)))
         arrived += crossed
-    keep, away = project(0, 0, width)
-    other = lax.ppermute(away, "tp", flip("tp", 1))
-    outs, begin = [], 0
-    for crossed in arrived:
-        end = begin + crossed[0].shape[1]
-        outs.append(add(keep[:, begin:end], other[:, begin:end], *crossed).astype(jnp.bfloat16))
-        begin = end
-    return jnp.concatenate(outs, axis=1)
+    outs = []
+    for half in range(2):
+        begin = half * (width // 2)
+        keep, away = project(0, begin, begin + width // 2)
+        other = lax.ppermute(away, "tp", flip("tp", 1))
+        for i in range(2):
+            lanes = slice(i * block, (i + 1) * block)
+            crossed = arrived[2 * half + i]
+            outs.append(add(keep[:, lanes], other[:, lanes], *crossed).astype(jnp.bfloat16))
+    last = block
+    early = jnp.concatenate(outs[:-1] + [keep[:, width // 2 - last :]], axis=1)
+    early = lax.optimization_barrier(early)
+    return lax.dynamic_update_slice(early, outs[-1], (0, width - last))
 
 
 def solution(mesh):

time: 164 us -> 172 us (1.049)
  Pallas kernels: 73.6 us -> 80.8 us
  waiting for transfers between devices: 49.7 us -> 43.4 us
  starting transfers between devices: 34.3 us -> 38.8 us
  local copies, waits for them, and re-layouts: 2.7 us -> 4.95 us
    pallas_call x1 -> x3, Pallas kernels: 41.9 us -> 46.7 us  [the longest x2 23.7 us: diff_last(): pl.pallas_call(functools.partial(diff_kernel, chunks, rows, heads, parts,...]
    ppermute x3 -> x6, starting transfers between devices: 4.45 us -> 8.89 us  [give_back(): lax.ppermute(mixed[d], 'sp', flip('sp', d * parts))]
    ppermute x6, waiting for transfers between devices: 9.67 us -> 5.88 us  [body(): moved.append(lax.ppermute(slots[d], 'sp', flip('sp', d * parts)))]
    ppermute x2, waiting for transfers between devices: 15 us -> 11.6 us  [body(): lax.ppermute(pieces[c], 'tp', flip('tp', 2 * o))]
    ppermute x3 -> x6, waiting for transfers between devices: 4.34 us -> 7.55 us  [give_back(): lax.ppermute(mixed[d], 'sp', flip('sp', d * parts))]
    ppermute x4, waiting for transfers between devices: 20.7 us -> 18.3 us  [body(): crossed[i].append(lax.ppermute(piece, 'tp', flip('tp', 2 * o)))]
    unnamed x20 -> x16, local copies, waits for them, and re-layouts: 2.61 us -> 4.84 us
    pallas_call x4, Pallas kernels: 5.76 us -> 7.76 us  [fetch(): pl.pallas_call(functools.partial(copy_kernel, begin), in_specs=[pl.BlockS...]
  transfers between devices with their start and end apart: 26 -> 30, of which waited for: 12 -> 13; matrix products, arithmetic and copies ran while one was open for 0% -> 1% of each run, Pallas kernels for 19% -> 39%
where the time goes in v2:
time: 172 us
  Pallas kernels  80.8 us (47%)
  waiting for transfers between devices  43.4 us (25%)
  starting transfers between devices  38.8 us (23%)
  local copies, waits for them, and re-layouts  4.95 us (3%)
  other arithmetic  2.71 us (2%)
    pallas_call x2, Pallas kernels, diff_last(): pl.pallas_call(functools.partial(diff_kernel, chunks, rows, heads, parts,...  23.7 us
    pallas_call x1, Pallas kernels, diff_first(): pl.pallas_call(functools.partial(diff_kernel, chunks, rows, heads, parts,...  23 us
    ppermute x4, waiting for transfers between devices, body(): crossed[i].append(lax.ppermute(piece, 'tp', flip('tp', 2 * o)))  18.3 us
    ppermute x2, waiting for transfers between devices, body(): lax.ppermute(pieces[c], 'tp', flip('tp', 2 * o))  11.6 us
    ppermute x6, starting transfers between devices, body(): moved.append(lax.ppermute(slots[d], 'sp', flip('sp', d * parts)))  9.52 us
    ppermute x6, starting transfers between devices, give_back(): lax.ppermute(mixed[d], 'sp', flip('sp', d * parts))  8.89 us
    pallas_call x5, Pallas kernels, out_part(): pl.pallas_call(functools.partial(out_kernel, heads, parts, offset, begin)...  8.12 us
    pallas_call x4, Pallas kernels, fetch(): pl.pallas_call(functools.partial(copy_kernel, begin), in_specs=[pl.BlockS...  7.76 us
  transfers between devices with their start and end apart: 30, of which 13 were waited for; matrix products, arithmetic and copies ran while one was open for 1% of the time, Pallas kernels for 39%

profile of v2, /device:TPU:0, one launch (start us, length us, event | category | flops | bytes accessed | tf_op | source)
XLA Modules:
  0.0 171.7 jit_solution(13004174474248964311)
XLA Ops:
  0.5 1.0 shard_map.129
  1.6 2.5 %collective-permute-start.1 = (bf16[256,1024]{1,0:T(8,128)(2,1)S(1)}, bf16[256,1024]{1,0:T(8,128)(2,1)}, u32[]{:S(2)}, u32[]{:S(2)}) collective-permute-start(bf16[256,1024]{1,0:T(8,128)(2,1)S(1)} %shard_map.129), channel_id=1, source_target_pairs={{0,2},{1,3},{2,0},{3,1},{4,6},{5,7},{6,4},{7,5},{8,10},{9,11},{10,... | collective-permute-start | bytes 1572872 | tf_op jit(solution)/shard_map/ppermute | solution.py:515
  4.1 1.8 %shard_map.131 = bf16[256,1024]{1,0:T(8,128)(2,1)} custom-call(bf16[512,1024]{1,0:T(8,128)(2,1)} %refs_0_.6), custom_call_target="tpu_custom_call" | custom-call | flops 1073741824 | tf_op jit(solution)/shard_map/pallas_call | solution.py:86
  6.0 10.9 %collective-permute-done.1.refs_0_ = bf16[256,1024]{1,0:T(8,128)(2,1)} collective-permute-done((bf16[256,1024]{1,0:T(8,128)(2,1)S(1)}, bf16[256,1024]{1,0:T(8,128)(2,1)}, u32[]{:S(2)}, u32[]{:S(2)}) %collective-permute-start.1) | collective-permute-done | bytes 524320 | tf_op jit(solution)/shard_map/ppermute | solution.py:515
  17.0 1.9 %copy-done.2 = bf16[384,4096]{1,0:T(8,128)(2,1)S(1)} copy-done((bf16[384,4096]{1,0:T(8,128)(2,1)S(1)}, bf16[384,4096]{1,0:T(8,128)(2,1)}, u32[]{:S(2)}) %copy-start.2) | copy-done | bytes 3145752
  18.9 1.6 copy-done.3
  20.9 1.3 copy-done
  22.8 4.5 %shard_map.127 = (bf16[4096,384]{1,0:T(8,128)(2,1)S(1)}, bf16[4096,128]{1,0:T(8,128)(2,1)S(1)}, bf16[4096,128]{1,0:T(8,128)(2,1)S(1)}, bf16[4096,256]{1,0:T(8,12...) custom-call(bf16[4096,384]{1,0:T(8,128)(2,1)} %refs_0_.4, bf16[4096,128]{1,0:T(8,128)(2,1)} %refs_1_.2, ...), custom_call_target="tpu_custom_call" | custom-call | flops 1073741824 | tf_op jit(solution)/shard_map/pallas_call | solution.py:86
  27.4 0.7 collective-permute-done.3.refs_0_
  28.1 4.6 %shard_map.128.acc_ref = f32[512,1408]{1,0:T(8,128)S(1)} custom-call(s32[3]{0:T(128)S(1)} %pad_add_fusion.scal_ref, bf16[512,1024]{1,0:T(8,128)(2,1)S(1)} %copy-done.4, bf16[512,1024]{1,0:T(8,128)(2,1)} %collective-permute-done.sib_ref, bf16[4096,384]{1,0:T(8,128)(2,1)S(1)} %get-tuple-element.47.refs_0_.refs_2_, ...), custom_call_target="tpu_custom_call" | custom-call | flops 2952790016 | tf_op jit(solution)/shard_map/pallas_call | solution.py:59
  32.8 3.1 %shard_map.130 = (bf16[384,256]{1,0:T(8,128)(2,1)S(1)}, bf16[256,256]{1,0:T(8,128)(2,1)S(1)}, bf16[384,128]{1,0:T(8,128)(2,1)S(1)}, bf16[384,128]{1,0:T(8,128)(2...) custom-call(s32[3]{0:T(128)S(1)} %pad_add_fusion.scal_ref, f32[512,1408]{1,0:T(8,128)S(1)} %shard_map.128.acc_ref, ...), custom_call_target="tpu_custom_call" | custom-call | flops 1476395008 | tf_op jit(solution)/shard_map/pallas_call | solution.py:140
  35.9 1.3 collective-permute-start.6
  37.2 3.0 %shard_map.132 = (bf16[384,256]{1,0:T(8,128)(2,1)S(1)}, bf16[256,256]{1,0:T(8,128)(2,1)S(1)}, bf16[384,128]{1,0:T(8,128)(2,1)S(1)}, bf16[384,128]{1,0:T(8,128)(2...) custom-call(s32[3]{0:T(128)S(1)} %pad_add_fusion.scal_ref, f32[512,1408]{1,0:T(8,128)S(1)} %shard_map.128.acc_ref, ...), custom_call_target="tpu_custom_call" | custom-call | flops 1476395008 | tf_op jit(solution)/shard_map/pallas_call | solution.py:140
  40.2 4.6 %collective-permute-start.5 = (bf16[128,256]{1,0:T(8,128)(2,1)S(1)}, bf16[128,256]{1,0:T(8,128)(2,1)S(1)}, u32[]{:S(2)}, u32[]{:S(2)}) collective-permute-start(bf16[128,256]{1,0:T(8,128)(2,1)S(1)} %slice.61), channel_id=1, source_target_pairs={{0,4},{4,8},{8,12},{12,16},{16,20},{20,24},{24,28},{1,5},{5,9},{9,... | collective-permute-start | bytes 196616 | tf_op jit(solution)/shard_map/ppermute | solution.py:538
  44.8 4.1 %collective-permute-start.9 = (bf16[384,128]{1,0:T(8,128)(2,1)S(1)}, bf16[384,128]{1,0:T(8,128)(2,1)S(1)}, u32[]{:S(2)}, u32[]{:S(2)}) collective-permute-start(bf16[384,128]{1,0:T(8,128)(2,1)S(1)} %get-tuple-element.60), channel_id=1, source_target_pairs={{0,24},{4,28},{8,16},{12,20},{16,8},{20,12},{24,0},{28,4},{1,25},{... | collective-permute-start | bytes 294920 | tf_op jit(solution)/shard_map/ppermute | solution.py:530
  49.5 3.8 %collective-permute-start.13 = (bf16[384,128]{1,0:T(8,128)(2,1)S(1)}, bf16[384,128]{1,0:T(8,128)(2,1)S(1)}, u32[]{:S(2)}, u32[]{:S(2)}) collective-permute-start(bf16[384,128]{1,0:T(8,128)(2,1)S(1)} %get-tuple-element.64), channel_id=1, source_target_pairs={{0,24},{4,28},{8,16},{12,20},{16,8},{20,12},{24,0},{28,4},{1,25},{... | collective-permute-start | bytes 294920 | tf_op jit(solution)/shard_map/ppermute | solution.py:530
  53.3 3.8 %shard_map.134 = bf16[256,384]{1,0:T(8,128)(2,1)S(1)} custom-call(s32[3]{0:T(128)S(1)} %pad_add_fusion.scal_ref, f32[6]{0:T(128)S(1)} %copy-done.5, bf16[384,256]{1,0:T(8,128)(2,1)S(1)} %get-tuple-element.56.refs_0_, bf16[256,256]{1,0:T(8,128)(2,1)S(1)} %get-tuple-element.55.refs_2_.refs_1_, bf16[256,256]{1,0:T(8,128)(2,1)S(1)} %get-tuple-element.54.refs_3_.refs_2_, ...), custom_call_target="tpu_custom_call" | custom-call | flops 1509949440 | tf_op jit(solution)/shard_map/pallas_call | solution.py:216
  57.1 1.0 collective-permute-start.12
  58.1 3.0 %collective-permute-done.8.refs_4_ = bf16[384,128]{1,0:T(8,128)(2,1)S(1)} collective-permute-done((bf16[384,128]{1,0:T(8,128)(2,1)S(1)}, bf16[384,128]{1,0:T(8,128)(2,1)S(1)}, u32[]{:S(2)}, u32[]{:S(2)}) %collective-permute-start.8) | collective-permute-done | bytes 98336 | tf_op jit(solution)/shard_map/ppermute | solution.py:530
  61.2 2.4 %collective-permute-start.10 = (bf16[4,256,128]{2,1,0:T(8,128)(2,1)S(1)}, bf16[4,256,128]{2,1,0:T(8,128)(2,1)S(1)}, u32[]{:S(2)}, u32[]{:S(2)}) collective-permute-start(bf16[4,256,128]{2,1,0:T(8,128)(2,1)S(1)} %pad_maximum_fusion.2.refs_0_), channel_id=1, source_target_pairs={{0,4},{4,0},{8,12},{12,8},{16,20},{20,16},{24,28},{28,24},{1,5},{5... | collective-permute-start | bytes 786440 | tf_op jit(solution)/shard_map/ppermute | solution.py:533
  63.7 1.9 %collective-permute-done.12.refs_8_ = bf16[384,128]{1,0:T(8,128)(2,1)S(1)} collective-permute-done((bf16[384,128]{1,0:T(8,128)(2,1)S(1)}, bf16[384,128]{1,0:T(8,128)(2,1)S(1)}, u32[]{:S(2)}, u32[]{:S(2)}) %collective-permute-start.12) | collective-permute-done | bytes 98336 | tf_op jit(solution)/shard_map/ppermute | solution.py:530
  65.6 1.0 collective-permute-done.11.refs_7_
  66.6 2.5 %collective-permute-start.14 = (bf16[4,256,128]{2,1,0:T(8,128)(2,1)S(1)}, bf16[4,256,128]{2,1,0:T(8,128)(2,1)S(1)}, u32[]{:S(2)}, u32[]{:S(2)}) collective-permute-start(bf16[4,256,128]{2,1,0:T(8,128)(2,1)S(1)} %pad_maximum_fusion.3.refs_1_), channel_id=1, source_target_pairs={{0,4},{4,0},{8,12},{12,8},{16,20},{20,16},{24,28},{28,24},{1,5},{5... | collective-permute-start | bytes 786440 | tf_op jit(solution)/shard_map/ppermute | solution.py:533
  69.1 3.8 %shard_map.133 = bf16[256,384]{1,0:T(8,128)(2,1)S(1)} custom-call(s32[3]{0:T(128)S(1)} %pad_add_fusion.scal_ref, f32[6]{0:T(128)S(1)} %copy-done.5, bf16[384,256]{1,0:T(8,128)(2,1)S(1)} %get-tuple-element.53.refs_0_, bf16[128,256]{1,0:T(8,128)(2,1)S(1)} %collective-permute-done.5.refs_1_, bf16[256,256]{1,0:T(8,128)(2,1)S(1)} %get-tuple-element.55.refs_2_.refs_1_, ...), custom_call_target="tpu_custom_call" | custom-call | flops 1509949440 | tf_op jit(solution)/shard_map/pallas_call | solution.py:216
  72.9 23.0 %shard_map.135 = (bf16[8,128,512]{2,1,0:T(8,128)(2,1)S(1)}, f32[8,80,512]{2,1,0:T(8,128)S(1)}, f32[8,1,512]{2,1,0:T(1,128)S(1)}, s32[8]{0:T(128)S(1)}) custom-call(s32[3]{0:T(128)S(1)} %pad_add_fusion.scal_ref, bf16[4,256,128]{2,1,0:T(8,128)(2,1)S(1)} %pad_maximum_fusion.2.refs_0_, bf16[4,256,128]{2,1,0:T(8,128)(2,1)S(1)} %pad_maximum_fusion.3.refs_1_, ...), custom_call_target="tpu_custom_call" | custom-call | flops 2097152000 | tf_op jit(solution)/shard_map/pallas_call | solution.py:388
  96.0 11.8 %shard_map.139 = (bf16[64,256]{1,0:T(8,128)(2,1)S(1)}, bf16[64,256]{1,0:T(8,128)(2,1)S(1)}, bf16[64,256]{1,0:T(8,128)(2,1)S(1)}, bf16[64,256]{1,0:T(8,128)(2,1)S(1)}) custom-call(s32[3]{0:T(128)S(1)} %pad_add_fusion.scal_ref, bf16[4,256,128]{2,1,0:T(8,128)(2,1)S(1)} %collective-permute-done.10.refs_0_, ...), custom_call_target="tpu_custom_call" | custom-call | flops 2097152000 | tf_op jit(solution)/shard_map/pallas_call | solution.py:413
  107.9 3.0 %collective-permute-start.20 = (bf16[64,256]{1,0:T(8,128)(2,1)S(1)}, bf16[64,256]{1,0:T(8,128)(2,1)S(1)}, u32[]{:S(2)}, u32[]{:S(2)}) collective-permute-start(bf16[64,256]{1,0:T(8,128)(2,1)S(1)} %get-tuple-element.79), channel_id=1, source_target_pairs={{0,16},{4,20},{8,24},{12,28},{16,0},{20,4},{24,8},{28,12},{1,17},{... | collective-permute-start | bytes 98312 | tf_op jit(solution)/shard_map/ppermute | solution.py:558
  110.9 1.3 collective-permute-start.21
  112.8 3.8 %collective-permute-done.21.refs_3_ = bf16[64,256]{1,0:T(8,128)(2,1)S(1)} collective-permute-done((bf16[64,256]{1,0:T(8,128)(2,1)S(1)}, bf16[64,256]{1,0:T(8,128)(2,1)S(1)}, u32[]{:S(2)}, u32[]{:S(2)}) %collective-permute-start.21) | collective-permute-done | bytes 32800 | tf_op jit(solution)/shard_map/ppermute | solution.py:558
  116.6 1.2 shard_map.140
  117.9 11.8 %shard_map.136 = (bf16[64,256]{1,0:T(8,128)(2,1)S(1)}, bf16[64,256]{1,0:T(8,128)(2,1)S(1)}, bf16[64,256]{1,0:T(8,128)(2,1)S(1)}, bf16[64,256]{1,0:T(8,128)(2,1)S(1)}) custom-call(s32[3]{0:T(128)S(1)} %pad_add_fusion.scal_ref, bf16[4,256,128]{2,1,0:T(8,128)(2,1)S(1)} %collective-permute-done.10.refs_0_, ...), custom_call_target="tpu_custom_call" | custom-call | flops 2097152000 | tf_op jit(solution)/shard_map/pallas_call | solution.py:413
  129.8 1.9 %collective-permute-start.16 = (bf16[64,256]{1,0:T(8,128)(2,1)S(1)}, bf16[64,256]{1,0:T(8,128)(2,1)S(1)}, u32[]{:S(2)}, u32[]{:S(2)}) collective-permute-start(bf16[64,256]{1,0:T(8,128)(2,1)S(1)} %get-tuple-element.71), channel_id=1, source_target_pairs={{0,16},{4,20},{8,24},{12,28},{16,0},{20,4},{24,8},{28,12},{1,17},{... | collective-permute-start | bytes 98312 | tf_op jit(solution)/shard_map/ppermute | solution.py:558
  131.7 2.5 %collective-permute-start.17 = (bf16[64,256]{1,0:T(8,128)(2,1)S(1)}, bf16[64,256]{1,0:T(8,128)(2,1)S(1)}, u32[]{:S(2)}, u32[]{:S(2)}) collective-permute-start(bf16[64,256]{1,0:T(8,128)(2,1)S(1)} %get-tuple-element.72), channel_id=1, source_target_pairs={{0,24},{4,28},{8,16},{12,20},{16,8},{20,12},{24,0},{28,4},{1,25},{... | collective-permute-start | bytes 98312 | tf_op jit(solution)/shard_map/ppermute | solution.py:558
  134.2 0.7 collective-permute-done.16.refs_2_
  134.9 2.5 %collective-permute-done.17.refs_3_ = bf16[64,256]{1,0:T(8,128)(2,1)S(1)} collective-permute-done((bf16[64,256]{1,0:T(8,128)(2,1)S(1)}, bf16[64,256]{1,0:T(8,128)(2,1)S(1)}, u32[]{:S(2)}, u32[]{:S(2)}) %collective-permute-start.17) | collective-permute-done | bytes 32800 | tf_op jit(solution)/shard_map/ppermute | solution.py:558
  137.4 1.9 %shard_map.142 = (bf16[128,2048]{1,0:T(8,128)(2,1)S(1)}, bf16[128,2048]{1,0:T(8,128)(2,1)S(1)}) custom-call(s32[3]{0:T(128)S(1)} %pad_add_fusion.scal_ref, bf16[512,384]{1,0:T(8,128)(2,1)S(1)} %pad_maximum_fusion.1.win_ref, bf16[64,256]{1,0:T(8,128)(2,1)S(1)} %get-tuple-element.69.refs_0_, bf16[64,256]{1,0:T(8,128)(2,1)S(1)} %collective-permute-done.15.refs_1_, ...), custom_call_target="tpu_custom_call" | custom-call | flops 671088640 | tf_op jit(solution)/shard_map/pallas_call | solution.py:470
  139.3 1.9 %shard_map.143 = (bf16[128,2048]{1,0:T(8,128)(2,1)S(1)}, bf16[128,2048]{1,0:T(8,128)(2,1)S(1)}) custom-call(s32[3]{0:T(128)S(1)} %pad_add_fusion.scal_ref, bf16[512,384]{1,0:T(8,128)(2,1)S(1)} %pad_maximum_fusion.1.win_ref, bf16[64,256]{1,0:T(8,128)(2,1)S(1)} %get-tuple-element.77.refs_0_, bf16[64,256]{1,0:T(8,128)(2,1)S(1)} %collective-permute-done.19.refs_1_, ...), custom_call_target="tpu_custom_call" | custom-call | flops 671088640 | tf_op jit(solution)/shard_map/pallas_call | solution.py:470
  141.9 1.2 shard_map.141
  143.2 1.9 %shard_map.138 = (bf16[128,2048]{1,0:T(8,128)(2,1)S(1)}, bf16[128,2048]{1,0:T(8,128)(2,1)S(1)}) custom-call(s32[3]{0:T(128)S(1)} %pad_add_fusion.scal_ref, bf16[512,384]{1,0:T(8,128)(2,1)S(1)} %pad_maximum_fusion.1.win_ref, bf16[64,256]{1,0:T(8,128)(2,1)S(1)} %get-tuple-element.69.refs_0_, bf16[64,256]{1,0:T(8,128)(2,1)S(1)} %collective-permute-done.15.refs_1_, ...), custom_call_target="tpu_custom_call" | custom-call | flops 671088640 | tf_op jit(solution)/shard_map/pallas_call | solution.py:470
  145.7 1.6 collective-permute-start.23
  148.1 1.6 collective-permute-start.28
  149.6 5.3 %collective-permute-done.23 = bf16[128,1024]{1,0:T(8,128)(2,1)S(1)} collective-permute-done((bf16[128,1024]{1,0:T(8,128)(2,1)S(1)}, bf16[128,1024]{1,0:T(8,128)(2,1)S(1)}, u32[]{:S(2)}, u32[]{:S(2)}) %collective-permute-start.23) | collective-permute-done | bytes 262176 | tf_op jit(solution)/shard_map/ppermute | solution.py:587
  154.9 1.5 collective-permute-start.29
  156.4 4.1 %collective-permute-done.25 = bf16[128,1024]{1,0:T(8,128)(2,1)S(1)} collective-permute-done((bf16[128,1024]{1,0:T(8,128)(2,1)S(1)}, bf16[128,1024]{1,0:T(8,128)(2,1)S(1)}, u32[]{:S(2)}, u32[]{:S(2)}) %collective-permute-start.25) | collective-permute-done | bytes 262176 | tf_op jit(solution)/shard_map/ppermute | solution.py:587
  160.8 5.3 %collective-permute-done.28 = bf16[128,1024]{1,0:T(8,128)(2,1)S(1)} collective-permute-done((bf16[128,1024]{1,0:T(8,128)(2,1)S(1)}, bf16[128,1024]{1,0:T(8,128)(2,1)S(1)}, u32[]{:S(2)}, u32[]{:S(2)}) %collective-permute-start.28) | collective-permute-done | bytes 262176 | tf_op jit(solution)/shard_map/ppermute | solution.py:587
  166.3 1.0 pad_maximum_fusion
  167.3 3.6 %collective-permute-done.29 = bf16[128,1024]{1,0:T(8,128)(2,1)S(1)} collective-permute-done((bf16[128,1024]{1,0:T(8,128)(2,1)S(1)}, bf16[128,1024]{1,0:T(8,128)(2,1)S(1)}, u32[]{:S(2)}, u32[]{:S(2)}) %collective-permute-start.29) | collective-permute-done | bytes 262176 | tf_op jit(solution)/shard_map/ppermute | solution.py:587
  170.9 0.8 fusion
  (68 shorter events, 5.1 us)
Async XLA Ops:
  0.0 28.1 %collective-permute-start = (bf16[512,1024]{1,0:T(8,128)(2,1)}, bf16[512,1024]{1,0:T(8,128)(2,1)}, u32[]{:S(2)}, u32[]{:S(2)}) collective-permute-start(bf16[512,1024]{1,0:T(8,128)(2,1)} %refs_0_.6), channel_id=1, source_target_pairs={{0,1},{1,0},{2,3},{3,2},{4,5},{5,4},{6,7},{7,6},{8,9},{9,8},{10,11... | collective-permute-start | bytes 3145736 | tf_op jit(solution)/shard_map/ppermute | solution.py:518
  1.6 15.4 %collective-permute-start.1 = (bf16[256,1024]{1,0:T(8,128)(2,1)S(1)}, bf16[256,1024]{1,0:T(8,128)(2,1)}, u32[]{:S(2)}, u32[]{:S(2)}) collective-permute-start(bf16[256,1024]{1,0:T(8,128)(2,1)S(1)} %shard_map.129), channel_id=1, source_target_pairs={{0,2},{1,3},{2,0},{3,1},{4,6},{5,7},{6,4},{7,5},{8,10},{9,11},{10,... | collective-permute-start | bytes 1572872 | tf_op jit(solution)/shard_map/ppermute | solution.py:515
  5.9 22.1 %collective-permute-start.3 = (bf16[256,1024]{1,0:T(8,128)(2,1)}, bf16[256,1024]{1,0:T(8,128)(2,1)}, u32[]{:S(2)}, u32[]{:S(2)}) collective-permute-start(bf16[256,1024]{1,0:T(8,128)(2,1)} %shard_map.131), channel_id=1, source_target_pairs={{0,2},{1,3},{2,0},{3,1},{4,6},{5,7},{6,4},{7,5},{8,10},{9,11},{10,... | collective-permute-start | bytes 1572872 | tf_op jit(solution)/shard_map/ppermute | solution.py:515
  17.0 15.8 %collective-permute-start.2 = (bf16[256,1024]{1,0:T(8,128)(2,1)}, bf16[256,1024]{1,0:T(8,128)(2,1)}, u32[]{:S(2)}, u32[]{:S(2)}) collective-permute-start(bf16[256,1024]{1,0:T(8,128)(2,1)} %collective-permute-done.1.refs_0_), channel_id=1, source_target_pairs={{0,1},{1,0},{2,3},{3,2},{4,5},{5,4},{6,7},{7,6},{8,9},{9,8},{10,11... | collective-permute-start | bytes 1572872 | tf_op jit(solution)/shard_map/ppermute | solution.py:524
  17.0 1.9 %copy-start.2 = (bf16[384,4096]{1,0:T(8,128)(2,1)S(1)}, bf16[384,4096]{1,0:T(8,128)(2,1)}, u32[]{:S(2)}) copy-start(bf16[384,4096]{1,0:T(8,128)(2,1)} %refs_0_.7) | copy-start | bytes 9437188
  18.9 1.6 copy-start.3
  20.8 1.3 copy-start
  22.8 5.3 %copy-start.4 = (bf16[512,1024]{1,0:T(8,128)(2,1)S(1)}, bf16[512,1024]{1,0:T(8,128)(2,1)}, u32[]{:S(2)}) copy-start(bf16[512,1024]{1,0:T(8,128)(2,1)} %refs_0_.6) | copy-start | bytes 3145732
  28.0 9.2 %collective-permute-start.4 = (bf16[256,1024]{1,0:T(8,128)(2,1)}, bf16[256,1024]{1,0:T(8,128)(2,1)S(1)}, u32[]{:S(2)}, u32[]{:S(2)}) collective-permute-start(bf16[256,1024]{1,0:T(8,128)(2,1)} %collective-permute-done.3.refs_0_), channel_id=1, source_target_pairs={{0,1},{1,0},{2,3},{3,2},{4,5},{5,4},{6,7},{7,6},{8,9},{9,8},{10,11... | collective-permute-start | bytes 1572872 | tf_op jit(solution)/shard_map/ppermute | solution.py:524
  35.9 17.4 %copy-start.5 = (f32[6]{0:T(128)S(1)}, f32[6]{0:T(128)}, u32[]{:S(2)}) copy-start(f32[6]{0:T(128)} %sink_ref.3) | copy-start | bytes 76
  35.9 13.6 %collective-permute-start.6 = (bf16[128,256]{1,0:T(8,128)(2,1)S(1)}, bf16[128,256]{1,0:T(8,128)(2,1)S(1)}, u32[]{:S(2)}, u32[]{:S(2)}) collective-permute-start(bf16[128,256]{1,0:T(8,128)(2,1)S(1)} %slice.62), channel_id=1, source_target_pairs={{4,0},{8,4},{12,8},{16,12},{20,16},{24,20},{28,24},{5,1},{9,5},{13... | collective-permute-start | bytes 196616 | tf_op jit(solution)/shard_map/ppermute | solution.py:539
  40.2 28.9 %collective-permute-start.5 = (bf16[128,256]{1,0:T(8,128)(2,1)S(1)}, bf16[128,256]{1,0:T(8,128)(2,1)S(1)}, u32[]{:S(2)}, u32[]{:S(2)}) collective-permute-start(bf16[128,256]{1,0:T(8,128)(2,1)S(1)} %slice.61), channel_id=1, source_target_pairs={{0,4},{4,8},{8,12},{12,16},{16,20},{20,24},{24,28},{1,5},{5,9},{9,... | collective-permute-start | bytes 196616 | tf_op jit(solution)/shard_map/ppermute | solution.py:538
  44.8 12.4 %collective-permute-start.9 = (bf16[384,128]{1,0:T(8,128)(2,1)S(1)}, bf16[384,128]{1,0:T(8,128)(2,1)S(1)}, u32[]{:S(2)}, u32[]{:S(2)}) collective-permute-start(bf16[384,128]{1,0:T(8,128)(2,1)S(1)} %get-tuple-element.60), channel_id=1, source_target_pairs={{0,24},{4,28},{8,16},{12,20},{16,8},{20,12},{24,0},{28,4},{1,25},{... | collective-permute-start | bytes 294920 | tf_op jit(solution)/shard_map/ppermute | solution.py:530
  48.9 12.3 %collective-permute-start.8 = (bf16[384,128]{1,0:T(8,128)(2,1)S(1)}, bf16[384,128]{1,0:T(8,128)(2,1)S(1)}, u32[]{:S(2)}, u32[]{:S(2)}) collective-permute-start(bf16[384,128]{1,0:T(8,128)(2,1)S(1)} %get-tuple-element.59), channel_id=1, source_target_pairs={{0,16},{4,20},{8,24},{12,28},{16,0},{20,4},{24,8},{28,12},{1,17},{... | collective-permute-start | bytes 294920 | tf_op jit(solution)/shard_map/ppermute | solution.py:530
  48.9 12.3 %collective-permute-start.7 = (bf16[384,128]{1,0:T(8,128)(2,1)S(1)}, bf16[384,128]{1,0:T(8,128)(2,1)S(1)}, u32[]{:S(2)}, u32[]{:S(2)}) collective-permute-start(bf16[384,128]{1,0:T(8,128)(2,1)S(1)} %get-tuple-element.58), channel_id=1, source_target_pairs={{0,8},{4,12},{8,0},{12,4},{16,24},{20,28},{24,16},{28,20},{1,9},{5... | collective-permute-start | bytes 294920 | tf_op jit(solution)/shard_map/ppermute | solution.py:530
  49.5 14.2 %collective-permute-start.13 = (bf16[384,128]{1,0:T(8,128)(2,1)S(1)}, bf16[384,128]{1,0:T(8,128)(2,1)S(1)}, u32[]{:S(2)}, u32[]{:S(2)}) collective-permute-start(bf16[384,128]{1,0:T(8,128)(2,1)S(1)} %get-tuple-element.64), channel_id=1, source_target_pairs={{0,24},{4,28},{8,16},{12,20},{16,8},{20,12},{24,0},{28,4},{1,25},{... | collective-permute-start | bytes 294920 | tf_op jit(solution)/shard_map/ppermute | solution.py:530
  57.1 8.4 %collective-permute-start.12 = (bf16[384,128]{1,0:T(8,128)(2,1)S(1)}, bf16[384,128]{1,0:T(8,128)(2,1)S(1)}, u32[]{:S(2)}, u32[]{:S(2)}) collective-permute-start(bf16[384,128]{1,0:T(8,128)(2,1)S(1)} %get-tuple-element.63), channel_id=1, source_target_pairs={{0,16},{4,20},{8,24},{12,28},{16,0},{20,4},{24,8},{28,12},{1,17},{... | collective-permute-start | bytes 294920 | tf_op jit(solution)/shard_map/ppermute | solution.py:530
  61.2 5.4 %collective-permute-start.11 = (bf16[384,128]{1,0:T(8,128)(2,1)S(1)}, bf16[384,128]{1,0:T(8,128)(2,1)S(1)}, u32[]{:S(2)}, u32[]{:S(2)}) collective-permute-start(bf16[384,128]{1,0:T(8,128)(2,1)S(1)} %get-tuple-element.62), channel_id=1, source_target_pairs={{0,8},{4,12},{8,0},{12,4},{16,24},{20,28},{24,16},{28,20},{1,9},{5... | collective-permute-start | bytes 294920 | tf_op jit(solution)/shard_map/ppermute | solution.py:530
  61.2 34.7 %collective-permute-start.10 = (bf16[4,256,128]{2,1,0:T(8,128)(2,1)S(1)}, bf16[4,256,128]{2,1,0:T(8,128)(2,1)S(1)}, u32[]{:S(2)}, u32[]{:S(2)}) collective-permute-start(bf16[4,256,128]{2,1,0:T(8,128)(2,1)S(1)} %pad_maximum_fusion.2.refs_0_), channel_id=1, source_target_pairs={{0,4},{4,0},{8,12},{12,8},{16,20},{20,16},{24,28},{28,24},{1,5},{5... | collective-permute-start | bytes 786440 | tf_op jit(solution)/shard_map/ppermute | solution.py:533
  66.6 29.3 %collective-permute-start.14 = (bf16[4,256,128]{2,1,0:T(8,128)(2,1)S(1)}, bf16[4,256,128]{2,1,0:T(8,128)(2,1)S(1)}, u32[]{:S(2)}, u32[]{:S(2)}) collective-permute-start(bf16[4,256,128]{2,1,0:T(8,128)(2,1)S(1)} %pad_maximum_fusion.3.refs_1_), channel_id=1, source_target_pairs={{0,4},{4,0},{8,12},{12,8},{16,20},{20,16},{24,28},{28,24},{1,5},{5... | collective-permute-start | bytes 786440 | tf_op jit(solution)/shard_map/ppermute | solution.py:533
  72.9 23.1 %copy-start.6 = (f32[4]{0:T(128)S(1)}, f32[4]{0:T(128)}, u32[]{:S(2)}) copy-start(f32[4]{0:T(128)} %refs_6_.3) | copy-start | bytes 52
  72.9 23.1 %copy-start.7 = (f32[64]{0:T(128)S(1)}, f32[64]{0:T(128)}, u32[]{:S(2)}) copy-start(f32[64]{0:T(128)} %param.23) | copy-start | bytes 772
  95.9 20.7 %copy-start.1 = (bf16[256,4096]{1,0:T(8,128)(2,1)S(1)}, bf16[256,4096]{1,0:T(8,128)(2,1)}, u32[]{:S(2)}) copy-start(bf16[256,4096]{1,0:T(8,128)(2,1)} %copy-done) | copy-start | bytes 6291460
  107.8 4.5 %collective-permute-start.19 = (bf16[64,256]{1,0:T(8,128)(2,1)S(1)}, bf16[64,256]{1,0:T(8,128)(2,1)S(1)}, u32[]{:S(2)}, u32[]{:S(2)}) collective-permute-start(bf16[64,256]{1,0:T(8,128)(2,1)S(1)} %get-tuple-element.78), channel_id=1, source_target_pairs={{0,8},{4,12},{8,0},{12,4},{16,24},{20,28},{24,16},{28,20},{1,9},{5... | collective-permute-start | bytes 98312 | tf_op jit(solution)/shard_map/ppermute | solution.py:558
  107.9 4.9 %collective-permute-start.20 = (bf16[64,256]{1,0:T(8,128)(2,1)S(1)}, bf16[64,256]{1,0:T(8,128)(2,1)S(1)}, u32[]{:S(2)}, u32[]{:S(2)}) collective-permute-start(bf16[64,256]{1,0:T(8,128)(2,1)S(1)} %get-tuple-element.79), channel_id=1, source_target_pairs={{0,16},{4,20},{8,24},{12,28},{16,0},{20,4},{24,8},{28,12},{1,17},{... | collective-permute-start | bytes 98312 | tf_op jit(solution)/shard_map/ppermute | solution.py:558
  110.9 5.7 %collective-permute-start.21 = (bf16[64,256]{1,0:T(8,128)(2,1)S(1)}, bf16[64,256]{1,0:T(8,128)(2,1)S(1)}, u32[]{:S(2)}, u32[]{:S(2)}) collective-permute-start(bf16[64,256]{1,0:T(8,128)(2,1)S(1)} %get-tuple-element.80), channel_id=1, source_target_pairs={{0,24},{4,28},{8,16},{12,20},{16,8},{20,12},{24,0},{28,4},{1,25},{... | collective-permute-start | bytes 98312 | tf_op jit(solution)/shard_map/ppermute | solution.py:558
  117.8 27.8 %collective-permute-start.22 = (bf16[128,1024]{1,0:T(8,128)(2,1)S(1)}, bf16[128,1024]{1,0:T(8,128)(2,1)S(1)}, u32[]{:S(2)}, u32[]{:S(2)}) collective-permute-start(bf16[128,1024]{1,0:T(8,128)(2,1)S(1)} %get-tuple-element.82), channel_id=1, source_target_pairs={{0,1},{1,0},{2,3},{3,2},{4,5},{5,4},{6,7},{7,6},{8,9},{9,8},{10,11... | collective-permute-start | bytes 786440 | tf_op jit(solution)/shard_map/ppermute | solution.py:583
  129.7 4.5 %collective-permute-start.15 = (bf16[64,256]{1,0:T(8,128)(2,1)S(1)}, bf16[64,256]{1,0:T(8,128)(2,1)S(1)}, u32[]{:S(2)}, u32[]{:S(2)}) collective-permute-start(bf16[64,256]{1,0:T(8,128)(2,1)S(1)} %get-tuple-element.70), channel_id=1, source_target_pairs={{0,8},{4,12},{8,0},{12,4},{16,24},{20,28},{24,16},{28,20},{1,9},{5... | collective-permute-start | bytes 98312 | tf_op jit(solution)/shard_map/ppermute | solution.py:558
  129.8 5.1 %collective-permute-start.16 = (bf16[64,256]{1,0:T(8,128)(2,1)S(1)}, bf16[64,256]{1,0:T(8,128)(2,1)S(1)}, u32[]{:S(2)}, u32[]{:S(2)}) collective-permute-start(bf16[64,256]{1,0:T(8,128)(2,1)S(1)} %get-tuple-element.71), channel_id=1, source_target_pairs={{0,16},{4,20},{8,24},{12,28},{16,0},{20,4},{24,8},{28,12},{1,17},{... | collective-permute-start | bytes 98312 | tf_op jit(solution)/shard_map/ppermute | solution.py:558
  131.7 5.7 %collective-permute-start.17 = (bf16[64,256]{1,0:T(8,128)(2,1)S(1)}, bf16[64,256]{1,0:T(8,128)(2,1)S(1)}, u32[]{:S(2)}, u32[]{:S(2)}) collective-permute-start(bf16[64,256]{1,0:T(8,128)(2,1)S(1)} %get-tuple-element.72), channel_id=1, source_target_pairs={{0,24},{4,28},{8,16},{12,20},{16,8},{20,12},{24,0},{28,4},{1,25},{... | collective-permute-start | bytes 98312 | tf_op jit(solution)/shard_map/ppermute | solution.py:558
  141.3 6.6 %collective-permute-start.27 = (bf16[128,2048]{1,0:T(8,128)(2,1)S(1)}, bf16[128,2048]{1,0:T(8,128)(2,1)S(1)}, u32[]{:S(2)}, u32[]{:S(2)}) collective-permute-start(bf16[128,2048]{1,0:T(8,128)(2,1)S(1)} %get-tuple-element.88), channel_id=1, source_target_pairs={{0,1},{1,0},{2,3},{3,2},{4,5},{5,4},{6,7},{7,6},{8,9},{9,8},{10,11... | collective-permute-start | bytes 1572872 | tf_op jit(solution)/shard_map/ppermute | solution.py:583
  141.4 19.5 %collective-permute-start.26 = (bf16[128,2048]{1,0:T(8,128)(2,1)S(1)}, bf16[128,2048]{1,0:T(8,128)(2,1)S(1)}, u32[]{:S(2)}, u32[]{:S(2)}) collective-permute-start(bf16[128,2048]{1,0:T(8,128)(2,1)S(1)} %get-tuple-element.86), channel_id=1, source_target_pairs={{0,1},{1,0},{2,3},{3,2},{4,5},{5,4},{6,7},{7,6},{8,9},{9,8},{10,11... | collective-permute-start | bytes 1572872 | tf_op jit(solution)/shard_map/ppermute | solution.py:593
  143.0 4.2 %collective-permute-start.24 = (bf16[128,1024]{1,0:T(8,128)(2,1)S(1)}, bf16[128,1024]{1,0:T(8,128)(2,1)S(1)}, u32[]{:S(2)}, u32[]{:S(2)}) collective-permute-start(bf16[128,1024]{1,0:T(8,128)(2,1)S(1)} %get-tuple-element.84), channel_id=1, source_target_pairs={{0,1},{1,0},{2,3},{3,2},{4,5},{5,4},{6,7},{7,6},{8,9},{9,8},{10,11... | collective-permute-start | bytes 786440 | tf_op jit(solution)/shard_map/ppermute | solution.py:583
  145.1 15.4 %collective-permute-start.18 = (bf16[128,2048]{1,0:T(8,128)(2,1)S(1)}, bf16[128,2048]{1,0:T(8,128)(2,1)S(1)}, u32[]{:S(2)}, u32[]{:S(2)}) collective-permute-start(bf16[128,2048]{1,0:T(8,128)(2,1)S(1)} %get-tuple-element.76), channel_id=1, source_target_pairs={{0,1},{1,0},{2,3},{3,2},{4,5},{5,4},{6,7},{7,6},{8,9},{9,8},{10,11... | collective-permute-start | bytes 1572872 | tf_op jit(solution)/shard_map/ppermute | solution.py:593
  145.7 9.2 %collective-permute-start.23 = (bf16[128,1024]{1,0:T(8,128)(2,1)S(1)}, bf16[128,1024]{1,0:T(8,128)(2,1)S(1)}, u32[]{:S(2)}, u32[]{:S(2)}) collective-permute-start(bf16[128,1024]{1,0:T(8,128)(2,1)S(1)} %add_convert_fusion.6), channel_id=1, source_target_pairs={{0,2},{1,3},{2,0},{3,1},{4,6},{5,7},{6,4},{7,5},{8,10},{9,11},{10,... | collective-permute-start | bytes 786440 | tf_op jit(solution)/shard_map/ppermute | solution.py:587
  147.3 13.2 %collective-permute-start.25 = (bf16[128,1024]{1,0:T(8,128)(2,1)S(1)}, bf16[128,1024]{1,0:T(8,128)(2,1)S(1)}, u32[]{:S(2)}, u32[]{:S(2)}) collective-permute-start(bf16[128,1024]{1,0:T(8,128)(2,1)S(1)} %add_convert_fusion.4), channel_id=1, source_target_pairs={{0,2},{1,3},{2,0},{3,1},{4,6},{5,7},{6,4},{7,5},{8,10},{9,11},{10,... | collective-permute-start | bytes 786440 | tf_op jit(solution)/shard_map/ppermute | solution.py:587
  148.1 18.1 %collective-permute-start.28 = (bf16[128,1024]{1,0:T(8,128)(2,1)S(1)}, bf16[128,1024]{1,0:T(8,128)(2,1)S(1)}, u32[]{:S(2)}, u32[]{:S(2)}) collective-permute-start(bf16[128,1024]{1,0:T(8,128)(2,1)S(1)} %get-tuple-element.92), channel_id=1, source_target_pairs={{0,2},{1,3},{2,0},{3,1},{4,6},{5,7},{6,4},{7,5},{8,10},{9,11},{10,... | collective-permute-start | bytes 786440 | tf_op jit(solution)/shard_map/ppermute | solution.py:587
  154.9 16.0 %collective-permute-start.29 = (bf16[128,1024]{1,0:T(8,128)(2,1)S(1)}, bf16[128,1024]{1,0:T(8,128)(2,1)S(1)}, u32[]{:S(2)}, u32[]{:S(2)}) collective-permute-start(bf16[128,1024]{1,0:T(8,128)(2,1)S(1)} %get-tuple-element.91), channel_id=1, source_target_pairs={{0,2},{1,3},{2,0},{3,1},{4,6},{5,7},{6,4},{7,5},{8,10},{9,11},{10,... | collective-permute-start | bytes 786440 | tf_op jit(solution)/shard_map/ppermute | solution.py:587

commit v3 on v2

--- a/solution.py
+++ b/solution.py
@@ -164,49 +164,45 @@
         values_t[h, 0:HEAD, :] = turned[h * HEAD : (h + 1) * HEAD]
         values_t[h, HEAD : HEAD + 16, :] = tail
     step = 128
-    for b in range(rows // step):
-        first = here * whole_rows + begin + b * step
-
-        @pl.when(first >= live)
-        def _():
-            out_ref[:, b * step : (b + 1) * step] = jnp.zeros(
-                (out_ref.shape[0], step), jnp.float32
-            )
-
-        @pl.when(first < live)
-        def _():
-            wide = step + 2 * WINDOW
-            at = b * step
+    wide = step + 2 * WINDOW
+    start = here * whole_rows + begin
+
+    @pl.when(start >= live)
+    def _():
+        rows_ref[...] = jnp.zeros_like(rows_ref)
+
+    @pl.when(start < live)
+    def _():
+        for b in range(rows // step):
+            first, at = start + b * step, b * step
             key_at = lax.broadcasted_iota(jnp.int32, (wide, step), 0)
-            query_at = lax.broadcasted_iota(jnp.int32, (wide, step), 1)
+            gap = key_at - WINDOW - lax.broadcasted_iota(jnp.int32, (wide, step), 1)
             key_pos = first - WINDOW + key_at
-            gap = key_at - WINDOW - query_at
-            allowed = (
-                (gap <= WINDOW) & (gap >= -WINDOW) & (key_pos >= 0) & (key_pos < live)
-            )
-            live_row = (
-                first + lax.broadcasted_iota(jnp.int32, (1, step), 1)
-            ) < live
+            allowed = (gap <= WINDOW) & (gap >= -WINDOW) & (key_pos >= 0) & (key_pos < live)
+            hidden = jnp.where(allowed, 0.0, masked_score)
+            hidden = jnp.concatenate([hidden] * GROUP, axis=1)
+            live_row = (first + lax.broadcasted_iota(jnp.int32, (1, step), 1)) < live
             for h in range(kv_local):
-                key_block = keys[b * step : b * step + wide, h * HEAD : (h + 1) * HEAD]
-                value_block = values_t[h, :, b * step : b * step + wide]
-                for g in range(GROUP):
-                    head = h * GROUP + g
-                    q = q_ref[head * HEAD : (head + 1) * HEAD, at : at + step]
-                    s = jnp.dot(key_block, q, preferred_element_type=jnp.float32)
-                    s = jnp.where(allowed, s, masked_score)
-                    sink = sink_ref[head] * LOG2E
-                    top = jnp.maximum(jnp.max(s, axis=0, keepdims=True), sink)
-                    e = jnp.exp2(s - top).astype(jnp.bfloat16)
-                    mixed = jnp.dot(value_block, e, preferred_element_type=jnp.float32)
-                    total = mixed[HEAD : HEAD + 1] + jnp.exp2(sink - top)
-                    result = jnp.where(live_row, mixed[0:HEAD] / total, 0.0)
-                    out_ref[head * HEAD : (head + 1) * HEAD, b * step : (b + 1) * step] = (
-                        result
+                key_block = keys[at : at + wide, h * HEAD : (h + 1) * HEAD]
+                value_block = values_t[h, :, at : at + wide]
+                members = range(h * GROUP, (h + 1) * GROUP)
+                q = jnp.concatenate(
+                    [q_ref[g * HEAD : (g + 1) * HEAD, at : at + step] for g in members], axis=1
+                )
+                sink = jnp.concatenate(
+                    [jnp.full((1, step), sink_ref[g] * LOG2E, jnp.float32) for g in members], axis=1
+                )
+                s = jnp.dot(key_block, q, preferred_element_type=jnp.float32) + hidden
+                top = jnp.maximum(jnp.max(s, axis=0, keepdims=True), sink)
+                e = jnp.exp2(s - top).astype(jnp.bfloat16)
+                mixed = jnp.dot(value_block, e, preferred_element_type=jnp.float32)
+                total = mixed[HEAD : HEAD + 1] + jnp.exp2(sink - top)
+                result = mixed[0:HEAD] / total
+                for n, g in enumerate(members):
+                    out_ref[g * HEAD : (g + 1) * HEAD, at : at + step] = jnp.where(
+                        live_row, result[:, n * step : (n + 1) * step], 0.0
                     )
-
-        block = out_ref[:, b * step : (b + 1) * step]
-        rows_ref[b * step : (b + 1) * step, :] = jnp.transpose(block).astype(jnp.bfloat16)
+        rows_ref[...] = jnp.transpose(out_ref[...]).astype(jnp.bfloat16)
 
 
 def window_part(scal, sink_logit, q_t, low, kv, high, begin, whole_rows):

time: 172 us -> 171 us (level)
  Pallas kernels: 80.8 us -> 77.9 us
    pallas_call x2, Pallas kernels: 7.55 us -> 4.63 us  [window_part(): pl.pallas_call(functools.partial(window_kernel, begin, whole_rows, kv_loc...]
  transfers between devices with their start and end apart: 30 -> 30, of which waited for: 13 -> 13; matrix products, arithmetic and copies ran while one was open for 1% -> 1% of each run, Pallas kernels for 39% -> 38%
where the time goes in v3:
time: 171 us; the launch traced here: 170 us
  Pallas kernels  77.9 us (46%)
  waiting for transfers between devices  43.4 us (25%)
  starting transfers between devices  40.2 us (24%)
  local copies, waits for them, and re-layouts  4.95 us (3%)
  other arithmetic  2.71 us (2%)
    pallas_call x2, Pallas kernels, diff_last(): pl.pallas_call(functools.partial(diff_kernel, chunks, rows, heads, parts,...  23.7 us
    pallas_call x1, Pallas kernels, diff_first(): pl.pallas_call(functools.partial(diff_kernel, chunks, rows, heads, parts,...  23 us
    ppermute x4, waiting for transfers between devices, body(): crossed[i].append(lax.ppermute(piece, 'tp', flip('tp', 2 * o)))  18.3 us
    ppermute x2, waiting for transfers between devices, body(): lax.ppermute(pieces[c], 'tp', flip('tp', 2 * o))  11.6 us
    ppermute x6, starting transfers between devices, body(): moved.append(lax.ppermute(slots[d], 'sp', flip('sp', d * parts)))  11 us
    ppermute x6, starting transfers between devices, give_back(): lax.ppermute(mixed[d], 'sp', flip('sp', d * parts))  8.89 us
    pallas_call x5, Pallas kernels, out_part(): pl.pallas_call(functools.partial(out_kernel, heads, parts, offset, begin)...  8.12 us
    pallas_call x4, Pallas kernels, fetch(): pl.pallas_call(functools.partial(copy_kernel, begin), in_specs=[pl.BlockS...  7.76 us
  transfers between devices with their start and end apart: 30, of which 13 were waited for; matrix products, arithmetic and copies ran while one was open for 1% of the time, Pallas kernels for 38%

profile of v3, /device:TPU:0, one launch (start us, length us, event | category | flops | bytes accessed | tf_op | source)
XLA Modules:
  0.0 170.3 jit_solution(12877590412960374729)
XLA Ops:
  0.5 1.0 shard_map.129
  1.6 2.5 %collective-permute-start.1 = (bf16[256,1024]{1,0:T(8,128)(2,1)S(1)}, bf16[256,1024]{1,0:T(8,128)(2,1)}, u32[]{:S(2)}, u32[]{:S(2)}) collective-permute-start(bf16[256,1024]{1,0:T(8,128)(2,1)S(1)} %shard_map.129), channel_id=1, source_target_pairs={{0,2},{1,3},{2,0},{3,1},{4,6},{5,7},{6,4},{7,5},{8,10},{9,11},{10,... | collective-permute-start | bytes 1572872 | tf_op jit(solution)/shard_map/ppermute | solution.py:511
  4.1 1.8 %shard_map.131 = bf16[256,1024]{1,0:T(8,128)(2,1)} custom-call(bf16[512,1024]{1,0:T(8,128)(2,1)} %refs_0_.6), custom_call_target="tpu_custom_call" | custom-call | flops 1073741824 | tf_op jit(solution)/shard_map/pallas_call | solution.py:86
  6.0 10.9 %collective-permute-done.1.refs_0_ = bf16[256,1024]{1,0:T(8,128)(2,1)} collective-permute-done((bf16[256,1024]{1,0:T(8,128)(2,1)S(1)}, bf16[256,1024]{1,0:T(8,128)(2,1)}, u32[]{:S(2)}, u32[]{:S(2)}) %collective-permute-start.1) | collective-permute-done | bytes 524320 | tf_op jit(solution)/shard_map/ppermute | solution.py:511
  17.0 1.9 %copy-done.2 = bf16[384,4096]{1,0:T(8,128)(2,1)S(1)} copy-done((bf16[384,4096]{1,0:T(8,128)(2,1)S(1)}, bf16[384,4096]{1,0:T(8,128)(2,1)}, u32[]{:S(2)}) %copy-start.2) | copy-done | bytes 3145752
  18.9 1.6 copy-done.3
  20.9 1.3 copy-done
  22.8 4.5 %shard_map.127 = (bf16[4096,384]{1,0:T(8,128)(2,1)S(1)}, bf16[4096,128]{1,0:T(8,128)(2,1)S(1)}, bf16[4096,128]{1,0:T(8,128)(2,1)S(1)}, bf16[4096,256]{1,0:T(8,12...) custom-call(bf16[4096,384]{1,0:T(8,128)(2,1)} %refs_0_.4, bf16[4096,128]{1,0:T(8,128)(2,1)} %refs_1_.2, ...), custom_call_target="tpu_custom_call" | custom-call | flops 1073741824 | tf_op jit(solution)/shard_map/pallas_call | solution.py:86
  27.4 0.7 collective-permute-done.3.refs_0_
  28.1 4.6 %shard_map.128.acc_ref = f32[512,1408]{1,0:T(8,128)S(1)} custom-call(s32[3]{0:T(128)S(1)} %pad_add_fusion.scal_ref, bf16[512,1024]{1,0:T(8,128)(2,1)S(1)} %copy-done.4, bf16[512,1024]{1,0:T(8,128)(2,1)} %collective-permute-done.sib_ref, bf16[4096,384]{1,0:T(8,128)(2,1)S(1)} %get-tuple-element.47.refs_0_.refs_2_, ...), custom_call_target="tpu_custom_call" | custom-call | flops 2952790016 | tf_op jit(solution)/shard_map/pallas_call | solution.py:59
  32.8 3.1 %shard_map.130 = (bf16[384,256]{1,0:T(8,128)(2,1)S(1)}, bf16[256,256]{1,0:T(8,128)(2,1)S(1)}, bf16[384,128]{1,0:T(8,128)(2,1)S(1)}, bf16[384,128]{1,0:T(8,128)(2...) custom-call(s32[3]{0:T(128)S(1)} %pad_add_fusion.scal_ref, f32[512,1408]{1,0:T(8,128)S(1)} %shard_map.128.acc_ref, ...), custom_call_target="tpu_custom_call" | custom-call | flops 1476395008 | tf_op jit(solution)/shard_map/pallas_call | solution.py:140
  35.9 1.3 collective-permute-start.6
  37.2 3.0 %shard_map.132 = (bf16[384,256]{1,0:T(8,128)(2,1)S(1)}, bf16[256,256]{1,0:T(8,128)(2,1)S(1)}, bf16[384,128]{1,0:T(8,128)(2,1)S(1)}, bf16[384,128]{1,0:T(8,128)(2...) custom-call(s32[3]{0:T(128)S(1)} %pad_add_fusion.scal_ref, f32[512,1408]{1,0:T(8,128)S(1)} %shard_map.128.acc_ref, ...), custom_call_target="tpu_custom_call" | custom-call | flops 1476395008 | tf_op jit(solution)/shard_map/pallas_call | solution.py:140
  40.2 4.6 %collective-permute-start.5 = (bf16[128,256]{1,0:T(8,128)(2,1)S(1)}, bf16[128,256]{1,0:T(8,128)(2,1)S(1)}, u32[]{:S(2)}, u32[]{:S(2)}) collective-permute-start(bf16[128,256]{1,0:T(8,128)(2,1)S(1)} %slice.61), channel_id=1, source_target_pairs={{0,4},{4,8},{8,12},{12,16},{16,20},{20,24},{24,28},{1,5},{5,9},{9,... | collective-permute-start | bytes 196616 | tf_op jit(solution)/shard_map/ppermute | solution.py:534
  44.8 4.1 %collective-permute-start.9 = (bf16[384,128]{1,0:T(8,128)(2,1)S(1)}, bf16[384,128]{1,0:T(8,128)(2,1)S(1)}, u32[]{:S(2)}, u32[]{:S(2)}) collective-permute-start(bf16[384,128]{1,0:T(8,128)(2,1)S(1)} %get-tuple-element.60), channel_id=1, source_target_pairs={{0,24},{4,28},{8,16},{12,20},{16,8},{20,12},{24,0},{28,4},{1,25},{... | collective-permute-start | bytes 294920 | tf_op jit(solution)/shard_map/ppermute | solution.py:526
  49.5 3.8 %collective-permute-start.13 = (bf16[384,128]{1,0:T(8,128)(2,1)S(1)}, bf16[384,128]{1,0:T(8,128)(2,1)S(1)}, u32[]{:S(2)}, u32[]{:S(2)}) collective-permute-start(bf16[384,128]{1,0:T(8,128)(2,1)S(1)} %get-tuple-element.64), channel_id=1, source_target_pairs={{0,24},{4,28},{8,16},{12,20},{16,8},{20,12},{24,0},{28,4},{1,25},{... | collective-permute-start | bytes 294920 | tf_op jit(solution)/shard_map/ppermute | solution.py:526
  53.3 2.3 %shard_map.134 = bf16[256,384]{1,0:T(8,128)(2,1)S(1)} custom-call(s32[3]{0:T(128)S(1)} %pad_add_fusion.scal_ref, f32[6]{0:T(128)S(1)} %copy-done.5, bf16[384,256]{1,0:T(8,128)(2,1)S(1)} %get-tuple-element.56.refs_0_, bf16[256,256]{1,0:T(8,128)(2,1)S(1)} %get-tuple-element.55.refs_2_.refs_1_, bf16[256,256]{1,0:T(8,128)(2,1)S(1)} %get-tuple-element.54.refs_3_.refs_2_, ...), custom_call_target="tpu_custom_call" | custom-call | flops 1509949440 | tf_op jit(solution)/shard_map/pallas_call | solution.py:212
  55.7 2.4 %collective-permute-start.12 = (bf16[384,128]{1,0:T(8,128)(2,1)S(1)}, bf16[384,128]{1,0:T(8,128)(2,1)S(1)}, u32[]{:S(2)}, u32[]{:S(2)}) collective-permute-start(bf16[384,128]{1,0:T(8,128)(2,1)S(1)} %get-tuple-element.63), channel_id=1, source_target_pairs={{0,16},{4,20},{8,24},{12,28},{16,0},{20,4},{24,8},{28,12},{1,17},{... | collective-permute-start | bytes 294920 | tf_op jit(solution)/shard_map/ppermute | solution.py:526
  58.1 3.0 %collective-permute-done.8.refs_4_ = bf16[384,128]{1,0:T(8,128)(2,1)S(1)} collective-permute-done((bf16[384,128]{1,0:T(8,128)(2,1)S(1)}, bf16[384,128]{1,0:T(8,128)(2,1)S(1)}, u32[]{:S(2)}, u32[]{:S(2)}) %collective-permute-start.8) | collective-permute-done | bytes 98336 | tf_op jit(solution)/shard_map/ppermute | solution.py:526
  61.2 2.4 %collective-permute-start.10 = (bf16[4,256,128]{2,1,0:T(8,128)(2,1)S(1)}, bf16[4,256,128]{2,1,0:T(8,128)(2,1)S(1)}, u32[]{:S(2)}, u32[]{:S(2)}) collective-permute-start(bf16[4,256,128]{2,1,0:T(8,128)(2,1)S(1)} %pad_maximum_fusion.2.refs_0_), channel_id=1, source_target_pairs={{0,4},{4,0},{8,12},{12,8},{16,20},{20,16},{24,28},{28,24},{1,5},{5... | collective-permute-start | bytes 786440 | tf_op jit(solution)/shard_map/ppermute | solution.py:529
  63.7 1.9 %collective-permute-done.12.refs_8_ = bf16[384,128]{1,0:T(8,128)(2,1)S(1)} collective-permute-done((bf16[384,128]{1,0:T(8,128)(2,1)S(1)}, bf16[384,128]{1,0:T(8,128)(2,1)S(1)}, u32[]{:S(2)}, u32[]{:S(2)}) %collective-permute-start.12) | collective-permute-done | bytes 98336 | tf_op jit(solution)/shard_map/ppermute | solution.py:526
  65.6 1.0 collective-permute-done.11.refs_7_
  66.6 2.5 %collective-permute-start.14 = (bf16[4,256,128]{2,1,0:T(8,128)(2,1)S(1)}, bf16[4,256,128]{2,1,0:T(8,128)(2,1)S(1)}, u32[]{:S(2)}, u32[]{:S(2)}) collective-permute-start(bf16[4,256,128]{2,1,0:T(8,128)(2,1)S(1)} %pad_maximum_fusion.3.refs_1_), channel_id=1, source_target_pairs={{0,4},{4,0},{8,12},{12,8},{16,20},{20,16},{24,28},{28,24},{1,5},{5... | collective-permute-start | bytes 786440 | tf_op jit(solution)/shard_map/ppermute | solution.py:529
  69.1 2.3 %shard_map.133 = bf16[256,384]{1,0:T(8,128)(2,1)S(1)} custom-call(s32[3]{0:T(128)S(1)} %pad_add_fusion.scal_ref, f32[6]{0:T(128)S(1)} %copy-done.5, bf16[384,256]{1,0:T(8,128)(2,1)S(1)} %get-tuple-element.53.refs_0_, bf16[128,256]{1,0:T(8,128)(2,1)S(1)} %collective-permute-done.5.refs_1_, bf16[256,256]{1,0:T(8,128)(2,1)S(1)} %get-tuple-element.55.refs_2_.refs_1_, ...), custom_call_target="tpu_custom_call" | custom-call | flops 1509949440 | tf_op jit(solution)/shard_map/pallas_call | solution.py:212
  71.4 23.0 %shard_map.135 = (bf16[8,128,512]{2,1,0:T(8,128)(2,1)S(1)}, f32[8,80,512]{2,1,0:T(8,128)S(1)}, f32[8,1,512]{2,1,0:T(1,128)S(1)}, s32[8]{0:T(128)S(1)}) custom-call(s32[3]{0:T(128)S(1)} %pad_add_fusion.scal_ref, bf16[4,256,128]{2,1,0:T(8,128)(2,1)S(1)} %pad_maximum_fusion.2.refs_0_, bf16[4,256,128]{2,1,0:T(8,128)(2,1)S(1)} %pad_maximum_fusion.3.refs_1_, ...), custom_call_target="tpu_custom_call" | custom-call | flops 2097152000 | tf_op jit(solution)/shard_map/pallas_call | solution.py:384
  94.5 11.8 %shard_map.139 = (bf16[64,256]{1,0:T(8,128)(2,1)S(1)}, bf16[64,256]{1,0:T(8,128)(2,1)S(1)}, bf16[64,256]{1,0:T(8,128)(2,1)S(1)}, bf16[64,256]{1,0:T(8,128)(2,1)S(1)}) custom-call(s32[3]{0:T(128)S(1)} %pad_add_fusion.scal_ref, bf16[4,256,128]{2,1,0:T(8,128)(2,1)S(1)} %collective-permute-done.10.refs_0_, ...), custom_call_target="tpu_custom_call" | custom-call | flops 2097152000 | tf_op jit(solution)/shard_map/pallas_call | solution.py:409
  106.4 3.0 %collective-permute-start.20 = (bf16[64,256]{1,0:T(8,128)(2,1)S(1)}, bf16[64,256]{1,0:T(8,128)(2,1)S(1)}, u32[]{:S(2)}, u32[]{:S(2)}) collective-permute-start(bf16[64,256]{1,0:T(8,128)(2,1)S(1)} %get-tuple-element.79), channel_id=1, source_target_pairs={{0,16},{4,20},{8,24},{12,28},{16,0},{20,4},{24,8},{28,12},{1,17},{... | collective-permute-start | bytes 98312 | tf_op jit(solution)/shard_map/ppermute | solution.py:554
  109.4 1.3 collective-permute-start.21
  111.3 3.8 %collective-permute-done.21.refs_3_ = bf16[64,256]{1,0:T(8,128)(2,1)S(1)} collective-permute-done((bf16[64,256]{1,0:T(8,128)(2,1)S(1)}, bf16[64,256]{1,0:T(8,128)(2,1)S(1)}, u32[]{:S(2)}, u32[]{:S(2)}) %collective-permute-start.21) | collective-permute-done | bytes 32800 | tf_op jit(solution)/shard_map/ppermute | solution.py:554
  115.2 1.2 shard_map.140
  116.4 11.8 %shard_map.136 = (bf16[64,256]{1,0:T(8,128)(2,1)S(1)}, bf16[64,256]{1,0:T(8,128)(2,1)S(1)}, bf16[64,256]{1,0:T(8,128)(2,1)S(1)}, bf16[64,256]{1,0:T(8,128)(2,1)S(1)}) custom-call(s32[3]{0:T(128)S(1)} %pad_add_fusion.scal_ref, bf16[4,256,128]{2,1,0:T(8,128)(2,1)S(1)} %collective-permute-done.10.refs_0_, ...), custom_call_target="tpu_custom_call" | custom-call | flops 2097152000 | tf_op jit(solution)/shard_map/pallas_call | solution.py:409
  128.3 1.9 %collective-permute-start.16 = (bf16[64,256]{1,0:T(8,128)(2,1)S(1)}, bf16[64,256]{1,0:T(8,128)(2,1)S(1)}, u32[]{:S(2)}, u32[]{:S(2)}) collective-permute-start(bf16[64,256]{1,0:T(8,128)(2,1)S(1)} %get-tuple-element.71), channel_id=1, source_target_pairs={{0,16},{4,20},{8,24},{12,28},{16,0},{20,4},{24,8},{28,12},{1,17},{... | collective-permute-start | bytes 98312 | tf_op jit(solution)/shard_map/ppermute | solution.py:554
  130.2 2.5 %collective-permute-start.17 = (bf16[64,256]{1,0:T(8,128)(2,1)S(1)}, bf16[64,256]{1,0:T(8,128)(2,1)S(1)}, u32[]{:S(2)}, u32[]{:S(2)}) collective-permute-start(bf16[64,256]{1,0:T(8,128)(2,1)S(1)} %get-tuple-element.72), channel_id=1, source_target_pairs={{0,24},{4,28},{8,16},{12,20},{16,8},{20,12},{24,0},{28,4},{1,25},{... | collective-permute-start | bytes 98312 | tf_op jit(solution)/shard_map/ppermute | solution.py:554
  132.7 0.7 collective-permute-done.16.refs_2_
  133.4 2.5 %collective-permute-done.17.refs_3_ = bf16[64,256]{1,0:T(8,128)(2,1)S(1)} collective-permute-done((bf16[64,256]{1,0:T(8,128)(2,1)S(1)}, bf16[64,256]{1,0:T(8,128)(2,1)S(1)}, u32[]{:S(2)}, u32[]{:S(2)}) %collective-permute-start.17) | collective-permute-done | bytes 32800 | tf_op jit(solution)/shard_map/ppermute | solution.py:554
  135.9 1.9 %shard_map.142 = (bf16[128,2048]{1,0:T(8,128)(2,1)S(1)}, bf16[128,2048]{1,0:T(8,128)(2,1)S(1)}) custom-call(s32[3]{0:T(128)S(1)} %pad_add_fusion.scal_ref, bf16[512,384]{1,0:T(8,128)(2,1)S(1)} %pad_maximum_fusion.1.win_ref, bf16[64,256]{1,0:T(8,128)(2,1)S(1)} %get-tuple-element.69.refs_0_, bf16[64,256]{1,0:T(8,128)(2,1)S(1)} %collective-permute-done.15.refs_1_, ...), custom_call_target="tpu_custom_call" | custom-call | flops 671088640 | tf_op jit(solution)/shard_map/pallas_call | solution.py:466
  137.9 1.9 %shard_map.143 = (bf16[128,2048]{1,0:T(8,128)(2,1)S(1)}, bf16[128,2048]{1,0:T(8,128)(2,1)S(1)}) custom-call(s32[3]{0:T(128)S(1)} %pad_add_fusion.scal_ref, bf16[512,384]{1,0:T(8,128)(2,1)S(1)} %pad_maximum_fusion.1.win_ref, bf16[64,256]{1,0:T(8,128)(2,1)S(1)} %get-tuple-element.77.refs_0_, bf16[64,256]{1,0:T(8,128)(2,1)S(1)} %collective-permute-done.19.refs_1_, ...), custom_call_target="tpu_custom_call" | custom-call | flops 671088640 | tf_op jit(solution)/shard_map/pallas_call | solution.py:466
  140.4 1.2 shard_map.141
  141.7 1.9 %shard_map.138 = (bf16[128,2048]{1,0:T(8,128)(2,1)S(1)}, bf16[128,2048]{1,0:T(8,128)(2,1)S(1)}) custom-call(s32[3]{0:T(128)S(1)} %pad_add_fusion.scal_ref, bf16[512,384]{1,0:T(8,128)(2,1)S(1)} %pad_maximum_fusion.1.win_ref, bf16[64,256]{1,0:T(8,128)(2,1)S(1)} %get-tuple-element.69.refs_0_, bf16[64,256]{1,0:T(8,128)(2,1)S(1)} %collective-permute-done.15.refs_1_, ...), custom_call_target="tpu_custom_call" | custom-call | flops 671088640 | tf_op jit(solution)/shard_map/pallas_call | solution.py:466
  144.2 1.6 collective-permute-start.23
  146.6 1.6 collective-permute-start.28
  148.2 5.3 %collective-permute-done.23 = bf16[128,1024]{1,0:T(8,128)(2,1)S(1)} collective-permute-done((bf16[128,1024]{1,0:T(8,128)(2,1)S(1)}, bf16[128,1024]{1,0:T(8,128)(2,1)S(1)}, u32[]{:S(2)}, u32[]{:S(2)}) %collective-permute-start.23) | collective-permute-done | bytes 262176 | tf_op jit(solution)/shard_map/ppermute | solution.py:583
  153.4 1.5 collective-permute-start.29
  154.9 4.1 %collective-permute-done.25 = bf16[128,1024]{1,0:T(8,128)(2,1)S(1)} collective-permute-done((bf16[128,1024]{1,0:T(8,128)(2,1)S(1)}, bf16[128,1024]{1,0:T(8,128)(2,1)S(1)}, u32[]{:S(2)}, u32[]{:S(2)}) %collective-permute-start.25) | collective-permute-done | bytes 262176 | tf_op jit(solution)/shard_map/ppermute | solution.py:583
  159.4 5.3 %collective-permute-done.28 = bf16[128,1024]{1,0:T(8,128)(2,1)S(1)} collective-permute-done((bf16[128,1024]{1,0:T(8,128)(2,1)S(1)}, bf16[128,1024]{1,0:T(8,128)(2,1)S(1)}, u32[]{:S(2)}, u32[]{:S(2)}) %collective-permute-start.28) | collective-permute-done | bytes 262176 | tf_op jit(solution)/shard_map/ppermute | solution.py:583
  164.8 1.0 pad_maximum_fusion
  165.9 3.6 %collective-permute-done.29 = bf16[128,1024]{1,0:T(8,128)(2,1)S(1)} collective-permute-done((bf16[128,1024]{1,0:T(8,128)(2,1)S(1)}, bf16[128,1024]{1,0:T(8,128)(2,1)S(1)}, u32[]{:S(2)}, u32[]{:S(2)}) %collective-permute-start.29) | collective-permute-done | bytes 262176 | tf_op jit(solution)/shard_map/ppermute | solution.py:583
  169.4 0.8 fusion
  (68 shorter events, 5.1 us)
Async XLA Ops:
  0.0 28.1 %collective-permute-start = (bf16[512,1024]{1,0:T(8,128)(2,1)}, bf16[512,1024]{1,0:T(8,128)(2,1)}, u32[]{:S(2)}, u32[]{:S(2)}) collective-permute-start(bf16[512,1024]{1,0:T(8,128)(2,1)} %refs_0_.6), channel_id=1, source_target_pairs={{0,1},{1,0},{2,3},{3,2},{4,5},{5,4},{6,7},{7,6},{8,9},{9,8},{10,11... | collective-permute-start | bytes 3145736 | tf_op jit(solution)/shard_map/ppermute | solution.py:514
  1.6 15.4 %collective-permute-start.1 = (bf16[256,1024]{1,0:T(8,128)(2,1)S(1)}, bf16[256,1024]{1,0:T(8,128)(2,1)}, u32[]{:S(2)}, u32[]{:S(2)}) collective-permute-start(bf16[256,1024]{1,0:T(8,128)(2,1)S(1)} %shard_map.129), channel_id=1, source_target_pairs={{0,2},{1,3},{2,0},{3,1},{4,6},{5,7},{6,4},{7,5},{8,10},{9,11},{10,... | collective-permute-start | bytes 1572872 | tf_op jit(solution)/shard_map/ppermute | solution.py:511
  5.9 22.1 %collective-permute-start.3 = (bf16[256,1024]{1,0:T(8,128)(2,1)}, bf16[256,1024]{1,0:T(8,128)(2,1)}, u32[]{:S(2)}, u32[]{:S(2)}) collective-permute-start(bf16[256,1024]{1,0:T(8,128)(2,1)} %shard_map.131), channel_id=1, source_target_pairs={{0,2},{1,3},{2,0},{3,1},{4,6},{5,7},{6,4},{7,5},{8,10},{9,11},{10,... | collective-permute-start | bytes 1572872 | tf_op jit(solution)/shard_map/ppermute | solution.py:511
  17.0 15.8 %collective-permute-start.2 = (bf16[256,1024]{1,0:T(8,128)(2,1)}, bf16[256,1024]{1,0:T(8,128)(2,1)}, u32[]{:S(2)}, u32[]{:S(2)}) collective-permute-start(bf16[256,1024]{1,0:T(8,128)(2,1)} %collective-permute-done.1.refs_0_), channel_id=1, source_target_pairs={{0,1},{1,0},{2,3},{3,2},{4,5},{5,4},{6,7},{7,6},{8,9},{9,8},{10,11... | collective-permute-start | bytes 1572872 | tf_op jit(solution)/shard_map/ppermute | solution.py:520
  17.0 1.9 %copy-start.2 = (bf16[384,4096]{1,0:T(8,128)(2,1)S(1)}, bf16[384,4096]{1,0:T(8,128)(2,1)}, u32[]{:S(2)}) copy-start(bf16[384,4096]{1,0:T(8,128)(2,1)} %refs_0_.7) | copy-start | bytes 9437188
  18.9 1.6 copy-start.3
  20.8 1.3 copy-start
  22.8 5.3 %copy-start.4 = (bf16[512,1024]{1,0:T(8,128)(2,1)S(1)}, bf16[512,1024]{1,0:T(8,128)(2,1)}, u32[]{:S(2)}) copy-start(bf16[512,1024]{1,0:T(8,128)(2,1)} %refs_0_.6) | copy-start | bytes 3145732
  28.0 9.2 %collective-permute-start.4 = (bf16[256,1024]{1,0:T(8,128)(2,1)}, bf16[256,1024]{1,0:T(8,128)(2,1)S(1)}, u32[]{:S(2)}, u32[]{:S(2)}) collective-permute-start(bf16[256,1024]{1,0:T(8,128)(2,1)} %collective-permute-done.3.refs_0_), channel_id=1, source_target_pairs={{0,1},{1,0},{2,3},{3,2},{4,5},{5,4},{6,7},{7,6},{8,9},{9,8},{10,11... | collective-permute-start | bytes 1572872 | tf_op jit(solution)/shard_map/ppermute | solution.py:520
  35.9 17.4 %copy-start.5 = (f32[6]{0:T(128)S(1)}, f32[6]{0:T(128)}, u32[]{:S(2)}) copy-start(f32[6]{0:T(128)} %sink_ref.3) | copy-start | bytes 76
  35.9 13.6 %collective-permute-start.6 = (bf16[128,256]{1,0:T(8,128)(2,1)S(1)}, bf16[128,256]{1,0:T(8,128)(2,1)S(1)}, u32[]{:S(2)}, u32[]{:S(2)}) collective-permute-start(bf16[128,256]{1,0:T(8,128)(2,1)S(1)} %slice.62), channel_id=1, source_target_pairs={{4,0},{8,4},{12,8},{16,12},{20,16},{24,20},{28,24},{5,1},{9,5},{13... | collective-permute-start | bytes 196616 | tf_op jit(solution)/shard_map/ppermute | solution.py:535
  40.2 28.9 %collective-permute-start.5 = (bf16[128,256]{1,0:T(8,128)(2,1)S(1)}, bf16[128,256]{1,0:T(8,128)(2,1)S(1)}, u32[]{:S(2)}, u32[]{:S(2)}) collective-permute-start(bf16[128,256]{1,0:T(8,128)(2,1)S(1)} %slice.61), channel_id=1, source_target_pairs={{0,4},{4,8},{8,12},{12,16},{16,20},{20,24},{24,28},{1,5},{5,9},{9,... | collective-permute-start | bytes 196616 | tf_op jit(solution)/shard_map/ppermute | solution.py:534
  44.8 10.9 %collective-permute-start.9 = (bf16[384,128]{1,0:T(8,128)(2,1)S(1)}, bf16[384,128]{1,0:T(8,128)(2,1)S(1)}, u32[]{:S(2)}, u32[]{:S(2)}) collective-permute-start(bf16[384,128]{1,0:T(8,128)(2,1)S(1)} %get-tuple-element.60), channel_id=1, source_target_pairs={{0,24},{4,28},{8,16},{12,20},{16,8},{20,12},{24,0},{28,4},{1,25},{... | collective-permute-start | bytes 294920 | tf_op jit(solution)/shard_map/ppermute | solution.py:526
  48.9 12.3 %collective-permute-start.8 = (bf16[384,128]{1,0:T(8,128)(2,1)S(1)}, bf16[384,128]{1,0:T(8,128)(2,1)S(1)}, u32[]{:S(2)}, u32[]{:S(2)}) collective-permute-start(bf16[384,128]{1,0:T(8,128)(2,1)S(1)} %get-tuple-element.59), channel_id=1, source_target_pairs={{0,16},{4,20},{8,24},{12,28},{16,0},{20,4},{24,8},{28,12},{1,17},{... | collective-permute-start | bytes 294920 | tf_op jit(solution)/shard_map/ppermute | solution.py:526
  48.9 12.3 %collective-permute-start.7 = (bf16[384,128]{1,0:T(8,128)(2,1)S(1)}, bf16[384,128]{1,0:T(8,128)(2,1)S(1)}, u32[]{:S(2)}, u32[]{:S(2)}) collective-permute-start(bf16[384,128]{1,0:T(8,128)(2,1)S(1)} %get-tuple-element.58), channel_id=1, source_target_pairs={{0,8},{4,12},{8,0},{12,4},{16,24},{20,28},{24,16},{28,20},{1,9},{5... | collective-permute-start | bytes 294920 | tf_op jit(solution)/shard_map/ppermute | solution.py:526
  49.5 14.2 %collective-permute-start.13 = (bf16[384,128]{1,0:T(8,128)(2,1)S(1)}, bf16[384,128]{1,0:T(8,128)(2,1)S(1)}, u32[]{:S(2)}, u32[]{:S(2)}) collective-permute-start(bf16[384,128]{1,0:T(8,128)(2,1)S(1)} %get-tuple-element.64), channel_id=1, source_target_pairs={{0,24},{4,28},{8,16},{12,20},{16,8},{20,12},{24,0},{28,4},{1,25},{... | collective-permute-start | bytes 294920 | tf_op jit(solution)/shard_map/ppermute | solution.py:526
  55.7 9.9 %collective-permute-start.12 = (bf16[384,128]{1,0:T(8,128)(2,1)S(1)}, bf16[384,128]{1,0:T(8,128)(2,1)S(1)}, u32[]{:S(2)}, u32[]{:S(2)}) collective-permute-start(bf16[384,128]{1,0:T(8,128)(2,1)S(1)} %get-tuple-element.63), channel_id=1, source_target_pairs={{0,16},{4,20},{8,24},{12,28},{16,0},{20,4},{24,8},{28,12},{1,17},{... | collective-permute-start | bytes 294920 | tf_op jit(solution)/shard_map/ppermute | solution.py:526
  61.2 5.4 %collective-permute-start.11 = (bf16[384,128]{1,0:T(8,128)(2,1)S(1)}, bf16[384,128]{1,0:T(8,128)(2,1)S(1)}, u32[]{:S(2)}, u32[]{:S(2)}) collective-permute-start(bf16[384,128]{1,0:T(8,128)(2,1)S(1)} %get-tuple-element.62), channel_id=1, source_target_pairs={{0,8},{4,12},{8,0},{12,4},{16,24},{20,28},{24,16},{28,20},{1,9},{5... | collective-permute-start | bytes 294920 | tf_op jit(solution)/shard_map/ppermute | solution.py:526
  61.2 33.2 %collective-permute-start.10 = (bf16[4,256,128]{2,1,0:T(8,128)(2,1)S(1)}, bf16[4,256,128]{2,1,0:T(8,128)(2,1)S(1)}, u32[]{:S(2)}, u32[]{:S(2)}) collective-permute-start(bf16[4,256,128]{2,1,0:T(8,128)(2,1)S(1)} %pad_maximum_fusion.2.refs_0_), channel_id=1, source_target_pairs={{0,4},{4,0},{8,12},{12,8},{16,20},{20,16},{24,28},{28,24},{1,5},{5... | collective-permute-start | bytes 786440 | tf_op jit(solution)/shard_map/ppermute | solution.py:529
  66.6 27.9 %collective-permute-start.14 = (bf16[4,256,128]{2,1,0:T(8,128)(2,1)S(1)}, bf16[4,256,128]{2,1,0:T(8,128)(2,1)S(1)}, u32[]{:S(2)}, u32[]{:S(2)}) collective-permute-start(bf16[4,256,128]{2,1,0:T(8,128)(2,1)S(1)} %pad_maximum_fusion.3.refs_1_), channel_id=1, source_target_pairs={{0,4},{4,0},{8,12},{12,8},{16,20},{20,16},{24,28},{28,24},{1,5},{5... | collective-permute-start | bytes 786440 | tf_op jit(solution)/shard_map/ppermute | solution.py:529
  71.4 23.1 %copy-start.6 = (f32[4]{0:T(128)S(1)}, f32[4]{0:T(128)}, u32[]{:S(2)}) copy-start(f32[4]{0:T(128)} %refs_6_.3) | copy-start | bytes 52
  71.4 23.1 %copy-start.7 = (f32[64]{0:T(128)S(1)}, f32[64]{0:T(128)}, u32[]{:S(2)}) copy-start(f32[64]{0:T(128)} %param.23) | copy-start | bytes 772
  94.5 20.7 %copy-start.1 = (bf16[256,4096]{1,0:T(8,128)(2,1)S(1)}, bf16[256,4096]{1,0:T(8,128)(2,1)}, u32[]{:S(2)}) copy-start(bf16[256,4096]{1,0:T(8,128)(2,1)} %copy-done) | copy-start | bytes 6291460
  106.3 4.5 %collective-permute-start.19 = (bf16[64,256]{1,0:T(8,128)(2,1)S(1)}, bf16[64,256]{1,0:T(8,128)(2,1)S(1)}, u32[]{:S(2)}, u32[]{:S(2)}) collective-permute-start(bf16[64,256]{1,0:T(8,128)(2,1)S(1)} %get-tuple-element.78), channel_id=1, source_target_pairs={{0,8},{4,12},{8,0},{12,4},{16,24},{20,28},{24,16},{28,20},{1,9},{5... | collective-permute-start | bytes 98312 | tf_op jit(solution)/shard_map/ppermute | solution.py:554
  106.4 4.9 %collective-permute-start.20 = (bf16[64,256]{1,0:T(8,128)(2,1)S(1)}, bf16[64,256]{1,0:T(8,128)(2,1)S(1)}, u32[]{:S(2)}, u32[]{:S(2)}) collective-permute-start(bf16[64,256]{1,0:T(8,128)(2,1)S(1)} %get-tuple-element.79), channel_id=1, source_target_pairs={{0,16},{4,20},{8,24},{12,28},{16,0},{20,4},{24,8},{28,12},{1,17},{... | collective-permute-start | bytes 98312 | tf_op jit(solution)/shard_map/ppermute | solution.py:554
  109.4 5.7 %collective-permute-start.21 = (bf16[64,256]{1,0:T(8,128)(2,1)S(1)}, bf16[64,256]{1,0:T(8,128)(2,1)S(1)}, u32[]{:S(2)}, u32[]{:S(2)}) collective-permute-start(bf16[64,256]{1,0:T(8,128)(2,1)S(1)} %get-tuple-element.80), channel_id=1, source_target_pairs={{0,24},{4,28},{8,16},{12,20},{16,8},{20,12},{24,0},{28,4},{1,25},{... | collective-permute-start | bytes 98312 | tf_op jit(solution)/shard_map/ppermute | solution.py:554
  116.3 27.8 %collective-permute-start.22 = (bf16[128,1024]{1,0:T(8,128)(2,1)S(1)}, bf16[128,1024]{1,0:T(8,128)(2,1)S(1)}, u32[]{:S(2)}, u32[]{:S(2)}) collective-permute-start(bf16[128,1024]{1,0:T(8,128)(2,1)S(1)} %get-tuple-element.82), channel_id=1, source_target_pairs={{0,1},{1,0},{2,3},{3,2},{4,5},{5,4},{6,7},{7,6},{8,9},{9,8},{10,11... | collective-permute-start | bytes 786440 | tf_op jit(solution)/shard_map/ppermute | solution.py:579
  128.3 4.5 %collective-permute-start.15 = (bf16[64,256]{1,0:T(8,128)(2,1)S(1)}, bf16[64,256]{1,0:T(8,128)(2,1)S(1)}, u32[]{:S(2)}, u32[]{:S(2)}) collective-permute-start(bf16[64,256]{1,0:T(8,128)(2,1)S(1)} %get-tuple-element.70), channel_id=1, source_target_pairs={{0,8},{4,12},{8,0},{12,4},{16,24},{20,28},{24,16},{28,20},{1,9},{5... | collective-permute-start | bytes 98312 | tf_op jit(solution)/shard_map/ppermute | solution.py:554
  128.3 5.1 %collective-permute-start.16 = (bf16[64,256]{1,0:T(8,128)(2,1)S(1)}, bf16[64,256]{1,0:T(8,128)(2,1)S(1)}, u32[]{:S(2)}, u32[]{:S(2)}) collective-permute-start(bf16[64,256]{1,0:T(8,128)(2,1)S(1)} %get-tuple-element.71), channel_id=1, source_target_pairs={{0,16},{4,20},{8,24},{12,28},{16,0},{20,4},{24,8},{28,12},{1,17},{... | collective-permute-start | bytes 98312 | tf_op jit(solution)/shard_map/ppermute | solution.py:554
  130.2 5.7 %collective-permute-start.17 = (bf16[64,256]{1,0:T(8,128)(2,1)S(1)}, bf16[64,256]{1,0:T(8,128)(2,1)S(1)}, u32[]{:S(2)}, u32[]{:S(2)}) collective-permute-start(bf16[64,256]{1,0:T(8,128)(2,1)S(1)} %get-tuple-element.72), channel_id=1, source_target_pairs={{0,24},{4,28},{8,16},{12,20},{16,8},{20,12},{24,0},{28,4},{1,25},{... | collective-permute-start | bytes 98312 | tf_op jit(solution)/shard_map/ppermute | solution.py:554
  139.8 6.6 %collective-permute-start.27 = (bf16[128,2048]{1,0:T(8,128)(2,1)S(1)}, bf16[128,2048]{1,0:T(8,128)(2,1)S(1)}, u32[]{:S(2)}, u32[]{:S(2)}) collective-permute-start(bf16[128,2048]{1,0:T(8,128)(2,1)S(1)} %get-tuple-element.88), channel_id=1, source_target_pairs={{0,1},{1,0},{2,3},{3,2},{4,5},{5,4},{6,7},{7,6},{8,9},{9,8},{10,11... | collective-permute-start | bytes 1572872 | tf_op jit(solution)/shard_map/ppermute | solution.py:579
  139.9 19.5 %collective-permute-start.26 = (bf16[128,2048]{1,0:T(8,128)(2,1)S(1)}, bf16[128,2048]{1,0:T(8,128)(2,1)S(1)}, u32[]{:S(2)}, u32[]{:S(2)}) collective-permute-start(bf16[128,2048]{1,0:T(8,128)(2,1)S(1)} %get-tuple-element.86), channel_id=1, source_target_pairs={{0,1},{1,0},{2,3},{3,2},{4,5},{5,4},{6,7},{7,6},{8,9},{9,8},{10,11... | collective-permute-start | bytes 1572872 | tf_op jit(solution)/shard_map/ppermute | solution.py:589
  141.6 4.2 %collective-permute-start.24 = (bf16[128,1024]{1,0:T(8,128)(2,1)S(1)}, bf16[128,1024]{1,0:T(8,128)(2,1)S(1)}, u32[]{:S(2)}, u32[]{:S(2)}) collective-permute-start(bf16[128,1024]{1,0:T(8,128)(2,1)S(1)} %get-tuple-element.84), channel_id=1, source_target_pairs={{0,1},{1,0},{2,3},{3,2},{4,5},{5,4},{6,7},{7,6},{8,9},{9,8},{10,11... | collective-permute-start | bytes 786440 | tf_op jit(solution)/shard_map/ppermute | solution.py:579
  143.6 15.4 %collective-permute-start.18 = (bf16[128,2048]{1,0:T(8,128)(2,1)S(1)}, bf16[128,2048]{1,0:T(8,128)(2,1)S(1)}, u32[]{:S(2)}, u32[]{:S(2)}) collective-permute-start(bf16[128,2048]{1,0:T(8,128)(2,1)S(1)} %get-tuple-element.76), channel_id=1, source_target_pairs={{0,1},{1,0},{2,3},{3,2},{4,5},{5,4},{6,7},{7,6},{8,9},{9,8},{10,11... | collective-permute-start | bytes 1572872 | tf_op jit(solution)/shard_map/ppermute | solution.py:589
  144.2 9.2 %collective-permute-start.23 = (bf16[128,1024]{1,0:T(8,128)(2,1)S(1)}, bf16[128,1024]{1,0:T(8,128)(2,1)S(1)}, u32[]{:S(2)}, u32[]{:S(2)}) collective-permute-start(bf16[128,1024]{1,0:T(8,128)(2,1)S(1)} %add_convert_fusion.6), channel_id=1, source_target_pairs={{0,2},{1,3},{2,0},{3,1},{4,6},{5,7},{6,4},{7,5},{8,10},{9,11},{10,... | collective-permute-start | bytes 786440 | tf_op jit(solution)/shard_map/ppermute | solution.py:583
  145.8 13.2 %collective-permute-start.25 = (bf16[128,1024]{1,0:T(8,128)(2,1)S(1)}, bf16[128,1024]{1,0:T(8,128)(2,1)S(1)}, u32[]{:S(2)}, u32[]{:S(2)}) collective-permute-start(bf16[128,1024]{1,0:T(8,128)(2,1)S(1)} %add_convert_fusion.4), channel_id=1, source_target_pairs={{0,2},{1,3},{2,0},{3,1},{4,6},{5,7},{6,4},{7,5},{8,10},{9,11},{10,... | collective-permute-start | bytes 786440 | tf_op jit(solution)/shard_map/ppermute | solution.py:583
  146.6 18.1 %collective-permute-start.28 = (bf16[128,1024]{1,0:T(8,128)(2,1)S(1)}, bf16[128,1024]{1,0:T(8,128)(2,1)S(1)}, u32[]{:S(2)}, u32[]{:S(2)}) collective-permute-start(bf16[128,1024]{1,0:T(8,128)(2,1)S(1)} %get-tuple-element.92), channel_id=1, source_target_pairs={{0,2},{1,3},{2,0},{3,1},{4,6},{5,7},{6,4},{7,5},{8,10},{9,11},{10,... | collective-permute-start | bytes 786440 | tf_op jit(solution)/shard_map/ppermute | solution.py:583
  153.4 16.0 %collective-permute-start.29 = (bf16[128,1024]{1,0:T(8,128)(2,1)S(1)}, bf16[128,1024]{1,0:T(8,128)(2,1)S(1)}, u32[]{:S(2)}, u32[]{:S(2)}) collective-permute-start(bf16[128,1024]{1,0:T(8,128)(2,1)S(1)} %get-tuple-element.91), channel_id=1, source_target_pairs={{0,2},{1,3},{2,0},{3,1},{4,6},{5,7},{6,4},{7,5},{8,10},{9,11},{10,... | collective-permute-start | bytes 786440 | tf_op jit(solution)/shard_map/ppermute | solution.py:583
